TPU v7x, 512 devices: a whole 4x8x8 slice. The times are simulated.
512 devices in a mesh: ra: 64 (over z, y), cb: 4 (over x), dp: 2 (over core).
Axes of the slice: x: 4, y: 8, z: 8, core: 2. Of those that a mesh axis runs over, the one named last changes fastest.
Arguments:
- tokens: bfloat16 [2048, 4096], P('dp', 'cb'), may hold values from -3000 to 3000
- norm_gain: float32 [4096], P('cb'), may hold values from 0.1 to 1.9
- norm_bias: float32 [4096], P('cb'), may hold values from -2 to 2
- gate_weight: float32 [4096, 11264], P('cb', 'ra'), may hold values from -0.09375 to 0.09375
- up_weight: float32 [4096, 11264], P('cb', 'ra'), may hold values from -0.09375 to 0.09375
- gate_scale: float32 [11264], P('ra'), may hold values from 0.5 to 2
- up_scale: float32 [11264], P('ra'), may hold values from 0.5 to 2
- down_weight: float32 [11264, 4096], P('ra', 'cb'), may hold values from -0.0546875 to 0.0546875
- down_scale: float32 [4096], P('cb'), may hold values from 0.5 to 8
- out_gain: float32 [4096], P('cb'), may hold values from 0.1 to 1.9
- out_bias: float32 [4096], P('cb'), may hold values from -2 to 2
Outputs:
- result: bfloat16 [2048, 4096], P(('dp', 'ra'), 'cb')
All inputs are finite; a program needn't handle non-finite values.
Results may differ from a plain program's by a relative error of at most 0.018.
Values may be sent and summed in bfloat16 or wider, within the bound.
No kernel may reach another device: no remote copies, remote signals or barrier semaphores. Data moves between devices by JAX's collectives and lax.ppermute only.
A program may use at most 64 MiB of HBM per device.

v0:
```python
import jax
import jax.numpy as jnp
from jax import lax
from jax.sharding import PartitionSpec as P

D = 4096


def sent_to_all(shard, axis):
    length = lax.axis_size(axis)
    return lax.all_to_all(
        jnp.broadcast_to(shard[None], (length, *shard.shape)), axis, 0, 0, tiled=True
    )


def of_everyone(shard, axis):
    return sent_to_all(shard, axis).sum(axis=0)


def packed_total(arrays, axis):
    ends = [0]
    for a in arrays:
        ends.append(ends[-1] + a.size)
    total = of_everyone(jnp.concatenate([a.ravel() for a in arrays]), axis)
    return tuple((total[b:e].reshape(a.shape) for a, b, e in zip(arrays, ends, ends[1:])))


def cut_along(shard, dim, length):
    before, after = (shard.shape[:dim], shard.shape[dim + 1 :])
    return jnp.moveaxis(shard.reshape(*before, length, -1, *after), dim, 0)


def sum_at_owner(shard, axis, dim):
    length = lax.axis_size(axis)
    blocks = lax.all_to_all(cut_along(shard, dim, length), axis, 0, 0, tiled=True)
    return jnp.sum(blocks.astype(jnp.float32), axis=0)


def in_one_piece(arrays, axis, dim, along):
    widths = [a.shape[along] for a in arrays]
    both = jnp.concatenate(arrays, axis=along)
    result = sum_at_owner(both, axis, dim)
    return tuple(jnp.split(result, [sum(widths[:k]) for k in range(1, len(widths))], axis=along))


def laid_out(blocks, dim):
    blocks = jnp.moveaxis(blocks, 0, dim)
    dims = blocks.shape
    return blocks.reshape(*dims[:dim], dims[dim] * dims[dim + 1], *dims[dim + 2 :])


def gather_directly(shard, axis, dim):
    blocks = sent_to_all(shard, axis)
    return laid_out(blocks, dim)


def standardize(values):
    total, squares = packed_total((jnp.sum(values, axis=1), jnp.sum(values * values, axis=1)), "cb")
    mean = total / D
    spread = squares / D - mean * mean
    centred = values - mean[:, None]
    return centred * lax.rsqrt(spread + 1e-05)[:, None]


def local(
    tokens,
    norm_gain,
    norm_bias,
    gate_weight,
    up_weight,
    gate_scale,
    up_scale,
    down_weight,
    down_scale,
    out_gain,
    out_bias,
):
    normed = (standardize(tokens.astype(jnp.float32)) * norm_gain + norm_bias).astype(jnp.bfloat16)
    gate_part = jnp.dot(
        normed, gate_weight.astype(jnp.bfloat16), preferred_element_type=jnp.float32
    )
    up_part = jnp.dot(normed, up_weight.astype(jnp.bfloat16), preferred_element_type=jnp.float32)
    gate_share, up_share = in_one_piece(
        (gate_part.astype(jnp.bfloat16), up_part.astype(jnp.bfloat16)), "cb", 1, 0
    )
    share = gate_share.shape[1]
    offset = lax.axis_index("cb") * share
    gate_cols = lax.dynamic_slice_in_dim(gate_scale, offset, share, 0)
    up_cols = lax.dynamic_slice_in_dim(up_scale, offset, share, 0)
    hidden_share = (jax.nn.silu(gate_share * gate_cols) * (up_share * up_cols)).astype(jnp.bfloat16)
    hidden = gather_directly(hidden_share, "cb", 1)
    down_local = down_weight.astype(jnp.bfloat16)
    own_rows = hidden.shape[0] // lax.axis_size("ra")
    branch = (
        sum_at_owner(
            jnp.dot(hidden, down_local, preferred_element_type=jnp.float32).astype(jnp.bfloat16),
            "ra",
            0,
        )
        * down_scale
    )
    own_normed = lax.dynamic_slice_in_dim(normed, lax.axis_index("ra") * own_rows, own_rows, 0)
    mixed = 0.5 * own_normed.astype(jnp.float32) + branch
    return (standardize(mixed) * out_gain + out_bias).astype(jnp.bfloat16)


def solution(mesh):
    return jax.shard_map(
        local,
        mesh=mesh,
        in_specs=(
            P("dp", "cb"),
            P("cb"),
            P("cb"),
            P("cb", "ra"),
            P("cb", "ra"),
            P("ra"),
            P("ra"),
            P("ra", "cb"),
            P("cb"),
            P("cb"),
            P("cb"),
        ),
        out_specs=P(("dp", "ra"), "cb"),
        check_vma=False,
    )
```

profile of v0, /device:TPU:8, one launch (start us, length us, event | category | flops | bytes accessed | tf_op | source)
XLA Modules:
  0.0 120.9 jit_solution(5314449743315698336)
XLA Ops:
  0.0 0.0 copy-start.5
  0.0 0.0 copy-start.6
  0.0 2.3 %convert_reduce_fusion = (f32[1024]{0:T(1024)S(1)}, f32[1024]{0:T(1024)S(1)}) fusion(bf16[1024,1024]{1,0:T(8,128)(2,1)} %param.11), kind=kLoop, calls=%fused_computation.2 | loop fusion | flops 4192256 | bytes 2105344 | tf_op jit(solution)/shard_map/reduce_sum | solution.py:58
  2.3 9.5 %all_to_all.27 = f32[4,1,2048]{2,1,0:T(1,128)S(1)} all-to-all(f32[4,1,2048]{2,1,0:T(1,128)S(1)} %broadcast_in_dim.6), channel_id=1, replica_groups=mesh['ra'=64,'cb'=4,'dp'=2] {'cb'}, dimensions={0} | all-to-all | bytes 65536 | tf_op jit(solution)/shard_map/all_to_all | solution.py:11
  11.9 0.0 copy-done.5
  11.9 0.0 copy-done.6
  11.9 0.0 copy-start
  12.0 2.5 %fusion.4 = bf16[1024,1024]{1,0:T(8,128)(2,1)S(1)} fusion(bf16[1024,1024]{1,0:T(8,128)(2,1)} %param.11, f32[1024]{0:T(1024)S(1)} %copy-done.5, f32[1024]{0:T(1024)S(1)} %copy-done.6, f32[1024]{0:T(1024)S(1)} %get-tuple-element.10, f32[1024]{0:T(1024)S(1)} %get-tuple-element.9), kind=kLoop, calls=%fused_computation.7 | loop fusion | flops 6291456 | bytes 4210688 | tf_op jit(solution)/shard_map/convert_element_type | solution.py:78
  14.4 0.0 copy-done
  14.5 0.0 copy-start.1
  14.5 0.9 convolution_convert_fusion.1
  15.3 0.2 copy-done.1
  15.6 0.8 convolution_convert_fusion.2
  16.4 0.0 copy-start.7
  16.4 0.0 copy-start.8
  16.4 0.1 pad_maximum_fusion
  16.5 1.0 reshape.33
  17.5 3.5 %all-to-all-start.1 = ((bf16[4,2048,44]{1,2,0:T(8,128)(2,1)}), bf16[4,2048,44]{1,2,0:T(8,128)(2,1)S(1)}, u32[]{:S(2)}, u32[]{:S(2)}) async-start(bf16[4,2048,44]{1,2,0:T(8,128)(2,1)} %bitcast.12), calls=%async_computation.1 | async-start | bytes 1572864 | tf_op jit(solution)/shard_map/all_to_all | solution.py:35
  21.0 0.0 copy-done.7
  21.0 0.1 dynamic_slice.10
  21.1 0.0 copy-done.8
  21.1 0.1 dynamic_slice.11
  21.2 10.9 %all-to-all-done.1 = bf16[4,2048,44]{1,2,0:T(8,128)(2,1)S(1)} async-done(((bf16[4,2048,44]{1,2,0:T(8,128)(2,1)}), bf16[4,2048,44]{1,2,0:T(8,128)(2,1)S(1)}, u32[]{:S(2)}, u32[]{:S(2)}) %all-to-all-start.1) | async-done | bytes 720928 | tf_op jit(solution)/shard_map/all_to_all | solution.py:35
  32.1 0.1 convert_reduce_fusion.2
  32.2 0.1 fusion.9
  32.4 9.8 %all_to_all.28 = bf16[4,1024,44]{1,2,0:T(8,128)(2,1)S(1)} all-to-all(bf16[4,1024,44]{1,2,0:T(8,128)(2,1)S(1)} %broadcast_in_dim.7), channel_id=1, replica_groups=mesh['ra'=64,'cb'=4,'dp'=2] {'cb'}, dimensions={0} | all-to-all | bytes 720896 | tf_op jit(solution)/shard_map/all_to_all | solution.py:11
  42.2 0.1 reshape.34
  42.3 3.2 %convolution_convert_fusion = bf16[1024,1024]{1,0:T(8,128)(2,1)} fusion(bf16[1024,176]{0,1:T(8,128)(2,1)S(1)} %reshape.34, f32[176,1024]{1,0:T(8,128)} %param.18), kind=kOutput, calls=%fused_computation.9 | convolution fusion | flops 370327552 | bytes 3178496 | tf_op jit(solution)/shard_map/dot_general | solution.py:96
  45.4 16.8 %all-to-all-start.3 = ((bf16[64,16,1024]{2,1,0:T(8,128)(2,1)}), bf16[64,16,1024]{2,1,0:T(8,128)(2,1)}, u32[]{:S(2)}, u32[]{:S(2)}) async-start(bf16[64,16,1024]{2,1,0:T(8,128)(2,1)} %bitcast.11), calls=%async_computation.3 | async-start | bytes 4194304 | tf_op jit(solution)/shard_map/all_to_all | solution.py:35
  62.2 0.0 copy-start.2
  62.2 0.0 copy-start.3
  62.2 0.0 copy-start.4
  62.3 48.1 %all-to-all-done.3 = bf16[64,16,1024]{2,1,0:T(8,128)(2,1)} async-done(((bf16[64,16,1024]{2,1,0:T(8,128)(2,1)}), bf16[64,16,1024]{2,1,0:T(8,128)(2,1)}, u32[]{:S(2)}, u32[]{:S(2)}) %all-to-all-start.3) | async-done | bytes 2097184 | tf_op jit(solution)/shard_map/all_to_all | solution.py:35
  110.3 1.9 %convert_reduce_fusion.1 = f32[16,1024]{1,0:T(8,128)S(1)} fusion(bf16[64,16,1024]{2,1,0:T(8,128)(2,1)} %all-to-all-done.3), kind=kLoop, calls=%fused_computation.8 | loop fusion | flops 2080768 | bytes 2162688 | tf_op jit(solution)/shard_map/reduce_sum | solution.py:36
  112.3 0.0 copy-done.2
  112.3 0.1 fusion.13
  112.4 0.1 pad_maximum_fusion.2
  112.5 7.6 %all_to_all.29 = f32[4,1,32]{2,1,0:T(1,128)S(1)} all-to-all(f32[4,1,32]{2,1,0:T(1,128)S(1)} %broadcast_in_dim.8), channel_id=1, replica_groups=mesh['ra'=64,'cb'=4,'dp'=2] {'cb'}, dimensions={0} | all-to-all | bytes 1024 | tf_op jit(solution)/shard_map/all_to_all | solution.py:11
  120.1 0.1 slice_multiply_fusion.4
  120.2 0.0 copy-done.3
  120.2 0.0 copy-done.4
  120.2 0.7 add_convert_fusion
  (7 shorter events, 0.1 us)
Async XLA Ops:
  0.0 11.9 %copy-start.5 = (f32[1024]{0:T(1024)S(1)}, f32[1024]{0:T(1024)}, u32[]{:S(2)}) copy-start(f32[1024]{0:T(1024)} %param.13) | copy-start | bytes 12292
  0.0 11.9 %copy-start.6 = (f32[1024]{0:T(1024)S(1)}, f32[1024]{0:T(1024)}, u32[]{:S(2)}) copy-start(f32[1024]{0:T(1024)} %param.12) | copy-start | bytes 12292
  11.9 2.5 %copy-start = (f32[1024,176]{0,1:T(8,128)S(1)}, f32[1024,176]{0,1:T(8,128)}, u32[]{:S(2)}) copy-start(f32[1024,176]{0,1:T(8,128)} %param.15) | copy-start | bytes 2162692
  14.5 1.1 copy-start.1
  16.4 4.6 %copy-start.7 = (f32[176]{0:T(256)S(1)}, f32[176]{0:T(256)}, u32[]{:S(2)}) copy-start(f32[176]{0:T(256)} %param.16) | copy-start | bytes 2116
  16.4 4.7 %copy-start.8 = (f32[176]{0:T(256)S(1)}, f32[176]{0:T(256)}, u32[]{:S(2)}) copy-start(f32[176]{0:T(256)} %param.17) | copy-start | bytes 2116
  17.5 14.6 %all-to-all-start.1 = ((bf16[4,2048,44]{1,2,0:T(8,128)(2,1)}), bf16[4,2048,44]{1,2,0:T(8,128)(2,1)S(1)}, u32[]{:S(2)}, u32[]{:S(2)}) async-start(bf16[4,2048,44]{1,2,0:T(8,128)(2,1)} %bitcast.12), calls=%async_computation.1 | async-start | bytes 1572864 | tf_op jit(solution)/shard_map/all_to_all | solution.py:35
  45.4 64.9 %all-to-all-start.3 = ((bf16[64,16,1024]{2,1,0:T(8,128)(2,1)}), bf16[64,16,1024]{2,1,0:T(8,128)(2,1)}, u32[]{:S(2)}, u32[]{:S(2)}) async-start(bf16[64,16,1024]{2,1,0:T(8,128)(2,1)} %bitcast.11), calls=%async_computation.3 | async-start | bytes 4194304 | tf_op jit(solution)/shard_map/all_to_all | solution.py:35
  62.2 50.1 %copy-start.2 = (f32[1024]{0:T(1024)S(1)}, f32[1024]{0:T(1024)}, u32[]{:S(2)}) copy-start(f32[1024]{0:T(1024)} %param.19) | copy-start | bytes 12292
  62.2 58.0 %copy-start.3 = (f32[1024]{0:T(1024)S(1)}, f32[1024]{0:T(1024)}, u32[]{:S(2)}) copy-start(f32[1024]{0:T(1024)} %param.21) | copy-start | bytes 12292
  62.2 58.0 %copy-start.4 = (f32[1024]{0:T(1024)S(1)}, f32[1024]{0:T(1024)}, u32[]{:S(2)}) copy-start(f32[1024]{0:T(1024)} %param.20) | copy-start | bytes 12292
where the time goes:
time: 121 us
  waiting for transfers between devices  59 us (49%)
  blocking collectives  26.9 us (22%)
  starting transfers between devices  20.3 us (17%)
  other arithmetic  8.08 us (7%)
  matrix products  4.86 us (4%)
  local copies, waits for them, and re-layouts  1.6 us (1%)
    all_to_all x2, waiting for transfers between devices, sum_at_owner(): lax.all_to_all(cut_along(shard, dim, length), axis, 0, 0, tiled=True)  59 us
    all_to_all x3, blocking collectives, sent_to_all(): lax.all_to_all(jnp.broadcast_to(shard[None], (length, *shard.shape)), axi...  26.9 us
    all_to_all x2, starting transfers between devices, sum_at_owner(): lax.all_to_all(cut_along(shard, dim, length), axis, 0, 0, tiled=True)  20.3 us
    dot_general x1, matrix products, local(): jnp.dot(hidden, down_local, preferred_element_type=jnp.float32)  3.16 us
    convert_element_type x1, other arithmetic, local(): (standardize(tokens.astype(jnp.float32)) * norm_gain + norm_bias).astype(...  2.48 us
  transfers between devices with their start and end apart: 2, of which 2 were waited for; matrix products, arithmetic and copies ran while one was open for 0% of the time, Pallas kernels for 0%

commit v1 on v0

v1 whole, which is shorter than its diff:
```python
import jax
import jax.numpy as jnp
from jax import lax
from jax.experimental import pallas as pl
from jax.experimental.pallas import tpu as pltpu
from jax.sharding import Mesh, PartitionSpec as P

D = 4096
F32 = jnp.float32
BF16 = jnp.bfloat16
RA = ("Z", "zl", "Y", "yl")
UNITS = 44
SLOT = 48
PART = 2 * SLOT
ROWS = 1024
COLS = 1024
FFL = 176
CHUNK = 256


def iota(shape, dim):
    return lax.broadcasted_iota(jnp.int32, shape, dim)


def dot(a, b, ca, cb):
    return lax.dot_general(a, b, (((ca,), (cb,)), ((), ())), preferred_element_type=F32)


def rounded(v):
    return v.astype(BF16).astype(F32)


def one_hot(cond):
    return jnp.where(cond, 1.0, 0.0).astype(BF16)


def project_kernel(x_ref, gw_ref, uw_ref, gain_ref, bias_ref, out_ref, w_ref, vec_ref):
    step = pl.program_id(0)

    @pl.when(step == 0)
    def _():
        gw = gw_ref[...].astype(BF16)
        uw = uw_ref[...].astype(BF16)
        row = iota((PART, FFL), 0)
        col = iota((PART, FFL), 1)
        for k in range(4):
            unit = col - UNITS * k
            as_gate = one_hot((unit == row) & (row < UNITS))
            as_up = one_hot((unit == row - SLOT) & (row >= SLOT) & (row < SLOT + UNITS))
            w = dot(as_gate, gw, 1, 0) + dot(as_up, uw, 1, 0)
            w_ref[PART * k : PART * (k + 1), :] = w.astype(BF16)
        gain = gain_ref[...]
        bias = bias_ref[...]
        r = iota((8, COLS), 0)
        gh = rounded(gain)
        bh = rounded(bias)
        lead = jnp.where(r == 0, gh, jnp.where(r == 1, gain - gh, jnp.where(r == 2, bh, jnp.where(r == 3, bias - bh, 0.0))))
        sums = dot(lead.astype(BF16), w_ref[...], 1, 1)
        both = jnp.concatenate(
            [sums[0:1] + sums[1:2], sums[2:3] + sums[3:4], jnp.zeros((1, ROWS - 8 * PART), F32)], axis=1
        )
        hi = rounded(both)
        q = iota((8, ROWS), 0)
        vec_ref[...] = jnp.where(q == 0, hi, jnp.where(q == 1, both - hi, 0.0))

    x = x_ref[...].reshape(CHUNK, COLS).astype(F32)
    m = jnp.sum(x, axis=1, keepdims=True) * (1.0 / COLS)
    xc = x - m
    m2 = jnp.sum(xc * xc, axis=1, keepdims=True)
    xn = (xc * gain_ref[...]).astype(BF16)
    part = dot(w_ref[...], xn, 1, 1)
    lane = iota((CHUNK, 128), 1)
    stat = jnp.where(lane == 0, m, jnp.where(lane == 1, m2, 0.0)).T
    m_row = stat[0:1]
    m2_row = stat[1:2]
    m_hi = rounded(m_row)
    m_mid = rounded(m_row - m_hi)
    m_lo = m_row - m_hi - m_mid
    m2_hi = rounded(m2_row)
    m2_lo = m2_row - m2_hi
    vec = vec_ref[:, pl.ds(pl.multiple_of(step * CHUNK, CHUNK), CHUNK)]
    r = iota((8, CHUNK), 0)
    t1 = jnp.where(r == 4, m_hi, jnp.where(r == 5, m_mid, jnp.where(r == 6, m_lo, jnp.where(r == 7, vec[0:1], 0.0))))
    t2 = jnp.where(r == 4, m2_hi, jnp.where(r == 5, m2_lo, jnp.where(r == 6, vec[1:2], 0.0)))
    z = jnp.zeros((SLOT - 8, CHUNK), F32)
    extra = jnp.concatenate([z, t1, z, t2], axis=0)
    for k in range(4):
        out_ref[k] = (part[PART * k : PART * (k + 1)] + extra).astype(BF16)


def project(tokens, gate_t, up_t, gain, bias):
    x = tokens.reshape(4, 2, 4, 2, 16, COLS)
    return pl.pallas_call(
        project_kernel,
        grid=(4,),
        in_specs=[
            pl.BlockSpec((4, 1, 4, 1, 16, COLS), lambda j: (0, j // 2, 0, j % 2, 0, 0)),
            pl.BlockSpec((FFL, COLS), lambda j: (0, 0)),
            pl.BlockSpec((FFL, COLS), lambda j: (0, 0)),
            pl.BlockSpec((1, COLS), lambda j: (0, 0)),
            pl.BlockSpec((1, COLS), lambda j: (0, 0)),
        ],
        out_specs=pl.BlockSpec((4, PART, CHUNK), lambda j: (0, 0, j)),
        out_shape=jax.ShapeDtypeStruct((4, PART, ROWS), BF16),
        scratch_shapes=[pltpu.VMEM((4 * PART, COLS), BF16), pltpu.VMEM((8, ROWS), F32)],
        compiler_params=pltpu.CompilerParams(dimension_semantics=("arbitrary",)),
        name="project",
    )(x, gate_t, up_t, gain, bias)


def hidden_kernel(idx_ref, r_ref, gs_ref, us_ref, out_ref, stat_ref):
    me = idx_ref[0]
    means = []
    m2s = []
    for c in range(4):
        a = r_ref[c, 32:48, :].astype(F32)
        b = r_ref[c, 80:96, :].astype(F32)
        means.append(a[12:13] + a[13:14] + a[14:15])
        m2s.append(b[12:13] + b[13:14])
    mean = (means[0] + means[1] + means[2] + means[3]) * 0.25
    deltas = [v - mean for v in means]
    m2 = sum(m2s) + COLS * sum(d * d for d in deltas)
    rstd = lax.rsqrt(m2 * (1.0 / D) + 1e-05)
    q = iota((8, ROWS), 0)
    stat_ref[...] = jnp.where(q == 0, mean, jnp.where(q == 1, rstd, 0.0))

    wide = 8 * PART
    pick_row = iota((2 * PART, wide), 0)
    pick_lane = iota((2 * PART, wide), 1)
    base = jnp.where(pick_row < PART, me * PART, (4 + me) * PART - PART)
    pick = one_hot(pick_lane == pick_row + base)
    tiles = [r_ref[c, 32:48, 0:wide] for c in range(4)] + [r_ref[c, 80:96, 0:wide] for c in range(4)]
    vecs = dot(pick, jnp.concatenate(tiles, axis=0), 1, 1)
    col_sums = [vecs[0:PART, 16 * c + 15 : 16 * c + 16] + vecs[0:PART, 78 + 16 * c : 79 + 16 * c] for c in range(4)]
    biases = sum(vecs[PART:, 16 * c + 15 : 16 * c + 16] + vecs[PART:, 78 + 16 * c : 79 + 16 * c] for c in range(4))

    gs = gs_ref[...]
    us = us_ref[...]
    g1 = rounded(gs)
    g2 = rounded(gs - g1)
    u1 = rounded(us)
    u2 = rounded(us - u1)
    sr = iota((16, FFL), 0)
    pieces = jnp.where(sr == 0, g1, jnp.where(sr == 1, g2, jnp.where(sr == 2, gs - g1 - g2, 0.0)))
    pieces = pieces + jnp.where(sr == 3, u1, jnp.where(sr == 4, u2, jnp.where(sr == 5, us - u1 - u2, 0.0)))
    row = iota((PART, FFL), 0)
    unit = jnp.where(row < SLOT, row, row - SLOT)
    own = one_hot((iota((PART, FFL), 1) == unit + me * UNITS) & (unit < UNITS))
    sc = dot(own, pieces.astype(BF16), 1, 1)
    scale = jnp.where(iota((PART, 1), 0) < SLOT, sc[:, 0:1] + sc[:, 1:2] + sc[:, 2:3], sc[:, 3:4] + sc[:, 4:5] + sc[:, 5:6])

    keep = iota((SLOT, CHUNK), 0) < UNITS
    for j in range(4):
        at = slice(CHUNK * j, CHUNK * (j + 1))
        acc = jnp.zeros((PART, CHUNK), F32)
        for c in range(4):
            acc = acc + (r_ref[c, :, at].astype(F32) + col_sums[c] * deltas[c][:, at])
        y = (acc * rstd[:, at] + biases) * scale
        gate = y[0:SLOT]
        up = y[SLOT:PART]
        h = jnp.where(keep, gate / (1.0 + jnp.exp(-gate)) * up, 0.0).astype(BF16)
        for k in range(4):
            out_ref[j, k] = h


def hidden_of(idx, received, gate_scale, up_scale):
    vm = pl.BlockSpec(memory_space=pltpu.VMEM)
    return pl.pallas_call(
        hidden_kernel,
        in_specs=[pl.BlockSpec(memory_space=pltpu.SMEM), vm, vm, vm],
        out_specs=[vm, vm],
        out_shape=[jax.ShapeDtypeStruct((4, 4, SLOT, CHUNK), BF16), jax.ShapeDtypeStruct((8, ROWS), F32)],
        name="hidden",
    )(idx, received, gate_scale, up_scale)


def down_kernel(idx_ref, h_ref, w0_ref, w1_ref, w2_ref, w3_ref, out_ref):
    me = idx_ref[1]
    row = iota((FFL, 4 * SLOT), 0)
    lane = iota((FFL, 4 * SLOT), 1)
    hit = lane < 0
    for k in range(4):
        hit = hit | ((lane == row + (SLOT - UNITS) * k) & (row >= UNITS * k) & (row < UNITS * (k + 1)))
    squeeze = one_hot(hit)
    acc = jnp.zeros((CHUNK, COLS), F32)
    for r, w_ref in enumerate((w0_ref, w1_ref, w2_ref, w3_ref)):
        h = dot(h_ref[me ^ r], squeeze, 0, 1).astype(BF16)
        acc = acc + dot(h, w_ref[...], 1, 0)
    out_ref[...] = acc.astype(BF16)


def down(idx, hidden, weights):
    vm = pl.BlockSpec(memory_space=pltpu.VMEM)
    return pl.pallas_call(
        down_kernel,
        in_specs=[pl.BlockSpec(memory_space=pltpu.SMEM)] + [vm] * 5,
        out_specs=vm,
        out_shape=jax.ShapeDtypeStruct((CHUNK, COLS), BF16),
        name="down",
    )(idx, hidden, *weights)


def mix_kernel(idx_ref, r_ref, x_ref, stat_ref, gain_ref, bias_ref, scale_ref, mixed_ref, part_ref):
    branch = jnp.zeros((16, COLS), F32)
    for k in range(16):
        branch = branch + r_ref[k].astype(F32)
    mine = iota((16, ROWS), 1) == iota((16, ROWS), 0) + idx_ref[2]
    mean = jnp.sum(jnp.where(mine, stat_ref[0:1], 0.0), axis=1, keepdims=True)
    rstd = jnp.sum(jnp.where(mine, stat_ref[1:2], 0.0), axis=1, keepdims=True)
    normed = rounded((x_ref[0].astype(F32) - mean) * rstd * gain_ref[...] + bias_ref[...])
    mixed = 0.5 * normed + branch * scale_ref[...]
    mixed_ref[...] = mixed
    m = jnp.sum(mixed, axis=1, keepdims=True) * (1.0 / COLS)
    c = mixed - m
    m2 = jnp.sum(c * c, axis=1, keepdims=True)
    lane = iota((16, 128), 1)
    part = jnp.where(lane == 0, m, jnp.where(lane == 1, m2, 0.0))
    for k in range(4):
        part_ref[k] = part


def mix(idx, received, tokens, stats, gain, bias, scale):
    row = pl.BlockSpec((1, COLS), lambda i, s: (0, 0))
    return pl.pallas_call(
        mix_kernel,
        grid_spec=pltpu.PrefetchScalarGridSpec(
            num_scalar_prefetch=1,
            grid=(1,),
            in_specs=[
                pl.BlockSpec((16, 16, COLS), lambda i, s: (0, 0, 0)),
                pl.BlockSpec((1, 16, COLS), lambda i, s: (s[3], 0, 0)),
                pl.BlockSpec((8, ROWS), lambda i, s: (0, 0)),
                row,
                row,
                row,
            ],
            out_specs=[
                pl.BlockSpec((16, COLS), lambda i, s: (0, 0)),
                pl.BlockSpec((4, 16, 128), lambda i, s: (0, 0, 0)),
            ],
        ),
        out_shape=[jax.ShapeDtypeStruct((16, COLS), F32), jax.ShapeDtypeStruct((4, 16, 128), F32)],
        name="mix",
    )(idx, received, tokens.reshape(64, 16, COLS), stats, gain, bias, scale)


def finish_kernel(mixed_ref, part_ref, gain_ref, bias_ref, out_ref):
    parts = [part_ref[k] for k in range(4)]
    means = [p[:, 0:1] for p in parts]
    mean = (means[0] + means[1] + means[2] + means[3]) * 0.25
    m2 = sum(p[:, 1:2] for p in parts) + COLS * sum((v - mean) * (v - mean) for v in means)
    rstd = lax.rsqrt(m2 * (1.0 / D) + 1e-05)
    out_ref[...] = ((mixed_ref[...] - mean) * rstd * gain_ref[...] + bias_ref[...]).astype(BF16)


def finish(mixed, parts, gain, bias):
    vm = pl.BlockSpec(memory_space=pltpu.VMEM)
    return pl.pallas_call(
        finish_kernel,
        in_specs=[vm] * 4,
        out_specs=vm,
        out_shape=jax.ShapeDtypeStruct((16, COLS), BF16),
        name="finish",
    )(mixed, parts, gain, bias)


def swapped(n, k):
    return [(i, i ^ k) for i in range(n)]


def local(
    tokens,
    norm_gain,
    norm_bias,
    gate_weight,
    up_weight,
    gate_scale,
    up_scale,
    down_weight,
    down_scale,
    out_gain,
    out_bias,
):
    x_at = lax.axis_index("cb")
    member = lax.axis_index(("zl", "yl"))
    block = lax.axis_index(("Z", "Y"))
    idx = jnp.stack([x_at, member, member * CHUNK + block * 16, lax.axis_index(RA)]).astype(jnp.int32)
    gain = norm_gain.reshape(1, COLS)
    bias = norm_bias.reshape(1, COLS)

    w0 = down_weight.astype(BF16)
    w1 = lax.ppermute(w0, "yl", swapped(2, 1))
    w2 = lax.ppermute(w0, "zl", swapped(2, 1))
    w3 = lax.ppermute(w0, ("zl", "yl"), swapped(4, 3))

    shares = project(tokens, gate_weight.T, up_weight.T, gain, bias)
    received = lax.all_to_all(shares, "cb", 0, 0, tiled=True)
    sent, stats = hidden_of(idx, received, gate_scale.reshape(1, FFL), up_scale.reshape(1, FFL))
    hidden = lax.all_to_all(sent.reshape(16, SLOT, CHUNK), ("zl", "yl", "cb"), 0, 0, tiled=True)
    partial = down(idx, hidden.reshape(4, 4 * SLOT, CHUNK), (w0, w1, w2, w3))
    pieces = lax.all_to_all(partial.reshape(16, 16, COLS), ("Z", "Y"), 0, 0, tiled=True)
    mixed, part = mix(idx, pieces, tokens, stats, gain, bias, down_scale.reshape(1, COLS))
    parts = lax.all_to_all(part, "cb", 0, 0, tiled=True)
    return finish(mixed, parts, out_gain.reshape(1, COLS), out_bias.reshape(1, COLS))


def solution(mesh):
    split = Mesh(mesh.devices.reshape(4, 2, 4, 2, 4, 2), RA + ("cb", "dp"))
    return jax.shard_map(
        local,
        mesh=split,
        in_specs=(
            P("dp", "cb"),
            P("cb"),
            P("cb"),
            P("cb", RA),
            P("cb", RA),
            P(RA),
            P(RA),
            P(RA, "cb"),
            P("cb"),
            P("cb"),
            P("cb"),
        ),
        out_specs=P(("dp",) + RA, "cb"),
        check_vma=False,
    )
```

time: 121 us -> 104 us (0.86)
  waiting for transfers between devices: 59 us -> 23.1 us
  Pallas kernels: 0 us -> 16.3 us
  blocking collectives: 26.9 us -> 42.1 us
  other arithmetic: 8.08 us -> 0.7 us
  matrix products: 4.86 us -> 0 us
    all_to_all x2, waiting for transfers between devices: 59 us -> 11.6 us  [the longest x1 11.6 us: local(): received = lax.all_to_all(shares, 'cb', 0, 0, tiled=True)]
    pallas_call x0 -> x5, Pallas kernels: none -> 16.3 us  [the longest x1 6.05 us: project(): pl.pallas_call(project_kernel, grid=(4,), in_specs=[pl.BlockSpec((4, 1, 4...]
    all_to_all x3 -> x2, blocking collectives: 26.9 us -> 42.1 us  [the longest x1 32.2 us: local(): lax.all_to_all(partial.reshape(16, 16, COLS), ('Z', 'Y'), 0, 0, tiled=True)]
    ppermute x0 -> x3, waiting for transfers between devices: none -> 11.5 us  [the longest x1 6.13 us: local(): w2 = lax.ppermute(w0, 'zl', swapped(2, 1))]
    all_to_all x2, starting transfers between devices: 20.3 us -> 10.1 us  [the longest x1 5.73 us: local(): lax.all_to_all(sent.reshape(16, SLOT, CHUNK), ('zl', 'yl', 'cb'), 0, 0, t...]
    ppermute x0 -> x3, starting transfers between devices: none -> 9.21 us  [the longest x1 3.83 us: local(): w2 = lax.ppermute(w0, 'zl', swapped(2, 1))]
    dot_general x3 -> x0, matrix products: 4.86 us -> none  [the longest x1 3.16 us: local(): jnp.dot(hidden, down_local, preferred_element_type=jnp.float32)]
    reduce_sum x6 -> x0, other arithmetic: 4.55 us -> none  [the longest x2 2.42 us: standardize(): jnp.sum(values, axis=1)]
  transfers between devices with their start and end apart: 2 -> 5, of which waited for: 2 -> 4; matrix products, arithmetic and copies ran while one was open for 0% -> 1% of each run, Pallas kernels for 0% -> 0%
where the time goes in v1:
time: 104 us; the launch traced here: 103 us
  blocking collectives  42.1 us (40%)
  waiting for transfers between devices  23.1 us (22%)
  starting transfers between devices  19.4 us (19%)
  Pallas kernels  16.3 us (16%)
  local copies, waits for them, and re-layouts  1.76 us (2%)
    all_to_all x1, blocking collectives, local(): lax.all_to_all(partial.reshape(16, 16, COLS), ('Z', 'Y'), 0, 0, tiled=True)  32.2 us
    all_to_all x1, waiting for transfers between devices, local(): received = lax.all_to_all(shares, 'cb', 0, 0, tiled=True)  11.6 us
    all_to_all x1, blocking collectives, local(): parts = lax.all_to_all(part, 'cb', 0, 0, tiled=True)  9.87 us
    ppermute x1, waiting for transfers between devices, local(): w2 = lax.ppermute(w0, 'zl', swapped(2, 1))  6.13 us
    pallas_call x1, Pallas kernels, project(): pl.pallas_call(project_kernel, grid=(4,), in_specs=[pl.BlockSpec((4, 1, 4...  6.05 us
    all_to_all x1, starting transfers between devices, local(): lax.all_to_all(sent.reshape(16, SLOT, CHUNK), ('zl', 'yl', 'cb'), 0, 0, t...  5.73 us
    all_to_all x1, starting transfers between devices, local(): received = lax.all_to_all(shares, 'cb', 0, 0, tiled=True)  4.42 us
    ppermute x1, waiting for transfers between devices, local(): w1 = lax.ppermute(w0, 'yl', swapped(2, 1))  3.94 us
  transfers between devices with their start and end apart: 5, of which 4 were waited for; matrix products, arithmetic and copies ran while one was open for 1% of the time, Pallas kernels for 0%

profile of v1, /device:TPU:8, one launch (start us, length us, event | category | flops | bytes accessed | tf_op | source)
XLA Modules:
  0.0 103.4 jit_solution(1464637592979538865)
XLA Ops:
  0.0 6.1 %project.1 = bf16[4,96,1024]{2,1,0:T(8,128)(2,1)} custom-call(bf16[4,2,4,2,16,1024]{5,4,3,2,1,0:T(8,128)(2,1)} %bitcast.18, f32[176,1024]{1,0:T(8,128)} %bitcast.22, f32[176,1024]{1,0:T(8,128)} %bitcast.23, f32[1,1024]{1,0:T(1,128)} %bitcast.25, f32[1,1024]{1,0:T(1,128)} %bitcast.27), custom_call_target="tpu_custom_call" | custom-call | tf_op jit(solution)/shard_map/project/pallas_call | solution.py:93
  6.1 0.0 copy-start.3
  6.1 4.4 %all-to-all-start = ((bf16[4,96,1024]{2,1,0:T(8,128)(2,1)}), bf16[4,96,1024]{2,1,0:T(8,128)(2,1)S(1)}, u32[]{:S(2)}, u32[]{:S(2)}) async-start(bf16[4,96,1024]{2,1,0:T(8,128)(2,1)} %project.1), calls=%async_computation | async-start | bytes 1572864 | tf_op jit(solution)/shard_map/all_to_all | solution.py:297
  10.5 0.6 pad_add_fusion.idx_ref
  11.1 11.6 %all-to-all-done.r_ref = bf16[4,96,1024]{2,1,0:T(8,128)(2,1)S(1)} async-done(((bf16[4,96,1024]{2,1,0:T(8,128)(2,1)}), bf16[4,96,1024]{2,1,0:T(8,128)(2,1)S(1)}, u32[]{:S(2)}, u32[]{:S(2)}) %all-to-all-start) | async-done | bytes 786464 | tf_op jit(solution)/shard_map/all_to_all | solution.py:297
  22.8 0.0 copy-start
  22.8 0.9 copy-done
  23.7 2.6 %hidden.1 = (bf16[4,4,48,256]{3,2,1,0:T(8,128)(2,1)}, f32[8,1024]{1,0:T(8,128)}) custom-call(s32[4]{0:T(128)} %pad_add_fusion.idx_ref, bf16[4,96,1024]{2,1,0:T(8,128)(2,1)} %copy-done, f32[1,176]{1,0:T(1,128)} %bitcast.32, f32[1,176]{1,0:T(1,128)} %bitcast.33), custom_call_target="tpu_custom_call" | custom-call | tf_op jit(solution)/shard_map/hidden/pallas_call | solution.py:168
  26.3 5.7 %all-to-all-start.1 = ((bf16[16,48,256]{2,1,0:T(8,128)(2,1)}), bf16[16,48,256]{2,1,0:T(8,128)(2,1)S(1)}, u32[]{:S(2)}, u32[]{:S(2)}) async-start(bf16[16,48,256]{2,1,0:T(8,128)(2,1)} %bitcast.24), calls=%async_computation.1 | async-start | bytes 786432 | tf_op jit(solution)/shard_map/all_to_all | solution.py:299
  32.0 0.0 copy-done.3
  32.1 0.0 copy-start.2
  32.1 2.0 %collective-permute-start = (bf16[176,1024]{1,0:T(8,128)(2,1)S(1)}, bf16[176,1024]{1,0:T(8,128)(2,1)S(1)}, u32[]{:S(2)}, u32[]{:S(2)}) collective-permute-start(bf16[176,1024]{1,0:T(8,128)(2,1)S(1)} %convert_element_type.3.w0_ref), channel_id=1, source_target_pairs={{0,8},{8,0},{1,9},{9,1},{2,10},{10,2},{3,11},{11,3},{4,12},{12,4},... | collective-permute-start | bytes 1081352 | tf_op jit(solution)/shard_map/ppermute | solution.py:292
  34.1 3.8 %collective-permute-start.1 = (bf16[176,1024]{1,0:T(8,128)(2,1)S(1)}, bf16[176,1024]{1,0:T(8,128)(2,1)S(1)}, u32[]{:S(2)}, u32[]{:S(2)}) collective-permute-start(bf16[176,1024]{1,0:T(8,128)(2,1)S(1)} %convert_element_type.3.w0_ref), channel_id=1, source_target_pairs={{0,64},{64,0},{1,65},{65,1},{2,66},{66,2},{3,67},{67,3},{4,68},{68... | collective-permute-start | bytes 1081352 | tf_op jit(solution)/shard_map/ppermute | solution.py:293
  37.9 3.4 %collective-permute-start.2 = (bf16[176,1024]{1,0:T(8,128)(2,1)S(1)}, bf16[176,1024]{1,0:T(8,128)(2,1)S(1)}, u32[]{:S(2)}, u32[]{:S(2)}) collective-permute-start(bf16[176,1024]{1,0:T(8,128)(2,1)S(1)} %convert_element_type.3.w0_ref), channel_id=1, source_target_pairs={{0,72},{8,64},{64,8},{72,0},{1,73},{9,65},{65,9},{73,1},{2,74},{10... | collective-permute-start | bytes 1081352 | tf_op jit(solution)/shard_map/ppermute | solution.py:294
  41.3 3.9 %collective-permute-done.w1_ref = bf16[176,1024]{1,0:T(8,128)(2,1)S(1)} collective-permute-done((bf16[176,1024]{1,0:T(8,128)(2,1)S(1)}, bf16[176,1024]{1,0:T(8,128)(2,1)S(1)}, u32[]{:S(2)}, u32[]{:S(2)}) %collective-permute-start) | collective-permute-done | bytes 360480 | tf_op jit(solution)/shard_map/ppermute | solution.py:292
  45.3 0.0 copy-start.4
  45.3 6.1 %collective-permute-done.1.w2_ref = bf16[176,1024]{1,0:T(8,128)(2,1)S(1)} collective-permute-done((bf16[176,1024]{1,0:T(8,128)(2,1)S(1)}, bf16[176,1024]{1,0:T(8,128)(2,1)S(1)}, u32[]{:S(2)}, u32[]{:S(2)}) %collective-permute-start.1) | collective-permute-done | bytes 360480 | tf_op jit(solution)/shard_map/ppermute | solution.py:293
  51.4 0.0 copy-start.5
  51.4 1.4 %collective-permute-done.2.w3_ref = bf16[176,1024]{1,0:T(8,128)(2,1)S(1)} collective-permute-done((bf16[176,1024]{1,0:T(8,128)(2,1)S(1)}, bf16[176,1024]{1,0:T(8,128)(2,1)S(1)}, u32[]{:S(2)}, u32[]{:S(2)}) %collective-permute-start.2) | collective-permute-done | bytes 360480 | tf_op jit(solution)/shard_map/ppermute | solution.py:294
  52.8 0.0 copy-start.6
  52.8 0.0 all-to-all-done.1
  52.8 0.0 copy-start.1
  52.8 0.0 copy-done.2
  52.8 0.0 copy-done.4
  52.8 0.0 copy-done.5
  52.8 0.7 copy-done.6
  53.5 0.1 copy-done.1
  53.7 3.4 %down.1 = bf16[256,1024]{1,0:T(8,128)(2,1)} custom-call(s32[4]{0:T(128)} %pad_add_fusion.idx_ref, bf16[4,192,256]{2,1,0:T(8,128)(2,1)} %bitcast.21, bf16[176,1024]{1,0:T(8,128)(2,1)} %copy-done.2, bf16[176,1024]{1,0:T(8,128)(2,1)} %copy-done.4, bf16[176,1024]{1,0:T(8,128)(2,1)} %copy-done.5, bf16[176,1024]{1,0:T(8,128)(2,1)} %copy-done.6), custom_call_target="tpu_custom_call" | custom-call | tf_op jit(solution)/shard_map/down/pallas_call | solution.py:194
  57.1 32.2 %all_to_all.20.r_ref = bf16[16,16,1024]{2,1,0:T(8,128)(2,1)} all-to-all(bf16[16,16,1024]{2,1,0:T(8,128)(2,1)} %bitcast.20), channel_id=1, replica_groups=mesh['Z'=4,'zl'=2,'Y'=4,'yl'=2,'cb'=4,'dp'=2] {'Z','Y'}, dimensions={0} | all-to-all | bytes 1048576 | tf_op jit(solution)/shard_map/all_to_all | solution.py:301
  89.3 2.6 %mix.1 = (f32[16,1024]{1,0:T(8,128)}, f32[4,16,128]{2,1,0:T(8,128)}) custom-call(s32[4]{0:T(128)} %pad_add_fusion.idx_ref, bf16[16,16,1024]{2,1,0:T(8,128)(2,1)} %all_to_all.20.r_ref, bf16[64,16,1024]{2,1,0:T(8,128)(2,1)} %bitcast.19, f32[8,1024]{1,0:T(8,128)} %get-tuple-element.10.stat_ref, f32[1,1024]{1,0:T(1,128)} %bitcast.26, f32[1,1024]{1,0:T(1,128)} %bitcast.28, ...), custom_call_target="tpu_custom_call" | custom-call | tf_op jit(solution)/shard_map/mix/pallas_call | solution.py:224
  91.9 9.9 %all_to_all.21.part_ref = f32[4,16,128]{2,1,0:T(8,128)} all-to-all(f32[4,16,128]{2,1,0:T(8,128)} %get-tuple-element.12), channel_id=1, replica_groups=mesh['Z'=4,'zl'=2,'Y'=4,'yl'=2,'cb'=4,'dp'=2] {'cb'}, dimensions={0} | all-to-all | bytes 65536 | tf_op jit(solution)/shard_map/all_to_all | solution.py:303
  101.8 1.6 %finish.1 = bf16[16,1024]{1,0:T(8,128)(2,1)} custom-call(f32[16,1024]{1,0:T(8,128)} %get-tuple-element.11.mixed_ref, f32[4,16,128]{2,1,0:T(8,128)} %all_to_all.21.part_ref, f32[1,1024]{1,0:T(1,128)} %bitcast.30, f32[1,1024]{1,0:T(1,128)} %bitcast.31), custom_call_target="tpu_custom_call" | custom-call | tf_op jit(solution)/shard_map/finish/pallas_call | solution.py:258
  (1 shorter events, 0.0 us)
Async XLA Ops:
  6.1 26.0 %copy-start.3 = (f32[176,1024]{1,0:T(8,128)S(1)}, f32[176,1024]{1,0:T(8,128)}, u32[]{:S(2)}) copy-start(f32[176,1024]{1,0:T(8,128)} %param.18) | copy-start | bytes 2162692
  6.1 16.7 %all-to-all-start = ((bf16[4,96,1024]{2,1,0:T(8,128)(2,1)}), bf16[4,96,1024]{2,1,0:T(8,128)(2,1)S(1)}, u32[]{:S(2)}, u32[]{:S(2)}) async-start(bf16[4,96,1024]{2,1,0:T(8,128)(2,1)} %project.1), calls=%async_computation | async-start | bytes 1572864 | tf_op jit(solution)/shard_map/all_to_all | solution.py:297
  22.8 0.9 copy-start
  26.3 26.5 %all-to-all-start.1 = ((bf16[16,48,256]{2,1,0:T(8,128)(2,1)}), bf16[16,48,256]{2,1,0:T(8,128)(2,1)S(1)}, u32[]{:S(2)}, u32[]{:S(2)}) async-start(bf16[16,48,256]{2,1,0:T(8,128)(2,1)} %bitcast.24), calls=%async_computation.1 | async-start | bytes 786432 | tf_op jit(solution)/shard_map/all_to_all | solution.py:299
  32.1 20.7 %copy-start.2 = (bf16[176,1024]{1,0:T(8,128)(2,1)}, bf16[176,1024]{1,0:T(8,128)(2,1)S(1)}, u32[]{:S(2)}) copy-start(bf16[176,1024]{1,0:T(8,128)(2,1)S(1)} %convert_element_type.3.w0_ref) | copy-start | bytes 1081348
  32.1 13.2 %collective-permute-start = (bf16[176,1024]{1,0:T(8,128)(2,1)S(1)}, bf16[176,1024]{1,0:T(8,128)(2,1)S(1)}, u32[]{:S(2)}, u32[]{:S(2)}) collective-permute-start(bf16[176,1024]{1,0:T(8,128)(2,1)S(1)} %convert_element_type.3.w0_ref), channel_id=1, source_target_pairs={{0,8},{8,0},{1,9},{9,1},{2,10},{10,2},{3,11},{11,3},{4,12},{12,4},... | collective-permute-start | bytes 1081352 | tf_op jit(solution)/shard_map/ppermute | solution.py:292
  34.1 17.3 %collective-permute-start.1 = (bf16[176,1024]{1,0:T(8,128)(2,1)S(1)}, bf16[176,1024]{1,0:T(8,128)(2,1)S(1)}, u32[]{:S(2)}, u32[]{:S(2)}) collective-permute-start(bf16[176,1024]{1,0:T(8,128)(2,1)S(1)} %convert_element_type.3.w0_ref), channel_id=1, source_target_pairs={{0,64},{64,0},{1,65},{65,1},{2,66},{66,2},{3,67},{67,3},{4,68},{68... | collective-permute-start | bytes 1081352 | tf_op jit(solution)/shard_map/ppermute | solution.py:293
  37.9 14.9 %collective-permute-start.2 = (bf16[176,1024]{1,0:T(8,128)(2,1)S(1)}, bf16[176,1024]{1,0:T(8,128)(2,1)S(1)}, u32[]{:S(2)}, u32[]{:S(2)}) collective-permute-start(bf16[176,1024]{1,0:T(8,128)(2,1)S(1)} %convert_element_type.3.w0_ref), channel_id=1, source_target_pairs={{0,72},{8,64},{64,8},{72,0},{1,73},{9,65},{65,9},{73,1},{2,74},{10... | collective-permute-start | bytes 1081352 | tf_op jit(solution)/shard_map/ppermute | solution.py:294
  45.3 7.6 %copy-start.4 = (bf16[176,1024]{1,0:T(8,128)(2,1)}, bf16[176,1024]{1,0:T(8,128)(2,1)S(1)}, u32[]{:S(2)}) copy-start(bf16[176,1024]{1,0:T(8,128)(2,1)S(1)} %collective-permute-done.w1_ref) | copy-start | bytes 1081348
  51.4 1.4 %copy-start.5 = (bf16[176,1024]{1,0:T(8,128)(2,1)}, bf16[176,1024]{1,0:T(8,128)(2,1)S(1)}, u32[]{:S(2)}) copy-start(bf16[176,1024]{1,0:T(8,128)(2,1)S(1)} %collective-permute-done.1.w2_ref) | copy-start | bytes 1081348
  52.8 0.7 copy-start.6
  52.8 0.9 copy-start.1

commit v2 on v1

--- a/solution.py
+++ b/solution.py
@@ -4,6 +4,7 @@
 from jax.experimental import pallas as pl
 from jax.experimental.pallas import tpu as pltpu
 from jax.sharding import Mesh, PartitionSpec as P
+
 
 D = 4096
 F32 = jnp.float32
@@ -20,6 +21,10 @@
 
 def iota(shape, dim):
     return lax.broadcasted_iota(jnp.int32, shape, dim)
+
+
+def near(a):
+    return pltpu.with_memory_space_constraint(a, pltpu.VMEM)
 
 
 def dot(a, b, ca, cb):
@@ -169,9 +174,9 @@
         hidden_kernel,
         in_specs=[pl.BlockSpec(memory_space=pltpu.SMEM), vm, vm, vm],
         out_specs=[vm, vm],
-        out_shape=[jax.ShapeDtypeStruct((4, 4, SLOT, CHUNK), BF16), jax.ShapeDtypeStruct((8, ROWS), F32)],
+        out_shape=[pltpu.VMEM((4, 4, SLOT, CHUNK), BF16), pltpu.VMEM((8, ROWS), F32)],
         name="hidden",
-    )(idx, received, gate_scale, up_scale)
+    )(idx, *[near(a) for a in (received, gate_scale, up_scale)])
 
 
 def down_kernel(idx_ref, h_ref, w0_ref, w1_ref, w2_ref, w3_ref, out_ref):
@@ -195,9 +200,9 @@
         down_kernel,
         in_specs=[pl.BlockSpec(memory_space=pltpu.SMEM)] + [vm] * 5,
         out_specs=vm,
-        out_shape=jax.ShapeDtypeStruct((CHUNK, COLS), BF16),
+        out_shape=pltpu.VMEM((CHUNK, COLS), BF16),
         name="down",
-    )(idx, hidden, *weights)
+    )(idx, near(hidden), *[near(w) for w in weights])
 
 
 def mix_kernel(idx_ref, r_ref, x_ref, stat_ref, gain_ref, bias_ref, scale_ref, mixed_ref, part_ref):
@@ -207,7 +212,7 @@
     mine = iota((16, ROWS), 1) == iota((16, ROWS), 0) + idx_ref[2]
     mean = jnp.sum(jnp.where(mine, stat_ref[0:1], 0.0), axis=1, keepdims=True)
     rstd = jnp.sum(jnp.where(mine, stat_ref[1:2], 0.0), axis=1, keepdims=True)
-    normed = rounded((x_ref[0].astype(F32) - mean) * rstd * gain_ref[...] + bias_ref[...])
+    normed = rounded((x_ref[...].astype(F32) - mean) * rstd * gain_ref[...] + bias_ref[...])
     mixed = 0.5 * normed + branch * scale_ref[...]
     mixed_ref[...] = mixed
     m = jnp.sum(mixed, axis=1, keepdims=True) * (1.0 / COLS)
@@ -219,29 +224,15 @@
         part_ref[k] = part
 
 
-def mix(idx, received, tokens, stats, gain, bias, scale):
-    row = pl.BlockSpec((1, COLS), lambda i, s: (0, 0))
+def mix(idx, received, own, stats, gain, bias, scale):
+    vm = pl.BlockSpec(memory_space=pltpu.VMEM)
     return pl.pallas_call(
         mix_kernel,
-        grid_spec=pltpu.PrefetchScalarGridSpec(
-            num_scalar_prefetch=1,
-            grid=(1,),
-            in_specs=[
-                pl.BlockSpec((16, 16, COLS), lambda i, s: (0, 0, 0)),
-                pl.BlockSpec((1, 16, COLS), lambda i, s: (s[3], 0, 0)),
-                pl.BlockSpec((8, ROWS), lambda i, s: (0, 0)),
-                row,
-                row,
-                row,
-            ],
-            out_specs=[
-                pl.BlockSpec((16, COLS), lambda i, s: (0, 0)),
-                pl.BlockSpec((4, 16, 128), lambda i, s: (0, 0, 0)),
-            ],
-        ),
-        out_shape=[jax.ShapeDtypeStruct((16, COLS), F32), jax.ShapeDtypeStruct((4, 16, 128), F32)],
+        in_specs=[pl.BlockSpec(memory_space=pltpu.SMEM)] + [vm] * 6,
+        out_specs=[vm, vm],
+        out_shape=[pltpu.VMEM((16, COLS), F32), pltpu.VMEM((4, 16, 128), F32)],
         name="mix",
-    )(idx, received, tokens.reshape(64, 16, COLS), stats, gain, bias, scale)
+    )(idx, *[near(a) for a in (received, own, stats, gain, bias, scale)])
 
 
 def finish_kernel(mixed_ref, part_ref, gain_ref, bias_ref, out_ref):
@@ -261,7 +252,7 @@
         out_specs=vm,
         out_shape=jax.ShapeDtypeStruct((16, COLS), BF16),
         name="finish",
-    )(mixed, parts, gain, bias)
+    )(*[near(a) for a in (mixed, parts, gain, bias)])
 
 
 def swapped(n, k):
@@ -284,7 +275,7 @@
     x_at = lax.axis_index("cb")
     member = lax.axis_index(("zl", "yl"))
     block = lax.axis_index(("Z", "Y"))
-    idx = jnp.stack([x_at, member, member * CHUNK + block * 16, lax.axis_index(RA)]).astype(jnp.int32)
+    idx = jnp.stack([x_at, member, member * CHUNK + block * 16]).astype(jnp.int32)
     gain = norm_gain.reshape(1, COLS)
     bias = norm_bias.reshape(1, COLS)
 
@@ -296,10 +287,12 @@
     shares = project(tokens, gate_weight.T, up_weight.T, gain, bias)
     received = lax.all_to_all(shares, "cb", 0, 0, tiled=True)
     sent, stats = hidden_of(idx, received, gate_scale.reshape(1, FFL), up_scale.reshape(1, FFL))
+    own = lax.dynamic_slice_in_dim(tokens, lax.axis_index(RA) * 16, 16, 0)
+    sent, own = lax.optimization_barrier((sent, own))
     hidden = lax.all_to_all(sent.reshape(16, SLOT, CHUNK), ("zl", "yl", "cb"), 0, 0, tiled=True)
     partial = down(idx, hidden.reshape(4, 4 * SLOT, CHUNK), (w0, w1, w2, w3))
     pieces = lax.all_to_all(partial.reshape(16, 16, COLS), ("Z", "Y"), 0, 0, tiled=True)
-    mixed, part = mix(idx, pieces, tokens, stats, gain, bias, down_scale.reshape(1, COLS))
+    mixed, part = mix(idx, pieces, own, stats, gain, bias, down_scale.reshape(1, COLS))
     parts = lax.all_to_all(part, "cb", 0, 0, tiled=True)
     return finish(mixed, parts, out_gain.reshape(1, COLS), out_bias.reshape(1, COLS))
 

time: 104 us -> 97.1 us (0.934)
  Pallas kernels: 16.3 us -> 11.7 us
    unnamed x14 -> x16, local copies, waits for them, and re-layouts: 1.76 us -> 0.04 us
    pallas_call x1, Pallas kernels: 2.63 us -> 0.94 us  [mix(): pl.pallas_call(mix_kernel, in_specs=[pl.BlockSpec(memory_space=pltpu.SMEM...]
    pallas_call x1, Pallas kernels: 3.37 us -> 1.8 us  [down(): pl.pallas_call(down_kernel, in_specs=[pl.BlockSpec(memory_space=pltpu.SME...]
where the time goes in v2:
time: 97.1 us; the launch traced here: 96.5 us
  blocking collectives  41.5 us (43%)
  waiting for transfers between devices  22.4 us (23%)
  starting transfers between devices  19.4 us (20%)
  Pallas kernels  11.7 us (12%)
    all_to_all x1, blocking collectives, local(): lax.all_to_all(partial.reshape(16, 16, COLS), ('Z', 'Y'), 0, 0, tiled=True)  31.9 us
    all_to_all x1, waiting for transfers between devices, local(): received = lax.all_to_all(shares, 'cb', 0, 0, tiled=True)  10.9 us
    all_to_all x1, blocking collectives, local(): parts = lax.all_to_all(part, 'cb', 0, 0, tiled=True)  9.58 us
    pallas_call x1, Pallas kernels, project(): pl.pallas_call(project_kernel, grid=(4,), in_specs=[pl.BlockSpec((4, 1, 4...  6.09 us
    ppermute x1, waiting for transfers between devices, local(): w2 = lax.ppermute(w0, 'zl', swapped(2, 1))  6.09 us
    all_to_all x1, starting transfers between devices, local(): lax.all_to_all(sent.reshape(16, SLOT, CHUNK), ('zl', 'yl', 'cb'), 0, 0, t...  5.73 us
    all_to_all x1, starting transfers between devices, local(): received = lax.all_to_all(shares, 'cb', 0, 0, tiled=True)  4.43 us
    ppermute x1, waiting for transfers between devices, local(): w1 = lax.ppermute(w0, 'yl', swapped(2, 1))  3.94 us
  transfers between devices with their start and end apart: 5, of which 4 were waited for; matrix products, arithmetic and copies ran while one was open for 1% of the time, Pallas kernels for 0%

profile of v2, /device:TPU:8, one launch (start us, length us, event | category | flops | bytes accessed | tf_op | source)
XLA Modules:
  0.0 96.5 jit_solution(15094393938951272525)
XLA Ops:
  0.0 0.0 copy-start.5
  0.0 0.0 copy-start.6
  0.0 6.1 %project.1 = bf16[4,96,1024]{2,1,0:T(8,128)(2,1)} custom-call(bf16[4,2,4,2,16,1024]{5,4,3,2,1,0:T(8,128)(2,1)} %bitcast.27, f32[176,1024]{1,0:T(8,128)} %bitcast.28, f32[176,1024]{1,0:T(8,128)} %bitcast.29, f32[1,1024]{1,0:T(1,128)} %bitcast.18, f32[1,1024]{1,0:T(1,128)} %bitcast.20), custom_call_target="tpu_custom_call" | custom-call | tf_op jit(solution)/shard_map/project/pallas_call | solution.py:98
  6.1 0.0 copy-start.7
  6.1 4.4 %all-to-all-start = ((bf16[4,96,1024]{2,1,0:T(8,128)(2,1)}), bf16[4,96,1024]{2,1,0:T(8,128)(2,1)S(1)}, u32[]{:S(2)}, u32[]{:S(2)}) async-start(bf16[4,96,1024]{2,1,0:T(8,128)(2,1)} %project.1), calls=%async_computation | async-start | bytes 1572864 | tf_op jit(solution)/shard_map/all_to_all | solution.py:288
  10.5 0.6 pad_add_fusion.idx_ref
  11.1 0.8 constant_dynamic-slice_fusion.x_ref
  11.9 10.9 %all-to-all-done.r_ref = bf16[4,96,1024]{2,1,0:T(8,128)(2,1)S(1)} async-done(((bf16[4,96,1024]{2,1,0:T(8,128)(2,1)}), bf16[4,96,1024]{2,1,0:T(8,128)(2,1)S(1)}, u32[]{:S(2)}, u32[]{:S(2)}) %all-to-all-start) | async-done | bytes 786464 | tf_op jit(solution)/shard_map/all_to_all | solution.py:288
  22.8 0.0 copy-done.5
  22.8 0.0 copy-done.6
  22.8 2.1 %hidden.1 = (bf16[4,4,48,256]{3,2,1,0:T(8,128)(2,1)}, f32[8,1024]{1,0:T(8,128)S(1)}) custom-call(s32[3]{0:T(128)} %pad_add_fusion.idx_ref, bf16[4,96,1024]{2,1,0:T(8,128)(2,1)S(1)} %all-to-all-done.r_ref, f32[1,176]{1,0:T(1,128)S(1)} %bitcast.25, f32[1,176]{1,0:T(1,128)S(1)} %bitcast.26), custom_call_target="tpu_custom_call" | custom-call | tf_op jit(solution)/shard_map/hidden/pallas_call | solution.py:173
  24.9 5.7 %all-to-all-start.1 = ((bf16[16,48,256]{2,1,0:T(8,128)(2,1)}), bf16[16,48,256]{2,1,0:T(8,128)(2,1)S(1)}, u32[]{:S(2)}, u32[]{:S(2)}) async-start(bf16[16,48,256]{2,1,0:T(8,128)(2,1)} %bitcast.10), calls=%async_computation.1 | async-start | bytes 786432 | tf_op jit(solution)/shard_map/all_to_all | solution.py:292
  30.7 0.0 copy-done.7
  30.7 0.0 copy-start
  30.7 0.0 copy-start.1
  30.7 0.0 copy-start.2
  30.8 0.0 copy-start.3
  30.8 0.0 copy-start.4
  30.8 2.0 %collective-permute-start = (bf16[176,1024]{1,0:T(8,128)(2,1)S(1)}, bf16[176,1024]{1,0:T(8,128)(2,1)S(1)}, u32[]{:S(2)}, u32[]{:S(2)}) collective-permute-start(bf16[176,1024]{1,0:T(8,128)(2,1)S(1)} %convert_element_type.3.w0_ref), channel_id=1, source_target_pairs={{0,8},{8,0},{1,9},{9,1},{2,10},{10,2},{3,11},{11,3},{4,12},{12,4},... | collective-permute-start | bytes 1081352 | tf_op jit(solution)/shard_map/ppermute | solution.py:283
  32.8 3.8 %collective-permute-start.1 = (bf16[176,1024]{1,0:T(8,128)(2,1)S(1)}, bf16[176,1024]{1,0:T(8,128)(2,1)S(1)}, u32[]{:S(2)}, u32[]{:S(2)}) collective-permute-start(bf16[176,1024]{1,0:T(8,128)(2,1)S(1)} %convert_element_type.3.w0_ref), channel_id=1, source_target_pairs={{0,64},{64,0},{1,65},{65,1},{2,66},{66,2},{3,67},{67,3},{4,68},{68... | collective-permute-start | bytes 1081352 | tf_op jit(solution)/shard_map/ppermute | solution.py:284
  36.7 3.4 %collective-permute-start.2 = (bf16[176,1024]{1,0:T(8,128)(2,1)S(1)}, bf16[176,1024]{1,0:T(8,128)(2,1)S(1)}, u32[]{:S(2)}, u32[]{:S(2)}) collective-permute-start(bf16[176,1024]{1,0:T(8,128)(2,1)S(1)} %convert_element_type.3.w0_ref), channel_id=1, source_target_pairs={{0,72},{8,64},{64,8},{72,0},{1,73},{9,65},{65,9},{73,1},{2,74},{10... | collective-permute-start | bytes 1081352 | tf_op jit(solution)/shard_map/ppermute | solution.py:285
  40.0 3.9 %collective-permute-done.w1_ref = bf16[176,1024]{1,0:T(8,128)(2,1)S(1)} collective-permute-done((bf16[176,1024]{1,0:T(8,128)(2,1)S(1)}, bf16[176,1024]{1,0:T(8,128)(2,1)S(1)}, u32[]{:S(2)}, u32[]{:S(2)}) %collective-permute-start) | collective-permute-done | bytes 360480 | tf_op jit(solution)/shard_map/ppermute | solution.py:283
  44.0 6.1 %collective-permute-done.1.w2_ref = bf16[176,1024]{1,0:T(8,128)(2,1)S(1)} collective-permute-done((bf16[176,1024]{1,0:T(8,128)(2,1)S(1)}, bf16[176,1024]{1,0:T(8,128)(2,1)S(1)}, u32[]{:S(2)}, u32[]{:S(2)}) %collective-permute-start.1) | collective-permute-done | bytes 360480 | tf_op jit(solution)/shard_map/ppermute | solution.py:284
  50.1 1.4 %collective-permute-done.2.w3_ref = bf16[176,1024]{1,0:T(8,128)(2,1)S(1)} collective-permute-done((bf16[176,1024]{1,0:T(8,128)(2,1)S(1)}, bf16[176,1024]{1,0:T(8,128)(2,1)S(1)}, u32[]{:S(2)}, u32[]{:S(2)}) %collective-permute-start.2) | collective-permute-done | bytes 360480 | tf_op jit(solution)/shard_map/ppermute | solution.py:285
  51.5 0.0 all-to-all-done.1
  51.5 1.8 %down.1 = bf16[256,1024]{1,0:T(8,128)(2,1)S(1)} custom-call(s32[3]{0:T(128)} %pad_add_fusion.idx_ref, bf16[4,192,256]{2,1,0:T(8,128)(2,1)S(1)} %bitcast.17, bf16[176,1024]{1,0:T(8,128)(2,1)S(1)} %convert_element_type.3.w0_ref, bf16[176,1024]{1,0:T(8,128)(2,1)S(1)} %collective-permute-done.w1_ref, bf16[176,1024]{1,0:T(8,128)(2,1)S(1)} %collective-permute-done.1.w2_ref, ...), custom_call_target="tpu_custom_call" | custom-call | tf_op jit(solution)/shard_map/down/pallas_call | solution.py:199
  53.3 31.9 %all_to_all.20.r_ref = bf16[16,16,1024]{2,1,0:T(8,128)(2,1)S(1)} all-to-all(bf16[16,16,1024]{2,1,0:T(8,128)(2,1)S(1)} %bitcast.16), channel_id=1, replica_groups=mesh['Z'=4,'zl'=2,'Y'=4,'yl'=2,'cb'=4,'dp'=2] {'Z','Y'}, dimensions={0} | all-to-all | bytes 1048576 | tf_op jit(solution)/shard_map/all_to_all | solution.py:294
  85.2 0.0 copy-done
  85.2 0.0 copy-done.1
  85.2 0.0 copy-done.2
  85.2 0.9 mix.1
  86.2 9.6 %all_to_all.21.part_ref = f32[4,16,128]{2,1,0:T(8,128)S(1)} all-to-all(f32[4,16,128]{2,1,0:T(8,128)S(1)} %get-tuple-element.16), channel_id=1, replica_groups=mesh['Z'=4,'zl'=2,'Y'=4,'yl'=2,'cb'=4,'dp'=2] {'cb'}, dimensions={0} | all-to-all | bytes 65536 | tf_op jit(solution)/shard_map/all_to_all | solution.py:296
  95.7 0.0 copy-done.3
  95.7 0.0 copy-done.4
  95.7 0.8 finish.1
  (1 shorter events, 0.0 us)
Async XLA Ops:
  0.0 22.8 %copy-start.5 = (f32[176]{0:T(256)S(1)}, f32[176]{0:T(256)}, u32[]{:S(2)}) copy-start(f32[176]{0:T(256)} %param.16) | copy-start | bytes 2116
  0.0 22.8 %copy-start.6 = (f32[176]{0:T(256)S(1)}, f32[176]{0:T(256)}, u32[]{:S(2)}) copy-start(f32[176]{0:T(256)} %param.17) | copy-start | bytes 2116
  6.1 24.6 %copy-start.7 = (f32[176,1024]{1,0:T(8,128)S(1)}, f32[176,1024]{1,0:T(8,128)}, u32[]{:S(2)}) copy-start(f32[176,1024]{1,0:T(8,128)} %param.18) | copy-start | bytes 2162692
  6.1 16.7 %all-to-all-start = ((bf16[4,96,1024]{2,1,0:T(8,128)(2,1)}), bf16[4,96,1024]{2,1,0:T(8,128)(2,1)S(1)}, u32[]{:S(2)}, u32[]{:S(2)}) async-start(bf16[4,96,1024]{2,1,0:T(8,128)(2,1)} %project.1), calls=%async_computation | async-start | bytes 1572864 | tf_op jit(solution)/shard_map/all_to_all | solution.py:288
  24.9 26.5 %all-to-all-start.1 = ((bf16[16,48,256]{2,1,0:T(8,128)(2,1)}), bf16[16,48,256]{2,1,0:T(8,128)(2,1)S(1)}, u32[]{:S(2)}, u32[]{:S(2)}) async-start(bf16[16,48,256]{2,1,0:T(8,128)(2,1)} %bitcast.10), calls=%async_computation.1 | async-start | bytes 786432 | tf_op jit(solution)/shard_map/all_to_all | solution.py:292
  30.7 54.5 %copy-start = (f32[1024]{0:T(1024)S(1)}, f32[1024]{0:T(1024)}, u32[]{:S(2)}) copy-start(f32[1024]{0:T(1024)} %param.12) | copy-start | bytes 12292
  30.7 54.5 %copy-start.1 = (f32[1024]{0:T(1024)S(1)}, f32[1024]{0:T(1024)}, u32[]{:S(2)}) copy-start(f32[1024]{0:T(1024)} %param.13) | copy-start | bytes 12292
  30.7 54.5 %copy-start.2 = (f32[1024]{0:T(1024)S(1)}, f32[1024]{0:T(1024)}, u32[]{:S(2)}) copy-start(f32[1024]{0:T(1024)} %param.19) | copy-start | bytes 12292
  30.8 65.0 %copy-start.3 = (f32[1024]{0:T(1024)S(1)}, f32[1024]{0:T(1024)}, u32[]{:S(2)}) copy-start(f32[1024]{0:T(1024)} %param.20) | copy-start | bytes 12292
  30.8 65.0 %copy-start.4 = (f32[1024]{0:T(1024)S(1)}, f32[1024]{0:T(1024)}, u32[]{:S(2)}) copy-start(f32[1024]{0:T(1024)} %param.21) | copy-start | bytes 12292
  30.8 13.2 %collective-permute-start = (bf16[176,1024]{1,0:T(8,128)(2,1)S(1)}, bf16[176,1024]{1,0:T(8,128)(2,1)S(1)}, u32[]{:S(2)}, u32[]{:S(2)}) collective-permute-start(bf16[176,1024]{1,0:T(8,128)(2,1)S(1)} %convert_element_type.3.w0_ref), channel_id=1, source_target_pairs={{0,8},{8,0},{1,9},{9,1},{2,10},{10,2},{3,11},{11,3},{4,12},{12,4},... | collective-permute-start | bytes 1081352 | tf_op jit(solution)/shard_map/ppermute | solution.py:283
  32.8 17.2 %collective-permute-start.1 = (bf16[176,1024]{1,0:T(8,128)(2,1)S(1)}, bf16[176,1024]{1,0:T(8,128)(2,1)S(1)}, u32[]{:S(2)}, u32[]{:S(2)}) collective-permute-start(bf16[176,1024]{1,0:T(8,128)(2,1)S(1)} %convert_element_type.3.w0_ref), channel_id=1, source_target_pairs={{0,64},{64,0},{1,65},{65,1},{2,66},{66,2},{3,67},{67,3},{4,68},{68... | collective-permute-start | bytes 1081352 | tf_op jit(solution)/shard_map/ppermute | solution.py:284
  36.7 14.8 %collective-permute-start.2 = (bf16[176,1024]{1,0:T(8,128)(2,1)S(1)}, bf16[176,1024]{1,0:T(8,128)(2,1)S(1)}, u32[]{:S(2)}, u32[]{:S(2)}) collective-permute-start(bf16[176,1024]{1,0:T(8,128)(2,1)S(1)} %convert_element_type.3.w0_ref), channel_id=1, source_target_pairs={{0,72},{8,64},{64,8},{72,0},{1,73},{9,65},{65,9},{73,1},{2,74},{10... | collective-permute-start | bytes 1081352 | tf_op jit(solution)/shard_map/ppermute | solution.py:285

commit v3 on v2

--- a/solution.py
+++ b/solution.py
@@ -113,8 +113,8 @@
     )(x, gate_t, up_t, gain, bias)
 
 
-def hidden_kernel(idx_ref, r_ref, gs_ref, us_ref, out_ref, stat_ref):
-    me = idx_ref[0]
+def hidden_kernel(r_ref, gs_ref, us_ref, out_ref, stat_ref):
+    me = lax.axis_index("cb")
     means = []
     m2s = []
     for c in range(4):
@@ -168,19 +168,19 @@
             out_ref[j, k] = h
 
 
-def hidden_of(idx, received, gate_scale, up_scale):
+def hidden_of(received, gate_scale, up_scale):
     vm = pl.BlockSpec(memory_space=pltpu.VMEM)
     return pl.pallas_call(
         hidden_kernel,
-        in_specs=[pl.BlockSpec(memory_space=pltpu.SMEM), vm, vm, vm],
+        in_specs=[vm, vm, vm],
         out_specs=[vm, vm],
         out_shape=[pltpu.VMEM((4, 4, SLOT, CHUNK), BF16), pltpu.VMEM((8, ROWS), F32)],
         name="hidden",
-    )(idx, *[near(a) for a in (received, gate_scale, up_scale)])
-
-
-def down_kernel(idx_ref, h_ref, w0_ref, w1_ref, w2_ref, w3_ref, out_ref):
-    me = idx_ref[1]
+    )(*[near(a) for a in (received, gate_scale, up_scale)])
+
+
+def down_kernel(h_ref, w0_ref, w1_ref, w2_ref, w3_ref, out_ref):
+    me = lax.axis_index("zl") * 2 + lax.axis_index("yl")
     row = iota((FFL, 4 * SLOT), 0)
     lane = iota((FFL, 4 * SLOT), 1)
     hit = lane < 0
@@ -194,22 +194,24 @@
     out_ref[...] = acc.astype(BF16)
 
 
-def down(idx, hidden, weights):
+def down(hidden, weights):
     vm = pl.BlockSpec(memory_space=pltpu.VMEM)
     return pl.pallas_call(
         down_kernel,
-        in_specs=[pl.BlockSpec(memory_space=pltpu.SMEM)] + [vm] * 5,
+        in_specs=[vm] * 5,
         out_specs=vm,
         out_shape=pltpu.VMEM((CHUNK, COLS), BF16),
         name="down",
-    )(idx, near(hidden), *[near(w) for w in weights])
-
-
-def mix_kernel(idx_ref, r_ref, x_ref, stat_ref, gain_ref, bias_ref, scale_ref, mixed_ref, part_ref):
+    )(near(hidden), *[near(w) for w in weights])
+
+
+def mix_kernel(r_ref, x_ref, stat_ref, gain_ref, bias_ref, scale_ref, mixed_ref, part_ref):
+    member = lax.axis_index("zl") * 2 + lax.axis_index("yl")
+    at = member * CHUNK + (lax.axis_index("Z") * 4 + lax.axis_index("Y")) * 16
     branch = jnp.zeros((16, COLS), F32)
     for k in range(16):
         branch = branch + r_ref[k].astype(F32)
-    mine = iota((16, ROWS), 1) == iota((16, ROWS), 0) + idx_ref[2]
+    mine = iota((16, ROWS), 1) == iota((16, ROWS), 0) + at
     mean = jnp.sum(jnp.where(mine, stat_ref[0:1], 0.0), axis=1, keepdims=True)
     rstd = jnp.sum(jnp.where(mine, stat_ref[1:2], 0.0), axis=1, keepdims=True)
     normed = rounded((x_ref[...].astype(F32) - mean) * rstd * gain_ref[...] + bias_ref[...])
@@ -224,15 +226,15 @@
         part_ref[k] = part
 
 
-def mix(idx, received, own, stats, gain, bias, scale):
+def mix(received, own, stats, gain, bias, scale):
     vm = pl.BlockSpec(memory_space=pltpu.VMEM)
     return pl.pallas_call(
         mix_kernel,
-        in_specs=[pl.BlockSpec(memory_space=pltpu.SMEM)] + [vm] * 6,
+        in_specs=[vm] * 6,
         out_specs=[vm, vm],
         out_shape=[pltpu.VMEM((16, COLS), F32), pltpu.VMEM((4, 16, 128), F32)],
         name="mix",
-    )(idx, *[near(a) for a in (received, own, stats, gain, bias, scale)])
+    )(*[near(a) for a in (received, own, stats, gain, bias, scale)])
 
 
 def finish_kernel(mixed_ref, part_ref, gain_ref, bias_ref, out_ref):
@@ -272,10 +274,6 @@
     out_gain,
     out_bias,
 ):
-    x_at = lax.axis_index("cb")
-    member = lax.axis_index(("zl", "yl"))
-    block = lax.axis_index(("Z", "Y"))
-    idx = jnp.stack([x_at, member, member * CHUNK + block * 16]).astype(jnp.int32)
     gain = norm_gain.reshape(1, COLS)
     bias = norm_bias.reshape(1, COLS)
 
@@ -286,13 +284,13 @@
 
     shares = project(tokens, gate_weight.T, up_weight.T, gain, bias)
     received = lax.all_to_all(shares, "cb", 0, 0, tiled=True)
-    sent, stats = hidden_of(idx, received, gate_scale.reshape(1, FFL), up_scale.reshape(1, FFL))
+    sent, stats = hidden_of(received, gate_scale.reshape(1, FFL), up_scale.reshape(1, FFL))
+    hidden = lax.all_to_all(sent.reshape(16, SLOT, CHUNK), ("zl", "yl", "cb"), 0, 0, tiled=True)
     own = lax.dynamic_slice_in_dim(tokens, lax.axis_index(RA) * 16, 16, 0)
-    sent, own = lax.optimization_barrier((sent, own))
-    hidden = lax.all_to_all(sent.reshape(16, SLOT, CHUNK), ("zl", "yl", "cb"), 0, 0, tiled=True)
-    partial = down(idx, hidden.reshape(4, 4 * SLOT, CHUNK), (w0, w1, w2, w3))
+    hidden, own = lax.optimization_barrier((hidden, own))
+    partial = down(hidden.reshape(4, 4 * SLOT, CHUNK), (w0, w1, w2, w3))
     pieces = lax.all_to_all(partial.reshape(16, 16, COLS), ("Z", "Y"), 0, 0, tiled=True)
-    mixed, part = mix(idx, pieces, own, stats, gain, bias, down_scale.reshape(1, COLS))
+    mixed, part = mix(pieces, own, stats, gain, bias, down_scale.reshape(1, COLS))
     parts = lax.all_to_all(part, "cb", 0, 0, tiled=True)
     return finish(mixed, parts, out_gain.reshape(1, COLS), out_bias.reshape(1, COLS))
 

time: 97.1 us -> 95.1 us (0.979)
  blocking collectives: 41.5 us -> 58.2 us
  waiting for transfers between devices: 22.4 us -> 10.7 us
  starting transfers between devices: 19.4 us -> 14.9 us
  Pallas kernels: 11.7 us -> 9.77 us
    all_to_all x0 -> x1, blocking collectives: none -> 16.7 us  [local(): received = lax.all_to_all(shares, 'cb', 0, 0, tiled=True)]
    all_to_all x1 -> x0, waiting for transfers between devices: 10.9 us -> none  [local(): received = lax.all_to_all(shares, 'cb', 0, 0, tiled=True)]
    all_to_all x1 -> x0, starting transfers between devices: 4.43 us -> none  [local(): received = lax.all_to_all(shares, 'cb', 0, 0, tiled=True)]
    pallas_call x3, Pallas kernels: 4.88 us -> 2.9 us  [the longest x1 1.46 us: hidden_of(): pl.pallas_call(hidden_kernel, in_specs=[vm, vm, vm], out_specs=[vm, vm],...]
  transfers between devices with their start and end apart: 5 -> 4, of which waited for: 4 -> 3; matrix products, arithmetic and copies ran while one was open for 1% -> 1% of each run, Pallas kernels for 0% -> 0%
where the time goes in v3:
time: 95.1 us; the launch traced here: 94.5 us
  blocking collectives  58.2 us (61%)
  starting transfers between devices  14.9 us (16%)
  waiting for transfers between devices  10.7 us (11%)
  Pallas kernels  9.77 us (10%)
    all_to_all x1, blocking collectives, local(): lax.all_to_all(partial.reshape(16, 16, COLS), ('Z', 'Y'), 0, 0, tiled=True)  31.9 us
    all_to_all x1, blocking collectives, local(): received = lax.all_to_all(shares, 'cb', 0, 0, tiled=True)  16.7 us
    all_to_all x1, blocking collectives, local(): parts = lax.all_to_all(part, 'cb', 0, 0, tiled=True)  9.57 us
    ppermute x1, waiting for transfers between devices, local(): w2 = lax.ppermute(w0, 'zl', swapped(2, 1))  6.11 us
    pallas_call x1, Pallas kernels, project(): pl.pallas_call(project_kernel, grid=(4,), in_specs=[pl.BlockSpec((4, 1, 4...  6.09 us
    all_to_all x1, starting transfers between devices, local(): lax.all_to_all(sent.reshape(16, SLOT, CHUNK), ('zl', 'yl', 'cb'), 0, 0, t...  5.73 us
    ppermute x1, starting transfers between devices, local(): w2 = lax.ppermute(w0, 'zl', swapped(2, 1))  3.83 us
    ppermute x1, starting transfers between devices, local(): w3 = lax.ppermute(w0, ('zl', 'yl'), swapped(4, 3))  3.37 us
  transfers between devices with their start and end apart: 4, of which 3 were waited for; matrix products, arithmetic and copies ran while one was open for 1% of the time, Pallas kernels for 0%

profile of v3, /device:TPU:8, one launch (start us, length us, event | category | flops | bytes accessed | tf_op | source)
XLA Modules:
  0.0 94.5 jit_solution(9709732571045191315)
XLA Ops:
  0.0 0.0 copy-start.5
  0.0 0.0 copy-start.6
  0.0 6.1 %project.1 = bf16[4,96,1024]{2,1,0:T(8,128)(2,1)} custom-call(bf16[4,2,4,2,16,1024]{5,4,3,2,1,0:T(8,128)(2,1)} %bitcast.24, f32[176,1024]{1,0:T(8,128)} %bitcast.25, f32[176,1024]{1,0:T(8,128)} %bitcast.26, f32[1,1024]{1,0:T(1,128)} %bitcast.15, f32[1,1024]{1,0:T(1,128)} %bitcast.17), custom_call_target="tpu_custom_call" | custom-call | tf_op jit(solution)/shard_map/project/pallas_call | solution.py:98
  6.1 0.0 copy-start.7
  6.1 16.7 %all_to_all.20.r_ref = bf16[4,96,1024]{2,1,0:T(8,128)(2,1)S(1)} all-to-all(bf16[4,96,1024]{2,1,0:T(8,128)(2,1)} %project.1), channel_id=1, replica_groups=mesh['Z'=4,'zl'=2,'Y'=4,'yl'=2,'cb'=4,'dp'=2] {'cb'}, dimensions={0} | all-to-all | bytes 1572864 | tf_op jit(solution)/shard_map/all_to_all | solution.py:286
  22.8 0.0 copy-done.5
  22.8 0.0 copy-done.6
  22.8 1.5 %hidden.1 = (bf16[4,4,48,256]{3,2,1,0:T(8,128)(2,1)}, f32[8,1024]{1,0:T(8,128)S(1)}) custom-call(bf16[4,96,1024]{2,1,0:T(8,128)(2,1)S(1)} %all_to_all.20.r_ref, f32[1,176]{1,0:T(1,128)S(1)} %bitcast.22, f32[1,176]{1,0:T(1,128)S(1)} %bitcast.23), custom_call_target="tpu_custom_call" | custom-call | tf_op jit(solution)/shard_map/hidden/pallas_call | solution.py:173
  24.3 5.7 %all-to-all-start.1 = ((bf16[16,48,256]{2,1,0:T(8,128)(2,1)}), bf16[16,48,256]{2,1,0:T(8,128)(2,1)S(1)}, u32[]{:S(2)}, u32[]{:S(2)}) async-start(bf16[16,48,256]{2,1,0:T(8,128)(2,1)} %bitcast.7), calls=%async_computation.1 | async-start | bytes 786432 | tf_op jit(solution)/shard_map/all_to_all | solution.py:288
  30.0 0.0 copy-done.7
  30.0 0.0 copy-start
  30.0 0.0 copy-start.1
  30.0 0.0 copy-start.2
  30.1 2.0 %collective-permute-start = (bf16[176,1024]{1,0:T(8,128)(2,1)S(1)}, bf16[176,1024]{1,0:T(8,128)(2,1)S(1)}, u32[]{:S(2)}, u32[]{:S(2)}) collective-permute-start(bf16[176,1024]{1,0:T(8,128)(2,1)S(1)} %convert_element_type.3.w0_ref), channel_id=1, source_target_pairs={{0,8},{8,0},{1,9},{9,1},{2,10},{10,2},{3,11},{11,3},{4,12},{12,4},... | collective-permute-start | bytes 1081352 | tf_op jit(solution)/shard_map/ppermute | solution.py:281
  32.1 3.8 %collective-permute-start.1 = (bf16[176,1024]{1,0:T(8,128)(2,1)S(1)}, bf16[176,1024]{1,0:T(8,128)(2,1)S(1)}, u32[]{:S(2)}, u32[]{:S(2)}) collective-permute-start(bf16[176,1024]{1,0:T(8,128)(2,1)S(1)} %convert_element_type.3.w0_ref), channel_id=1, source_target_pairs={{0,64},{64,0},{1,65},{65,1},{2,66},{66,2},{3,67},{67,3},{4,68},{68... | collective-permute-start | bytes 1081352 | tf_op jit(solution)/shard_map/ppermute | solution.py:282
  36.0 3.4 %collective-permute-start.2 = (bf16[176,1024]{1,0:T(8,128)(2,1)S(1)}, bf16[176,1024]{1,0:T(8,128)(2,1)S(1)}, u32[]{:S(2)}, u32[]{:S(2)}) collective-permute-start(bf16[176,1024]{1,0:T(8,128)(2,1)S(1)} %convert_element_type.3.w0_ref), channel_id=1, source_target_pairs={{0,72},{8,64},{64,8},{72,0},{1,73},{9,65},{65,9},{73,1},{2,74},{10... | collective-permute-start | bytes 1081352 | tf_op jit(solution)/shard_map/ppermute | solution.py:283
  39.3 0.0 copy-start.3
  39.4 0.0 copy-start.4
  39.4 0.8 constant_dynamic-slice_fusion.x_ref
  40.1 0.0 all-to-all-done.1
  40.1 3.1 %collective-permute-done.w1_ref = bf16[176,1024]{1,0:T(8,128)(2,1)S(1)} collective-permute-done((bf16[176,1024]{1,0:T(8,128)(2,1)S(1)}, bf16[176,1024]{1,0:T(8,128)(2,1)S(1)}, u32[]{:S(2)}, u32[]{:S(2)}) %collective-permute-start) | collective-permute-done | bytes 360480 | tf_op jit(solution)/shard_map/ppermute | solution.py:281
  43.3 6.1 %collective-permute-done.1.w2_ref = bf16[176,1024]{1,0:T(8,128)(2,1)S(1)} collective-permute-done((bf16[176,1024]{1,0:T(8,128)(2,1)S(1)}, bf16[176,1024]{1,0:T(8,128)(2,1)S(1)}, u32[]{:S(2)}, u32[]{:S(2)}) %collective-permute-start.1) | collective-permute-done | bytes 360480 | tf_op jit(solution)/shard_map/ppermute | solution.py:282
  49.4 1.4 %collective-permute-done.2.w3_ref = bf16[176,1024]{1,0:T(8,128)(2,1)S(1)} collective-permute-done((bf16[176,1024]{1,0:T(8,128)(2,1)S(1)}, bf16[176,1024]{1,0:T(8,128)(2,1)S(1)}, u32[]{:S(2)}, u32[]{:S(2)}) %collective-permute-start.2) | collective-permute-done | bytes 360480 | tf_op jit(solution)/shard_map/ppermute | solution.py:283
  50.8 1.2 %down.1 = bf16[256,1024]{1,0:T(8,128)(2,1)S(1)} custom-call(bf16[4,192,256]{2,1,0:T(8,128)(2,1)S(1)} %bitcast.14, bf16[176,1024]{1,0:T(8,128)(2,1)S(1)} %convert_element_type.3.w0_ref, bf16[176,1024]{1,0:T(8,128)(2,1)S(1)} %collective-permute-done.w1_ref, bf16[176,1024]{1,0:T(8,128)(2,1)S(1)} %collective-permute-done.1.w2_ref, ...), custom_call_target="tpu_custom_call" | custom-call | tf_op jit(solution)/shard_map/down/pallas_call | solution.py:199
  52.0 31.9 %all_to_all.21.r_ref = bf16[16,16,1024]{2,1,0:T(8,128)(2,1)S(1)} all-to-all(bf16[16,16,1024]{2,1,0:T(8,128)(2,1)S(1)} %bitcast.13), channel_id=1, replica_groups=mesh['Z'=4,'zl'=2,'Y'=4,'yl'=2,'cb'=4,'dp'=2] {'Z','Y'}, dimensions={0} | all-to-all | bytes 1048576 | tf_op jit(solution)/shard_map/all_to_all | solution.py:292
  83.9 0.0 copy-done
  83.9 0.0 copy-done.1
  83.9 0.0 copy-done.2
  83.9 0.3 mix.1
  84.2 9.6 %all_to_all.22.part_ref = f32[4,16,128]{2,1,0:T(8,128)S(1)} all-to-all(f32[4,16,128]{2,1,0:T(8,128)S(1)} %get-tuple-element.16), channel_id=1, replica_groups=mesh['Z'=4,'zl'=2,'Y'=4,'yl'=2,'cb'=4,'dp'=2] {'cb'}, dimensions={0} | all-to-all | bytes 65536 | tf_op jit(solution)/shard_map/all_to_all | solution.py:294
  93.7 0.0 copy-done.3
  93.7 0.0 copy-done.4
  93.7 0.8 finish.1
  (1 shorter events, 0.0 us)
Async XLA Ops:
  0.0 22.8 %copy-start.5 = (f32[176]{0:T(256)S(1)}, f32[176]{0:T(256)}, u32[]{:S(2)}) copy-start(f32[176]{0:T(256)} %param.16) | copy-start | bytes 2116
  0.0 22.8 %copy-start.6 = (f32[176]{0:T(256)S(1)}, f32[176]{0:T(256)}, u32[]{:S(2)}) copy-start(f32[176]{0:T(256)} %param.17) | copy-start | bytes 2116
  6.1 23.9 %copy-start.7 = (f32[176,1024]{1,0:T(8,128)S(1)}, f32[176,1024]{1,0:T(8,128)}, u32[]{:S(2)}) copy-start(f32[176,1024]{1,0:T(8,128)} %param.18) | copy-start | bytes 2162692
  24.3 15.9 %all-to-all-start.1 = ((bf16[16,48,256]{2,1,0:T(8,128)(2,1)}), bf16[16,48,256]{2,1,0:T(8,128)(2,1)S(1)}, u32[]{:S(2)}, u32[]{:S(2)}) async-start(bf16[16,48,256]{2,1,0:T(8,128)(2,1)} %bitcast.7), calls=%async_computation.1 | async-start | bytes 786432 | tf_op jit(solution)/shard_map/all_to_all | solution.py:288
  30.0 53.9 %copy-start = (f32[1024]{0:T(1024)S(1)}, f32[1024]{0:T(1024)}, u32[]{:S(2)}) copy-start(f32[1024]{0:T(1024)} %param.12) | copy-start | bytes 12292
  30.0 53.8 %copy-start.1 = (f32[1024]{0:T(1024)S(1)}, f32[1024]{0:T(1024)}, u32[]{:S(2)}) copy-start(f32[1024]{0:T(1024)} %param.13) | copy-start | bytes 12292
  30.0 53.8 %copy-start.2 = (f32[1024]{0:T(1024)S(1)}, f32[1024]{0:T(1024)}, u32[]{:S(2)}) copy-start(f32[1024]{0:T(1024)} %param.19) | copy-start | bytes 12292
  30.1 13.2 %collective-permute-start = (bf16[176,1024]{1,0:T(8,128)(2,1)S(1)}, bf16[176,1024]{1,0:T(8,128)(2,1)S(1)}, u32[]{:S(2)}, u32[]{:S(2)}) collective-permute-start(bf16[176,1024]{1,0:T(8,128)(2,1)S(1)} %convert_element_type.3.w0_ref), channel_id=1, source_target_pairs={{0,8},{8,0},{1,9},{9,1},{2,10},{10,2},{3,11},{11,3},{4,12},{12,4},... | collective-permute-start | bytes 1081352 | tf_op jit(solution)/shard_map/ppermute | solution.py:281
  32.1 17.3 %collective-permute-start.1 = (bf16[176,1024]{1,0:T(8,128)(2,1)S(1)}, bf16[176,1024]{1,0:T(8,128)(2,1)S(1)}, u32[]{:S(2)}, u32[]{:S(2)}) collective-permute-start(bf16[176,1024]{1,0:T(8,128)(2,1)S(1)} %convert_element_type.3.w0_ref), channel_id=1, source_target_pairs={{0,64},{64,0},{1,65},{65,1},{2,66},{66,2},{3,67},{67,3},{4,68},{68... | collective-permute-start | bytes 1081352 | tf_op jit(solution)/shard_map/ppermute | solution.py:282
  36.0 14.8 %collective-permute-start.2 = (bf16[176,1024]{1,0:T(8,128)(2,1)S(1)}, bf16[176,1024]{1,0:T(8,128)(2,1)S(1)}, u32[]{:S(2)}, u32[]{:S(2)}) collective-permute-start(bf16[176,1024]{1,0:T(8,128)(2,1)S(1)} %convert_element_type.3.w0_ref), channel_id=1, source_target_pairs={{0,72},{8,64},{64,8},{72,0},{1,73},{9,65},{65,9},{73,1},{2,74},{10... | collective-permute-start | bytes 1081352 | tf_op jit(solution)/shard_map/ppermute | solution.py:283
  39.3 54.4 %copy-start.3 = (f32[1024]{0:T(1024)S(1)}, f32[1024]{0:T(1024)}, u32[]{:S(2)}) copy-start(f32[1024]{0:T(1024)} %param.20) | copy-start | bytes 12292
  39.4 54.4 %copy-start.4 = (f32[1024]{0:T(1024)S(1)}, f32[1024]{0:T(1024)}, u32[]{:S(2)}) copy-start(f32[1024]{0:T(1024)} %param.21) | copy-start | bytes 12292

commit v4 on v3

--- a/solution.py
+++ b/solution.py
@@ -39,78 +39,96 @@
     return jnp.where(cond, 1.0, 0.0).astype(BF16)
 
 
-def project_kernel(x_ref, gw_ref, uw_ref, gain_ref, bias_ref, out_ref, w_ref, vec_ref):
-    step = pl.program_id(0)
-
-    @pl.when(step == 0)
-    def _():
-        gw = gw_ref[...].astype(BF16)
-        uw = uw_ref[...].astype(BF16)
-        row = iota((PART, FFL), 0)
-        col = iota((PART, FFL), 1)
+def project_kernel(x_ref, gw_ref, uw_ref, gain_ref, bias_ref, out_ref, x_buf, gw_buf, uw_buf, gb_buf, out_buf, w_ref, vec_ref, sems):
+    loads = [
+        pltpu.make_async_copy(gw_ref, gw_buf, sems.at[0]),
+        pltpu.make_async_copy(uw_ref, uw_buf, sems.at[1]),
+        pltpu.make_async_copy(gain_ref, gb_buf.at[0], sems.at[2]),
+        pltpu.make_async_copy(bias_ref, gb_buf.at[1], sems.at[3]),
+    ]
+    tokens = [pltpu.make_async_copy(x_ref.at[:, j // 2, :, j % 2], x_buf.at[j], sems.at[4 + j]) for j in range(4)]
+    for copy in loads + tokens[:1]:
+        copy.start()
+    for copy in loads:
+        copy.wait()
+    for copy in tokens[1:]:
+        copy.start()
+
+    gain = gb_buf[0]
+    row = iota((SLOT, COLS), 0)
+    for k in range(4):
+        first = UNITS * k - 4 * (k % 2)
+        for half, ref in enumerate((gw_buf, uw_buf)):
+            w = ref[first : min(first + SLOT + 8 * (k % 2), FFL)] * gain
+            if k % 2:
+                w = pltpu.roll(w, w.shape[0] - 4, 0)
+            fill = jnp.where(row == UNITS, 1.0, 0.0) if half == 0 else 0.0
+            at = PART * k + SLOT * half
+            w_ref[at : at + SLOT, :] = jnp.where(row < UNITS, w[0:SLOT], fill).astype(BF16)
+    r = iota((128, COLS), 0)
+    ratio = gb_buf[1] / gain
+    rh = rounded(ratio)
+    lead = jnp.where(r == 0, 1.0, jnp.where(r == 1, rh, jnp.where(r == 2, ratio - rh, 0.0))).astype(BF16)
+    cols = dot(w_ref[...], lead, 1, 1)
+    col = cols[:, 0:1]
+    sums = cols.T
+    both = jnp.concatenate([sums[0:1], sums[1:2] + sums[2:3], jnp.zeros((1, ROWS - 8 * PART), F32)], axis=1)
+    hi = rounded(both)
+    q = iota((8, ROWS), 0)
+    vec_ref[...] = jnp.where(q == 0, hi, jnp.where(q == 1, both - hi, 0.0))
+
+    stores = []
+    for j in range(4):
+        at = slice(CHUNK * j, CHUNK * (j + 1))
+        tokens[j].wait()
+        part = dot(w_ref[...], x_buf[j].reshape(CHUNK, COLS), 1, 1)
+        x = x_buf[j].reshape(CHUNK, COLS).astype(F32)
+        pivot = x[:, 0:1]
+        c = x - pivot
+        sq = jnp.sum(c * c, axis=1, keepdims=True)
+        lane = iota((CHUNK, 128), 1)
+        stat = jnp.where(lane == 0, sq, jnp.where(lane == 1, pivot, 0.0)).T
+        m_row = part[UNITS : UNITS + 1] * (1.0 / COLS)
+        off = m_row - stat[1:2]
+        m2_row = stat[0:1] - COLS * off * off
+        m_hi = rounded(m_row)
+        m_mid = rounded(m_row - m_hi)
+        m_lo = m_row - m_hi - m_mid
+        m2_hi = rounded(m2_row)
+        m2_lo = m2_row - m2_hi
+        r = iota((8, CHUNK), 0)
+        t1 = jnp.where(r == 4, m_hi, jnp.where(r == 5, m_mid, jnp.where(r == 6, m_lo, jnp.where(r == 7, vec_ref[0:1, at], 0.0))))
+        t2 = jnp.where(r == 4, m2_hi, jnp.where(r == 5, m2_lo, jnp.where(r == 6, vec_ref[1:2, at], 0.0)))
+        z = jnp.zeros((SLOT - 8, CHUNK), F32)
+        extra = jnp.concatenate([z, t1, z, t2], axis=0)
         for k in range(4):
-            unit = col - UNITS * k
-            as_gate = one_hot((unit == row) & (row < UNITS))
-            as_up = one_hot((unit == row - SLOT) & (row >= SLOT) & (row < SLOT + UNITS))
-            w = dot(as_gate, gw, 1, 0) + dot(as_up, uw, 1, 0)
-            w_ref[PART * k : PART * (k + 1), :] = w.astype(BF16)
-        gain = gain_ref[...]
-        bias = bias_ref[...]
-        r = iota((8, COLS), 0)
-        gh = rounded(gain)
-        bh = rounded(bias)
-        lead = jnp.where(r == 0, gh, jnp.where(r == 1, gain - gh, jnp.where(r == 2, bh, jnp.where(r == 3, bias - bh, 0.0))))
-        sums = dot(lead.astype(BF16), w_ref[...], 1, 1)
-        both = jnp.concatenate(
-            [sums[0:1] + sums[1:2], sums[2:3] + sums[3:4], jnp.zeros((1, ROWS - 8 * PART), F32)], axis=1
-        )
-        hi = rounded(both)
-        q = iota((8, ROWS), 0)
-        vec_ref[...] = jnp.where(q == 0, hi, jnp.where(q == 1, both - hi, 0.0))
-
-    x = x_ref[...].reshape(CHUNK, COLS).astype(F32)
-    m = jnp.sum(x, axis=1, keepdims=True) * (1.0 / COLS)
-    xc = x - m
-    m2 = jnp.sum(xc * xc, axis=1, keepdims=True)
-    xn = (xc * gain_ref[...]).astype(BF16)
-    part = dot(w_ref[...], xn, 1, 1)
-    lane = iota((CHUNK, 128), 1)
-    stat = jnp.where(lane == 0, m, jnp.where(lane == 1, m2, 0.0)).T
-    m_row = stat[0:1]
-    m2_row = stat[1:2]
-    m_hi = rounded(m_row)
-    m_mid = rounded(m_row - m_hi)
-    m_lo = m_row - m_hi - m_mid
-    m2_hi = rounded(m2_row)
-    m2_lo = m2_row - m2_hi
-    vec = vec_ref[:, pl.ds(pl.multiple_of(step * CHUNK, CHUNK), CHUNK)]
-    r = iota((8, CHUNK), 0)
-    t1 = jnp.where(r == 4, m_hi, jnp.where(r == 5, m_mid, jnp.where(r == 6, m_lo, jnp.where(r == 7, vec[0:1], 0.0))))
-    t2 = jnp.where(r == 4, m2_hi, jnp.where(r == 5, m2_lo, jnp.where(r == 6, vec[1:2], 0.0)))
-    z = jnp.zeros((SLOT - 8, CHUNK), F32)
-    extra = jnp.concatenate([z, t1, z, t2], axis=0)
-    for k in range(4):
-        out_ref[k] = (part[PART * k : PART * (k + 1)] + extra).astype(BF16)
+            rows = slice(PART * k, PART * (k + 1))
+            out_buf[k, :, at] = (part[rows] - col[rows] * m_row + extra).astype(BF16)
+        stores.append(pltpu.make_async_copy(out_buf.at[:, :, at], out_ref.at[:, :, at], sems.at[8 + j]))
+        stores[-1].start()
+    for copy in stores:
+        copy.wait()
 
 
 def project(tokens, gate_t, up_t, gain, bias):
-    x = tokens.reshape(4, 2, 4, 2, 16, COLS)
+    hbm = pl.BlockSpec(memory_space=pl.ANY)
     return pl.pallas_call(
         project_kernel,
-        grid=(4,),
-        in_specs=[
-            pl.BlockSpec((4, 1, 4, 1, 16, COLS), lambda j: (0, j // 2, 0, j % 2, 0, 0)),
-            pl.BlockSpec((FFL, COLS), lambda j: (0, 0)),
-            pl.BlockSpec((FFL, COLS), lambda j: (0, 0)),
-            pl.BlockSpec((1, COLS), lambda j: (0, 0)),
-            pl.BlockSpec((1, COLS), lambda j: (0, 0)),
+        in_specs=[hbm] * 5,
+        out_specs=hbm,
+        out_shape=pltpu.HBM((4, PART, ROWS), BF16),
+        scratch_shapes=[
+            pltpu.VMEM((4, 4, 4, 16, COLS), BF16),
+            pltpu.VMEM((FFL, COLS), F32),
+            pltpu.VMEM((FFL, COLS), F32),
+            pltpu.VMEM((2, 1, COLS), F32),
+            pltpu.VMEM((4, PART, ROWS), BF16),
+            pltpu.VMEM((4 * PART, COLS), BF16),
+            pltpu.VMEM((8, ROWS), F32),
+            pltpu.SemaphoreType.DMA((12,)),
         ],
-        out_specs=pl.BlockSpec((4, PART, CHUNK), lambda j: (0, 0, j)),
-        out_shape=jax.ShapeDtypeStruct((4, PART, ROWS), BF16),
-        scratch_shapes=[pltpu.VMEM((4 * PART, COLS), BF16), pltpu.VMEM((8, ROWS), F32)],
-        compiler_params=pltpu.CompilerParams(dimension_semantics=("arbitrary",)),
         name="project",
-    )(x, gate_t, up_t, gain, bias)
+    )(*[pltpu.with_memory_space_constraint(a, pltpu.HBM) for a in (tokens.reshape(4, 2, 4, 2, 16, COLS), gate_t, up_t, gain, bias)])
 
 
 def hidden_kernel(r_ref, gs_ref, us_ref, out_ref, stat_ref):

time: 95.1 us -> 94 us (0.988)
  Pallas kernels: 9.77 us -> 8.71 us
    pallas_call x1, Pallas kernels: 6.09 us -> 5.03 us  [project(): pl.pallas_call(project_kernel, in_specs=[hbm] * 5, out_specs=hbm, out_sha...]
where the time goes in v4:
time: 94 us; the launch traced here: 93.5 us
  blocking collectives  58.2 us (62%)
  starting transfers between devices  14.9 us (16%)
  waiting for transfers between devices  10.7 us (11%)
  Pallas kernels  8.71 us (9%)
    all_to_all x1, blocking collectives, local(): lax.all_to_all(partial.reshape(16, 16, COLS), ('Z', 'Y'), 0, 0, tiled=True)  31.9 us
    all_to_all x1, blocking collectives, local(): received = lax.all_to_all(shares, 'cb', 0, 0, tiled=True)  16.7 us
    all_to_all x1, blocking collectives, local(): parts = lax.all_to_all(part, 'cb', 0, 0, tiled=True)  9.58 us
    ppermute x1, waiting for transfers between devices, local(): w2 = lax.ppermute(w0, 'zl', swapped(2, 1))  6.11 us
    all_to_all x1, starting transfers between devices, local(): lax.all_to_all(sent.reshape(16, SLOT, CHUNK), ('zl', 'yl', 'cb'), 0, 0, t...  5.73 us
    pallas_call x1, Pallas kernels, project(): pl.pallas_call(project_kernel, in_specs=[hbm] * 5, out_specs=hbm, out_sha...  5.03 us
    ppermute x1, starting transfers between devices, local(): w2 = lax.ppermute(w0, 'zl', swapped(2, 1))  3.83 us
    ppermute x1, starting transfers between devices, local(): w3 = lax.ppermute(w0, ('zl', 'yl'), swapped(4, 3))  3.37 us
  transfers between devices with their start and end apart: 4, of which 3 were waited for; matrix products, arithmetic and copies ran while one was open for 1% of the time, Pallas kernels for 0%

profile of v4, /device:TPU:8, one launch (start us, length us, event | category | flops | bytes accessed | tf_op | source)
XLA Modules:
  0.0 93.5 jit_solution(15177734299172285054)
XLA Ops:
  0.0 0.0 copy-start.5
  0.0 0.0 copy-start.6
  0.0 5.0 %project.1 = bf16[4,96,1024]{2,1,0:T(8,128)(2,1)} custom-call(bf16[4,2,4,2,16,1024]{5,4,3,2,1,0:T(8,128)(2,1)} %bitcast.24, f32[176,1024]{1,0:T(8,128)} %bitcast.25, f32[176,1024]{1,0:T(8,128)} %bitcast.26, f32[1,1024]{1,0:T(1,128)} %bitcast.15, f32[1,1024]{1,0:T(1,128)} %bitcast.17), custom_call_target="tpu_custom_call" | custom-call | tf_op jit(solution)/shard_map/project/pallas_call | solution.py:115
  5.0 0.0 copy-start.7
  5.1 16.7 %all_to_all.20.r_ref = bf16[4,96,1024]{2,1,0:T(8,128)(2,1)S(1)} all-to-all(bf16[4,96,1024]{2,1,0:T(8,128)(2,1)} %project.1), channel_id=1, replica_groups=mesh['Z'=4,'zl'=2,'Y'=4,'yl'=2,'cb'=4,'dp'=2] {'cb'}, dimensions={0} | all-to-all | bytes 1572864 | tf_op jit(solution)/shard_map/all_to_all | solution.py:304
  21.8 0.0 copy-done.5
  21.8 0.0 copy-done.6
  21.8 1.5 %hidden.1 = (bf16[4,4,48,256]{3,2,1,0:T(8,128)(2,1)}, f32[8,1024]{1,0:T(8,128)S(1)}) custom-call(bf16[4,96,1024]{2,1,0:T(8,128)(2,1)S(1)} %all_to_all.20.r_ref, f32[1,176]{1,0:T(1,128)S(1)} %bitcast.22, f32[1,176]{1,0:T(1,128)S(1)} %bitcast.23), custom_call_target="tpu_custom_call" | custom-call | tf_op jit(solution)/shard_map/hidden/pallas_call | solution.py:191
  23.2 5.7 %all-to-all-start.1 = ((bf16[16,48,256]{2,1,0:T(8,128)(2,1)}), bf16[16,48,256]{2,1,0:T(8,128)(2,1)S(1)}, u32[]{:S(2)}, u32[]{:S(2)}) async-start(bf16[16,48,256]{2,1,0:T(8,128)(2,1)} %bitcast.7), calls=%async_computation.1 | async-start | bytes 786432 | tf_op jit(solution)/shard_map/all_to_all | solution.py:306
  29.0 0.0 copy-done.7
  29.0 0.0 copy-start
  29.0 0.0 copy-start.1
  29.0 0.0 copy-start.2
  29.1 2.0 %collective-permute-start = (bf16[176,1024]{1,0:T(8,128)(2,1)S(1)}, bf16[176,1024]{1,0:T(8,128)(2,1)S(1)}, u32[]{:S(2)}, u32[]{:S(2)}) collective-permute-start(bf16[176,1024]{1,0:T(8,128)(2,1)S(1)} %convert_element_type.3.w0_ref), channel_id=1, source_target_pairs={{0,8},{8,0},{1,9},{9,1},{2,10},{10,2},{3,11},{11,3},{4,12},{12,4},... | collective-permute-start | bytes 1081352 | tf_op jit(solution)/shard_map/ppermute | solution.py:299
  31.1 3.8 %collective-permute-start.1 = (bf16[176,1024]{1,0:T(8,128)(2,1)S(1)}, bf16[176,1024]{1,0:T(8,128)(2,1)S(1)}, u32[]{:S(2)}, u32[]{:S(2)}) collective-permute-start(bf16[176,1024]{1,0:T(8,128)(2,1)S(1)} %convert_element_type.3.w0_ref), channel_id=1, source_target_pairs={{0,64},{64,0},{1,65},{65,1},{2,66},{66,2},{3,67},{67,3},{4,68},{68... | collective-permute-start | bytes 1081352 | tf_op jit(solution)/shard_map/ppermute | solution.py:300
  34.9 3.4 %collective-permute-start.2 = (bf16[176,1024]{1,0:T(8,128)(2,1)S(1)}, bf16[176,1024]{1,0:T(8,128)(2,1)S(1)}, u32[]{:S(2)}, u32[]{:S(2)}) collective-permute-start(bf16[176,1024]{1,0:T(8,128)(2,1)S(1)} %convert_element_type.3.w0_ref), channel_id=1, source_target_pairs={{0,72},{8,64},{64,8},{72,0},{1,73},{9,65},{65,9},{73,1},{2,74},{10... | collective-permute-start | bytes 1081352 | tf_op jit(solution)/shard_map/ppermute | solution.py:301
  38.3 0.0 copy-start.3
  38.3 0.0 copy-start.4
  38.3 0.8 constant_dynamic-slice_fusion.x_ref
  39.1 0.0 all-to-all-done.1
  39.1 3.1 %collective-permute-done.w1_ref = bf16[176,1024]{1,0:T(8,128)(2,1)S(1)} collective-permute-done((bf16[176,1024]{1,0:T(8,128)(2,1)S(1)}, bf16[176,1024]{1,0:T(8,128)(2,1)S(1)}, u32[]{:S(2)}, u32[]{:S(2)}) %collective-permute-start) | collective-permute-done | bytes 360480 | tf_op jit(solution)/shard_map/ppermute | solution.py:299
  42.2 6.1 %collective-permute-done.1.w2_ref = bf16[176,1024]{1,0:T(8,128)(2,1)S(1)} collective-permute-done((bf16[176,1024]{1,0:T(8,128)(2,1)S(1)}, bf16[176,1024]{1,0:T(8,128)(2,1)S(1)}, u32[]{:S(2)}, u32[]{:S(2)}) %collective-permute-start.1) | collective-permute-done | bytes 360480 | tf_op jit(solution)/shard_map/ppermute | solution.py:300
  48.4 1.4 %collective-permute-done.2.w3_ref = bf16[176,1024]{1,0:T(8,128)(2,1)S(1)} collective-permute-done((bf16[176,1024]{1,0:T(8,128)(2,1)S(1)}, bf16[176,1024]{1,0:T(8,128)(2,1)S(1)}, u32[]{:S(2)}, u32[]{:S(2)}) %collective-permute-start.2) | collective-permute-done | bytes 360480 | tf_op jit(solution)/shard_map/ppermute | solution.py:301
  49.8 1.1 %down.1 = bf16[256,1024]{1,0:T(8,128)(2,1)S(1)} custom-call(bf16[4,192,256]{2,1,0:T(8,128)(2,1)S(1)} %bitcast.14, bf16[176,1024]{1,0:T(8,128)(2,1)S(1)} %convert_element_type.3.w0_ref, bf16[176,1024]{1,0:T(8,128)(2,1)S(1)} %collective-permute-done.w1_ref, bf16[176,1024]{1,0:T(8,128)(2,1)S(1)} %collective-permute-done.1.w2_ref, ...), custom_call_target="tpu_custom_call" | custom-call | tf_op jit(solution)/shard_map/down/pallas_call | solution.py:217
  50.9 31.9 %all_to_all.21.r_ref = bf16[16,16,1024]{2,1,0:T(8,128)(2,1)S(1)} all-to-all(bf16[16,16,1024]{2,1,0:T(8,128)(2,1)S(1)} %bitcast.13), channel_id=1, replica_groups=mesh['Z'=4,'zl'=2,'Y'=4,'yl'=2,'cb'=4,'dp'=2] {'Z','Y'}, dimensions={0} | all-to-all | bytes 1048576 | tf_op jit(solution)/shard_map/all_to_all | solution.py:310
  82.8 0.0 copy-done
  82.8 0.0 copy-done.1
  82.8 0.0 copy-done.2
  82.8 0.3 mix.1
  83.1 9.6 %all_to_all.22.part_ref = f32[4,16,128]{2,1,0:T(8,128)S(1)} all-to-all(f32[4,16,128]{2,1,0:T(8,128)S(1)} %get-tuple-element.16), channel_id=1, replica_groups=mesh['Z'=4,'zl'=2,'Y'=4,'yl'=2,'cb'=4,'dp'=2] {'cb'}, dimensions={0} | all-to-all | bytes 65536 | tf_op jit(solution)/shard_map/all_to_all | solution.py:312
  92.7 0.0 copy-done.3
  92.7 0.0 copy-done.4
  92.7 0.8 finish.1
  (1 shorter events, 0.0 us)
Async XLA Ops:
  0.0 21.8 %copy-start.5 = (f32[176]{0:T(256)S(1)}, f32[176]{0:T(256)}, u32[]{:S(2)}) copy-start(f32[176]{0:T(256)} %param.16) | copy-start | bytes 2116
  0.0 21.8 %copy-start.6 = (f32[176]{0:T(256)S(1)}, f32[176]{0:T(256)}, u32[]{:S(2)}) copy-start(f32[176]{0:T(256)} %param.17) | copy-start | bytes 2116
  5.0 23.9 %copy-start.7 = (f32[176,1024]{1,0:T(8,128)S(1)}, f32[176,1024]{1,0:T(8,128)}, u32[]{:S(2)}) copy-start(f32[176,1024]{1,0:T(8,128)} %param.18) | copy-start | bytes 2162692
  23.2 15.9 %all-to-all-start.1 = ((bf16[16,48,256]{2,1,0:T(8,128)(2,1)}), bf16[16,48,256]{2,1,0:T(8,128)(2,1)S(1)}, u32[]{:S(2)}, u32[]{:S(2)}) async-start(bf16[16,48,256]{2,1,0:T(8,128)(2,1)} %bitcast.7), calls=%async_computation.1 | async-start | bytes 786432 | tf_op jit(solution)/shard_map/all_to_all | solution.py:306
  29.0 53.8 %copy-start = (f32[1024]{0:T(1024)S(1)}, f32[1024]{0:T(1024)}, u32[]{:S(2)}) copy-start(f32[1024]{0:T(1024)} %param.12) | copy-start | bytes 12292
  29.0 53.8 %copy-start.1 = (f32[1024]{0:T(1024)S(1)}, f32[1024]{0:T(1024)}, u32[]{:S(2)}) copy-start(f32[1024]{0:T(1024)} %param.13) | copy-start | bytes 12292
  29.0 53.8 %copy-start.2 = (f32[1024]{0:T(1024)S(1)}, f32[1024]{0:T(1024)}, u32[]{:S(2)}) copy-start(f32[1024]{0:T(1024)} %param.19) | copy-start | bytes 12292
  29.1 13.2 %collective-permute-start = (bf16[176,1024]{1,0:T(8,128)(2,1)S(1)}, bf16[176,1024]{1,0:T(8,128)(2,1)S(1)}, u32[]{:S(2)}, u32[]{:S(2)}) collective-permute-start(bf16[176,1024]{1,0:T(8,128)(2,1)S(1)} %convert_element_type.3.w0_ref), channel_id=1, source_target_pairs={{0,8},{8,0},{1,9},{9,1},{2,10},{10,2},{3,11},{11,3},{4,12},{12,4},... | collective-permute-start | bytes 1081352 | tf_op jit(solution)/shard_map/ppermute | solution.py:299
  31.1 17.3 %collective-permute-start.1 = (bf16[176,1024]{1,0:T(8,128)(2,1)S(1)}, bf16[176,1024]{1,0:T(8,128)(2,1)S(1)}, u32[]{:S(2)}, u32[]{:S(2)}) collective-permute-start(bf16[176,1024]{1,0:T(8,128)(2,1)S(1)} %convert_element_type.3.w0_ref), channel_id=1, source_target_pairs={{0,64},{64,0},{1,65},{65,1},{2,66},{66,2},{3,67},{67,3},{4,68},{68... | collective-permute-start | bytes 1081352 | tf_op jit(solution)/shard_map/ppermute | solution.py:300
  34.9 14.8 %collective-permute-start.2 = (bf16[176,1024]{1,0:T(8,128)(2,1)S(1)}, bf16[176,1024]{1,0:T(8,128)(2,1)S(1)}, u32[]{:S(2)}, u32[]{:S(2)}) collective-permute-start(bf16[176,1024]{1,0:T(8,128)(2,1)S(1)} %convert_element_type.3.w0_ref), channel_id=1, source_target_pairs={{0,72},{8,64},{64,8},{72,0},{1,73},{9,65},{65,9},{73,1},{2,74},{10... | collective-permute-start | bytes 1081352 | tf_op jit(solution)/shard_map/ppermute | solution.py:301
  38.3 54.4 %copy-start.3 = (f32[1024]{0:T(1024)S(1)}, f32[1024]{0:T(1024)}, u32[]{:S(2)}) copy-start(f32[1024]{0:T(1024)} %param.20) | copy-start | bytes 12292
  38.3 54.4 %copy-start.4 = (f32[1024]{0:T(1024)S(1)}, f32[1024]{0:T(1024)}, u32[]{:S(2)}) copy-start(f32[1024]{0:T(1024)} %param.21) | copy-start | bytes 12292

commit v5 on v4

--- a/solution.py
+++ b/solution.py
@@ -197,18 +197,24 @@
     )(*[near(a) for a in (received, gate_scale, up_scale)])
 
 
-def down_kernel(h_ref, w0_ref, w1_ref, w2_ref, w3_ref, out_ref):
+def down_kernel(h_ref, own_ref, fetched_ref, other_ref, out_ref):
     me = lax.axis_index("zl") * 2 + lax.axis_index("yl")
-    row = iota((FFL, 4 * SLOT), 0)
-    lane = iota((FFL, 4 * SLOT), 1)
-    hit = lane < 0
-    for k in range(4):
-        hit = hit | ((lane == row + (SLOT - UNITS) * k) & (row >= UNITS * k) & (row < UNITS * (k + 1)))
-    squeeze = one_hot(hit)
-    acc = jnp.zeros((CHUNK, COLS), F32)
-    for r, w_ref in enumerate((w0_ref, w1_ref, w2_ref, w3_ref)):
-        h = dot(h_ref[me ^ r], squeeze, 0, 1).astype(BF16)
-        acc = acc + dot(h, w_ref[...], 1, 0)
+    core = lax.axis_index("dp")
+
+    def squeezed(member, first, count):
+        unit = iota((count, 4 * SLOT), 0) + first
+        lane = iota((count, 4 * SLOT), 1)
+        hit = lane < 0
+        for k in range(4):
+            hit = hit | ((lane == unit + (SLOT - UNITS) * k) & (unit >= UNITS * k) & (unit < UNITS * (k + 1)))
+        return dot(h_ref[member], one_hot(hit), 0, 1).astype(BF16)
+
+    half = FFL // 2
+    acc = dot(squeezed(me, 0, FFL), own_ref[...], 1, 0)
+    acc = acc + dot(squeezed(me ^ (1 + core), 0, FFL), fetched_ref[0:FFL], 1, 0)
+    acc = acc + dot(squeezed(me ^ (2 - core), 0, FFL), other_ref[0:FFL], 1, 0)
+    acc = acc + dot(squeezed(me ^ 3, core * half, half), fetched_ref[FFL:], 1, 0)
+    acc = acc + dot(squeezed(me ^ 3, half - core * half, half), other_ref[FFL:], 1, 0)
     out_ref[...] = acc.astype(BF16)
 
 
@@ -216,7 +222,7 @@
     vm = pl.BlockSpec(memory_space=pltpu.VMEM)
     return pl.pallas_call(
         down_kernel,
-        in_specs=[vm] * 5,
+        in_specs=[vm] * 4,
         out_specs=vm,
         out_shape=pltpu.VMEM((CHUNK, COLS), BF16),
         name="down",
@@ -296,17 +302,19 @@
     bias = norm_bias.reshape(1, COLS)
 
     w0 = down_weight.astype(BF16)
-    w1 = lax.ppermute(w0, "yl", swapped(2, 1))
-    w2 = lax.ppermute(w0, "zl", swapped(2, 1))
-    w3 = lax.ppermute(w0, ("zl", "yl"), swapped(4, 3))
+    beside = lax.ppermute(w0, ("zl", "yl", "dp"), [(i, i ^ (4 if i & 1 else 2)) for i in range(8)])
+    half = lax.dynamic_slice_in_dim(w0, lax.axis_index("dp") * (FFL // 2), FFL // 2, 0)
+    across = lax.ppermute(half, ("zl", "yl"), swapped(4, 3))
 
     shares = project(tokens, gate_weight.T, up_weight.T, gain, bias)
     received = lax.all_to_all(shares, "cb", 0, 0, tiled=True)
     sent, stats = hidden_of(received, gate_scale.reshape(1, FFL), up_scale.reshape(1, FFL))
     hidden = lax.all_to_all(sent.reshape(16, SLOT, CHUNK), ("zl", "yl", "cb"), 0, 0, tiled=True)
+    fetched = jnp.concatenate([beside, across], axis=0)
+    other = lax.ppermute(fetched, "dp", swapped(2, 1))
     own = lax.dynamic_slice_in_dim(tokens, lax.axis_index(RA) * 16, 16, 0)
     hidden, own = lax.optimization_barrier((hidden, own))
-    partial = down(hidden.reshape(4, 4 * SLOT, CHUNK), (w0, w1, w2, w3))
+    partial = down(hidden.reshape(4, 4 * SLOT, CHUNK), (w0, fetched, other))
     pieces = lax.all_to_all(partial.reshape(16, 16, COLS), ("Z", "Y"), 0, 0, tiled=True)
     mixed, part = mix(pieces, own, stats, gain, bias, down_scale.reshape(1, COLS))
     parts = lax.all_to_all(part, "cb", 0, 0, tiled=True)

time: 94 us -> 79.4 us (0.84)
  the two profiles are of different devices: /device:TPU:8 before, /device:TPU:2 now
where the time goes in v5:
time: 79.4 us; the launch traced here: 78.8 us
  blocking collectives  39.6 us (50%)
  starting transfers between devices  20.1 us (25%)
  Pallas kernels  9.03 us (11%)
  waiting for transfers between devices  8.98 us (11%)
  local copies, waits for them, and re-layouts  0.87 us (1%)
    all_to_all x1, blocking collectives, local(): lax.all_to_all(partial.reshape(16, 16, COLS), ('Z', 'Y'), 0, 0, tiled=True)  31.6 us
    all_to_all x1, starting transfers between devices, local(): received = lax.all_to_all(shares, 'cb', 0, 0, tiled=True)  9.36 us
    all_to_all x1, blocking collectives, local(): parts = lax.all_to_all(part, 'cb', 0, 0, tiled=True)  7.94 us
    pallas_call x1, Pallas kernels, project(): pl.pallas_call(project_kernel, in_specs=[hbm] * 5, out_specs=hbm, out_sha...  5.07 us
    all_to_all x1, starting transfers between devices, local(): lax.all_to_all(sent.reshape(16, SLOT, CHUNK), ('zl', 'yl', 'cb'), 0, 0, t...  5.01 us
    all_to_all x1, waiting for transfers between devices, local(): lax.all_to_all(sent.reshape(16, SLOT, CHUNK), ('zl', 'yl', 'cb'), 0, 0, t...  4.88 us
    all_to_all x1, waiting for transfers between devices, local(): received = lax.all_to_all(shares, 'cb', 0, 0, tiled=True)  4.09 us
    ppermute x1, starting transfers between devices, local(): lax.ppermute(w0, ('zl', 'yl', 'dp'), [(i, i ^ (4 if i & 1 else 2)) for i...  1.92 us
  transfers between devices with their start and end apart: 5, of which 2 were waited for; matrix products, arithmetic and copies ran while one was open for 1% of the time, Pallas kernels for 2%

profile of v5, /device:TPU:2, one launch (start us, length us, event | category | flops | bytes accessed | tf_op | source)
XLA Modules:
  0.0 78.8 jit_solution(16804314215515723834)
XLA Ops:
  0.0 0.0 copy-start.7
  0.0 5.1 %project.1 = bf16[4,96,1024]{2,1,0:T(8,128)(2,1)} custom-call(bf16[4,2,4,2,16,1024]{5,4,3,2,1,0:T(8,128)(2,1)} %bitcast.24, f32[176,1024]{1,0:T(8,128)} %bitcast.25, f32[176,1024]{1,0:T(8,128)} %bitcast.26, f32[1,1024]{1,0:T(1,128)} %bitcast.15, f32[1,1024]{1,0:T(1,128)} %bitcast.17), custom_call_target="tpu_custom_call" | custom-call | tf_op jit(solution)/shard_map/project/pallas_call | solution.py:115
  5.1 0.0 copy-start.5
  5.1 0.0 copy-start.6
  5.1 9.4 %all-to-all-start = ((bf16[4,96,1024]{2,1,0:T(8,128)(2,1)}), bf16[4,96,1024]{2,1,0:T(8,128)(2,1)S(1)}, u32[]{:S(2)}, u32[]{:S(2)}) async-start(bf16[4,96,1024]{2,1,0:T(8,128)(2,1)} %project.1), calls=%async_computation | async-start | bytes 1572864 | tf_op jit(solution)/shard_map/all_to_all | solution.py:310
  14.5 0.0 copy-done.7
  14.5 1.9 %collective-permute-start = (bf16[176,1024]{1,0:T(8,128)(2,1)S(1)}, bf16[176,1024]{1,0:T(8,128)(2,1)S(1)}, u32[]{:S(2)}, u32[]{:S(2)}) collective-permute-start(bf16[176,1024]{1,0:T(8,128)(2,1)S(1)} %convert_element_type.3.own_ref), channel_id=1, source_target_pairs={{0,8},{1,65},{8,0},{9,73},{64,72},{65,1},{72,64},{73,9},{2,10},{3,... | collective-permute-start | bytes 1081352 | tf_op jit(solution)/shard_map/ppermute | solution.py:305
  16.5 1.9 %collective-permute-start.1 = (bf16[88,1024]{1,0:T(8,128)(2,1)S(1)}, bf16[88,1024]{1,0:T(8,128)(2,1)S(1)}, u32[]{:S(2)}, u32[]{:S(2)}) collective-permute-start(bf16[88,1024]{1,0:T(8,128)(2,1)S(1)} %constant_dynamic-slice_fusion), channel_id=1, source_target_pairs={{0,72},{8,64},{64,8},{72,0},{1,73},{9,65},{65,9},{73,1},{2,74},{10... | collective-permute-start | bytes 540680 | tf_op jit(solution)/shard_map/ppermute | solution.py:307
  18.4 4.1 %all-to-all-done.r_ref = bf16[4,96,1024]{2,1,0:T(8,128)(2,1)S(1)} async-done(((bf16[4,96,1024]{2,1,0:T(8,128)(2,1)}), bf16[4,96,1024]{2,1,0:T(8,128)(2,1)S(1)}, u32[]{:S(2)}, u32[]{:S(2)}) %all-to-all-start) | async-done | bytes 786464 | tf_op jit(solution)/shard_map/all_to_all | solution.py:310
  22.5 0.0 copy-done.5
  22.5 0.0 copy-done.6
  22.5 1.5 %hidden.1 = (bf16[4,4,48,256]{3,2,1,0:T(8,128)(2,1)}, f32[8,1024]{1,0:T(8,128)S(1)}) custom-call(bf16[4,96,1024]{2,1,0:T(8,128)(2,1)S(1)} %all-to-all-done.r_ref, f32[1,176]{1,0:T(1,128)S(1)} %bitcast.22, f32[1,176]{1,0:T(1,128)S(1)} %bitcast.23), custom_call_target="tpu_custom_call" | custom-call | tf_op jit(solution)/shard_map/hidden/pallas_call | solution.py:191
  24.0 5.0 %all-to-all-start.1 = ((bf16[16,48,256]{2,1,0:T(8,128)(2,1)}), bf16[16,48,256]{2,1,0:T(8,128)(2,1)S(1)}, u32[]{:S(2)}, u32[]{:S(2)}) async-start(bf16[16,48,256]{2,1,0:T(8,128)(2,1)} %bitcast.7), calls=%async_computation.1 | async-start | bytes 786432 | tf_op jit(solution)/shard_map/all_to_all | solution.py:312
  29.0 0.0 collective-permute-done
  29.0 0.0 copy-start
  29.0 0.0 copy-start.1
  29.0 0.0 copy-start.2
  29.1 0.0 collective-permute-done.1
  29.1 1.9 %collective-permute-start.2 = (bf16[264,1024]{1,0:T(8,128)(2,1)S(1)}, bf16[264,1024]{1,0:T(8,128)(2,1)S(1)}, u32[]{:S(2)}, u32[]{:S(2)}) collective-permute-start(bf16[264,1024]{1,0:T(8,128)(2,1)S(1)} %constant_dynamic-update-slice_fusion.fetched_ref), channel_id=1, source_target_pairs={{0,1},{1,0},{2,3},{3,2},{4,5},{5,4},{6,7},{7,6},{8,9},{9,8},{10,11... | collective-permute-start | bytes 1622024 | tf_op jit(solution)/shard_map/ppermute | solution.py:314
  31.0 0.0 copy-start.3
  31.0 0.0 copy-start.4
  31.1 0.8 constant_dynamic-slice_fusion.1.x_ref
  31.8 4.9 %all-to-all-done.1 = bf16[16,48,256]{2,1,0:T(8,128)(2,1)S(1)} async-done(((bf16[16,48,256]{2,1,0:T(8,128)(2,1)}), bf16[16,48,256]{2,1,0:T(8,128)(2,1)S(1)}, u32[]{:S(2)}, u32[]{:S(2)}) %all-to-all-start.1) | async-done | bytes 393248 | tf_op jit(solution)/shard_map/all_to_all | solution.py:312
  36.7 0.0 collective-permute-done.2.other_ref
  36.7 1.4 %down.1 = bf16[256,1024]{1,0:T(8,128)(2,1)S(1)} custom-call(bf16[4,192,256]{2,1,0:T(8,128)(2,1)S(1)} %bitcast.14, bf16[176,1024]{1,0:T(8,128)(2,1)S(1)} %convert_element_type.3.own_ref, bf16[264,1024]{1,0:T(8,128)(2,1)S(1)} %constant_dynamic-update-slice_fusion.fetched_ref, bf16[264,1024]{1,0:T(8,128)(2,1)S(1)} %collective-permute-done.2.other_ref), custom_call_target="tpu_custom_call" | custom-call | tf_op jit(solution)/shard_map/down/pallas_call | solution.py:223
  38.1 31.6 %all_to_all.20.r_ref = bf16[16,16,1024]{2,1,0:T(8,128)(2,1)S(1)} all-to-all(bf16[16,16,1024]{2,1,0:T(8,128)(2,1)S(1)} %bitcast.13), channel_id=1, replica_groups=mesh['Z'=4,'zl'=2,'Y'=4,'yl'=2,'cb'=4,'dp'=2] {'Z','Y'}, dimensions={0} | all-to-all | bytes 1048576 | tf_op jit(solution)/shard_map/all_to_all | solution.py:318
  69.8 0.0 copy-done
  69.8 0.0 copy-done.1
  69.8 0.0 copy-done.2
  69.8 0.3 mix.1
  70.1 7.9 %all_to_all.21.part_ref = f32[4,16,128]{2,1,0:T(8,128)S(1)} all-to-all(f32[4,16,128]{2,1,0:T(8,128)S(1)} %get-tuple-element.16), channel_id=1, replica_groups=mesh['Z'=4,'zl'=2,'Y'=4,'yl'=2,'cb'=4,'dp'=2] {'cb'}, dimensions={0} | all-to-all | bytes 65536 | tf_op jit(solution)/shard_map/all_to_all | solution.py:320
  78.0 0.0 copy-done.3
  78.0 0.0 copy-done.4
  78.0 0.8 finish.1
  (4 shorter events, 0.1 us)
Async XLA Ops:
  0.0 14.5 %copy-start.7 = (f32[176,1024]{1,0:T(8,128)S(1)}, f32[176,1024]{1,0:T(8,128)}, u32[]{:S(2)}) copy-start(f32[176,1024]{1,0:T(8,128)} %param.18) | copy-start | bytes 2162692
  5.1 17.4 %copy-start.5 = (f32[176]{0:T(256)S(1)}, f32[176]{0:T(256)}, u32[]{:S(2)}) copy-start(f32[176]{0:T(256)} %param.16) | copy-start | bytes 2116
  5.1 17.4 %copy-start.6 = (f32[176]{0:T(256)S(1)}, f32[176]{0:T(256)}, u32[]{:S(2)}) copy-start(f32[176]{0:T(256)} %param.17) | copy-start | bytes 2116
  5.1 17.4 %all-to-all-start = ((bf16[4,96,1024]{2,1,0:T(8,128)(2,1)}), bf16[4,96,1024]{2,1,0:T(8,128)(2,1)S(1)}, u32[]{:S(2)}, u32[]{:S(2)}) async-start(bf16[4,96,1024]{2,1,0:T(8,128)(2,1)} %project.1), calls=%async_computation | async-start | bytes 1572864 | tf_op jit(solution)/shard_map/all_to_all | solution.py:310
  14.5 14.5 %collective-permute-start = (bf16[176,1024]{1,0:T(8,128)(2,1)S(1)}, bf16[176,1024]{1,0:T(8,128)(2,1)S(1)}, u32[]{:S(2)}, u32[]{:S(2)}) collective-permute-start(bf16[176,1024]{1,0:T(8,128)(2,1)S(1)} %convert_element_type.3.own_ref), channel_id=1, source_target_pairs={{0,8},{1,65},{8,0},{9,73},{64,72},{65,1},{72,64},{73,9},{2,10},{3,... | collective-permute-start | bytes 1081352 | tf_op jit(solution)/shard_map/ppermute | solution.py:305
  16.5 12.6 %collective-permute-start.1 = (bf16[88,1024]{1,0:T(8,128)(2,1)S(1)}, bf16[88,1024]{1,0:T(8,128)(2,1)S(1)}, u32[]{:S(2)}, u32[]{:S(2)}) collective-permute-start(bf16[88,1024]{1,0:T(8,128)(2,1)S(1)} %constant_dynamic-slice_fusion), channel_id=1, source_target_pairs={{0,72},{8,64},{64,8},{72,0},{1,73},{9,65},{65,9},{73,1},{2,74},{10... | collective-permute-start | bytes 540680 | tf_op jit(solution)/shard_map/ppermute | solution.py:307
  24.0 12.7 %all-to-all-start.1 = ((bf16[16,48,256]{2,1,0:T(8,128)(2,1)}), bf16[16,48,256]{2,1,0:T(8,128)(2,1)S(1)}, u32[]{:S(2)}, u32[]{:S(2)}) async-start(bf16[16,48,256]{2,1,0:T(8,128)(2,1)} %bitcast.7), calls=%async_computation.1 | async-start | bytes 786432 | tf_op jit(solution)/shard_map/all_to_all | solution.py:312
  29.0 40.8 %copy-start = (f32[1024]{0:T(1024)S(1)}, f32[1024]{0:T(1024)}, u32[]{:S(2)}) copy-start(f32[1024]{0:T(1024)} %param.12) | copy-start | bytes 12292
  29.0 40.8 %copy-start.1 = (f32[1024]{0:T(1024)S(1)}, f32[1024]{0:T(1024)}, u32[]{:S(2)}) copy-start(f32[1024]{0:T(1024)} %param.13) | copy-start | bytes 12292
  29.0 40.7 %copy-start.2 = (f32[1024]{0:T(1024)S(1)}, f32[1024]{0:T(1024)}, u32[]{:S(2)}) copy-start(f32[1024]{0:T(1024)} %param.19) | copy-start | bytes 12292
  29.1 7.6 %collective-permute-start.2 = (bf16[264,1024]{1,0:T(8,128)(2,1)S(1)}, bf16[264,1024]{1,0:T(8,128)(2,1)S(1)}, u32[]{:S(2)}, u32[]{:S(2)}) collective-permute-start(bf16[264,1024]{1,0:T(8,128)(2,1)S(1)} %constant_dynamic-update-slice_fusion.fetched_ref), channel_id=1, source_target_pairs={{0,1},{1,0},{2,3},{3,2},{4,5},{5,4},{6,7},{7,6},{8,9},{9,8},{10,11... | collective-permute-start | bytes 1622024 | tf_op jit(solution)/shard_map/ppermute | solution.py:314
  31.0 47.0 %copy-start.3 = (f32[1024]{0:T(1024)S(1)}, f32[1024]{0:T(1024)}, u32[]{:S(2)}) copy-start(f32[1024]{0:T(1024)} %param.20) | copy-start | bytes 12292
  31.0 47.0 %copy-start.4 = (f32[1024]{0:T(1024)S(1)}, f32[1024]{0:T(1024)}, u32[]{:S(2)}) copy-start(f32[1024]{0:T(1024)} %param.21) | copy-start | bytes 12292

commit v6 on v5

--- a/solution.py
+++ b/solution.py
@@ -17,6 +17,8 @@
 COLS = 1024
 FFL = 176
 CHUNK = 256
+PER = 2
+TILE = PER * CHUNK
 
 
 def iota(shape, dim):
@@ -47,11 +49,11 @@
         pltpu.make_async_copy(bias_ref, gb_buf.at[1], sems.at[3]),
     ]
     tokens = [pltpu.make_async_copy(x_ref.at[:, j // 2, :, j % 2], x_buf.at[j], sems.at[4 + j]) for j in range(4)]
-    for copy in loads + tokens[:1]:
+    for copy in loads + tokens[:PER]:
         copy.start()
     for copy in loads:
         copy.wait()
-    for copy in tokens[1:]:
+    for copy in tokens[PER:]:
         copy.start()
 
     gain = gb_buf[0]
@@ -78,15 +80,16 @@
     vec_ref[...] = jnp.where(q == 0, hi, jnp.where(q == 1, both - hi, 0.0))
 
     stores = []
-    for j in range(4):
-        at = slice(CHUNK * j, CHUNK * (j + 1))
-        tokens[j].wait()
-        part = dot(w_ref[...], x_buf[j].reshape(CHUNK, COLS), 1, 1)
-        x = x_buf[j].reshape(CHUNK, COLS).astype(F32)
+    for j in range(4 // PER):
+        at = slice(TILE * j, TILE * (j + 1))
+        for copy in tokens[PER * j : PER * (j + 1)]:
+            copy.wait()
+        part = dot(w_ref[...], x_buf[PER * j : PER * (j + 1)].reshape(TILE, COLS), 1, 1)
+        x = x_buf[PER * j : PER * (j + 1)].reshape(TILE, COLS).astype(F32)
         pivot = x[:, 0:1]
         c = x - pivot
         sq = jnp.sum(c * c, axis=1, keepdims=True)
-        lane = iota((CHUNK, 128), 1)
+        lane = iota((TILE, 128), 1)
         stat = jnp.where(lane == 0, sq, jnp.where(lane == 1, pivot, 0.0)).T
         m_row = part[UNITS : UNITS + 1] * (1.0 / COLS)
         off = m_row - stat[1:2]
@@ -96,10 +99,10 @@
         m_lo = m_row - m_hi - m_mid
         m2_hi = rounded(m2_row)
         m2_lo = m2_row - m2_hi
-        r = iota((8, CHUNK), 0)
+        r = iota((8, TILE), 0)
         t1 = jnp.where(r == 4, m_hi, jnp.where(r == 5, m_mid, jnp.where(r == 6, m_lo, jnp.where(r == 7, vec_ref[0:1, at], 0.0))))
         t2 = jnp.where(r == 4, m2_hi, jnp.where(r == 5, m2_lo, jnp.where(r == 6, vec_ref[1:2, at], 0.0)))
-        z = jnp.zeros((SLOT - 8, CHUNK), F32)
+        z = jnp.zeros((SLOT - 8, TILE), F32)
         extra = jnp.concatenate([z, t1, z, t2], axis=0)
         for k in range(4):
             rows = slice(PART * k, PART * (k + 1))
@@ -201,20 +204,20 @@
     me = lax.axis_index("zl") * 2 + lax.axis_index("yl")
     core = lax.axis_index("dp")
 
-    def squeezed(member, first, count):
-        unit = iota((count, 4 * SLOT), 0) + first
-        lane = iota((count, 4 * SLOT), 1)
-        hit = lane < 0
-        for k in range(4):
-            hit = hit | ((lane == unit + (SLOT - UNITS) * k) & (unit >= UNITS * k) & (unit < UNITS * (k + 1)))
-        return dot(h_ref[member], one_hot(hit), 0, 1).astype(BF16)
-
-    half = FFL // 2
-    acc = dot(squeezed(me, 0, FFL), own_ref[...], 1, 0)
-    acc = acc + dot(squeezed(me ^ (1 + core), 0, FFL), fetched_ref[0:FFL], 1, 0)
-    acc = acc + dot(squeezed(me ^ (2 - core), 0, FFL), other_ref[0:FFL], 1, 0)
-    acc = acc + dot(squeezed(me ^ 3, core * half, half), fetched_ref[FFL:], 1, 0)
-    acc = acc + dot(squeezed(me ^ 3, half - core * half, half), other_ref[FFL:], 1, 0)
+    unit = iota((FFL, 4 * SLOT), 0)
+    slot = jnp.where(unit < 2 * UNITS, jnp.where(unit < UNITS, 0, 1), jnp.where(unit < 3 * UNITS, 2, 3))
+    place = one_hot(iota((FFL, 4 * SLOT), 1) == unit + (SLOT - UNITS) * slot)
+
+    def squeezed(member):
+        return dot(h_ref[member], place, 0, 1).astype(BF16)
+
+    acc = dot(squeezed(me), own_ref[...], 1, 0)
+    acc = acc + dot(squeezed(me ^ (1 + core)), fetched_ref[:, 0:COLS], 1, 0)
+    acc = acc + dot(squeezed(me ^ (2 - core)), other_ref[:, 0:COLS], 1, 0)
+    h = squeezed(me ^ 3)
+    mine = dot(h, fetched_ref[:, COLS:], 1, 0)
+    theirs = dot(h, other_ref[:, COLS:], 1, 0)
+    acc = acc + jnp.concatenate([jnp.where(core == 0, mine, theirs), jnp.where(core == 0, theirs, mine)], axis=1)
     out_ref[...] = acc.astype(BF16)
 
 
@@ -303,17 +306,17 @@
 
     w0 = down_weight.astype(BF16)
     beside = lax.ppermute(w0, ("zl", "yl", "dp"), [(i, i ^ (4 if i & 1 else 2)) for i in range(8)])
-    half = lax.dynamic_slice_in_dim(w0, lax.axis_index("dp") * (FFL // 2), FFL // 2, 0)
+    half = lax.dynamic_slice_in_dim(w0, lax.axis_index("dp") * (COLS // 2), COLS // 2, 1)
     across = lax.ppermute(half, ("zl", "yl"), swapped(4, 3))
 
     shares = project(tokens, gate_weight.T, up_weight.T, gain, bias)
     received = lax.all_to_all(shares, "cb", 0, 0, tiled=True)
     sent, stats = hidden_of(received, gate_scale.reshape(1, FFL), up_scale.reshape(1, FFL))
+    own = lax.dynamic_slice_in_dim(tokens, lax.axis_index(RA) * 16, 16, 0)
+    sent, own = lax.optimization_barrier((sent, own))
     hidden = lax.all_to_all(sent.reshape(16, SLOT, CHUNK), ("zl", "yl", "cb"), 0, 0, tiled=True)
-    fetched = jnp.concatenate([beside, across], axis=0)
+    fetched = jnp.concatenate([beside, across], axis=1)
     other = lax.ppermute(fetched, "dp", swapped(2, 1))
-    own = lax.dynamic_slice_in_dim(tokens, lax.axis_index(RA) * 16, 16, 0)
-    hidden, own = lax.optimization_barrier((hidden, own))
     partial = down(hidden.reshape(4, 4 * SLOT, CHUNK), (w0, fetched, other))
     pieces = lax.all_to_all(partial.reshape(16, 16, COLS), ("Z", "Y"), 0, 0, tiled=True)
     mixed, part = mix(pieces, own, stats, gain, bias, down_scale.reshape(1, COLS))

time: 79.4 us -> 78.4 us (0.987)
  Pallas kernels: 9.03 us -> 8.09 us
    ppermute x1, waiting for transfers between devices: 0.01 us -> 1.9 us  [local(): other = lax.ppermute(fetched, 'dp', swapped(2, 1))]
    all_to_all x1, waiting for transfers between devices: 4.88 us -> 3.76 us  [local(): lax.all_to_all(sent.reshape(16, SLOT, CHUNK), ('zl', 'yl', 'cb'), 0, 0, t...]
  transfers between devices with their start and end apart: 5 -> 5, of which waited for: 2 -> 3; matrix products, arithmetic and copies ran while one was open for 1% -> 1% of each run, Pallas kernels for 2% -> 2%
where the time goes in v6:
time: 78.4 us; the launch traced here: 77.8 us
  blocking collectives  39.6 us (51%)
  starting transfers between devices  20.1 us (26%)
  waiting for transfers between devices  8.98 us (11%)
  Pallas kernels  8.09 us (10%)
  local copies, waits for them, and re-layouts  0.87 us (1%)
    all_to_all x1, blocking collectives, local(): lax.all_to_all(partial.reshape(16, 16, COLS), ('Z', 'Y'), 0, 0, tiled=True)  31.6 us
    all_to_all x1, starting transfers between devices, local(): received = lax.all_to_all(shares, 'cb', 0, 0, tiled=True)  9.35 us
    all_to_all x1, blocking collectives, local(): parts = lax.all_to_all(part, 'cb', 0, 0, tiled=True)  7.93 us
    all_to_all x1, starting transfers between devices, local(): lax.all_to_all(sent.reshape(16, SLOT, CHUNK), ('zl', 'yl', 'cb'), 0, 0, t...  5.02 us
    pallas_call x1, Pallas kernels, project(): pl.pallas_call(project_kernel, in_specs=[hbm] * 5, out_specs=hbm, out_sha...  4.35 us
    all_to_all x1, waiting for transfers between devices, local(): lax.all_to_all(sent.reshape(16, SLOT, CHUNK), ('zl', 'yl', 'cb'), 0, 0, t...  3.76 us
    all_to_all x1, waiting for transfers between devices, local(): received = lax.all_to_all(shares, 'cb', 0, 0, tiled=True)  3.31 us
    ppermute x1, starting transfers between devices, local(): lax.ppermute(w0, ('zl', 'yl', 'dp'), [(i, i ^ (4 if i & 1 else 2)) for i...  1.92 us
  transfers between devices with their start and end apart: 5, of which 3 were waited for; matrix products, arithmetic and copies ran while one was open for 1% of the time, Pallas kernels for 2%

profile of v6, /device:TPU:2, one launch (start us, length us, event | category | flops | bytes accessed | tf_op | source)
XLA Modules:
  0.0 77.8 jit_solution(10955003314118776055)
XLA Ops:
  0.0 0.0 copy-start.7
  0.0 4.4 %project.1 = bf16[4,96,1024]{2,1,0:T(8,128)(2,1)} custom-call(bf16[4,2,4,2,16,1024]{5,4,3,2,1,0:T(8,128)(2,1)} %bitcast.24, f32[176,1024]{1,0:T(8,128)} %bitcast.25, f32[176,1024]{1,0:T(8,128)} %bitcast.26, f32[1,1024]{1,0:T(1,128)} %bitcast.15, f32[1,1024]{1,0:T(1,128)} %bitcast.17), custom_call_target="tpu_custom_call" | custom-call | tf_op jit(solution)/shard_map/project/pallas_call | solution.py:118
  4.4 0.0 copy-start.5
  4.4 0.0 copy-start.6
  4.4 9.3 %all-to-all-start = ((bf16[4,96,1024]{2,1,0:T(8,128)(2,1)}), bf16[4,96,1024]{2,1,0:T(8,128)(2,1)S(1)}, u32[]{:S(2)}, u32[]{:S(2)}) async-start(bf16[4,96,1024]{2,1,0:T(8,128)(2,1)} %project.1), calls=%async_computation | async-start | bytes 1572864 | tf_op jit(solution)/shard_map/all_to_all | solution.py:313
  13.7 0.0 copy-done.7
  13.8 1.9 %collective-permute-start = (bf16[176,1024]{1,0:T(8,128)(2,1)S(1)}, bf16[176,1024]{1,0:T(8,128)(2,1)S(1)}, u32[]{:S(2)}, u32[]{:S(2)}) collective-permute-start(bf16[176,1024]{1,0:T(8,128)(2,1)S(1)} %convert_element_type.3.own_ref), channel_id=1, source_target_pairs={{0,8},{1,65},{8,0},{9,73},{64,72},{65,1},{72,64},{73,9},{2,10},{3,... | collective-permute-start | bytes 1081352 | tf_op jit(solution)/shard_map/ppermute | solution.py:308
  15.7 1.9 %collective-permute-start.1 = (bf16[176,512]{1,0:T(8,128)(2,1)S(1)}, bf16[176,512]{1,0:T(8,128)(2,1)S(1)}, u32[]{:S(2)}, u32[]{:S(2)}) collective-permute-start(bf16[176,512]{1,0:T(8,128)(2,1)S(1)} %constant_dynamic-slice_fusion), channel_id=1, source_target_pairs={{0,72},{8,64},{64,8},{72,0},{1,73},{9,65},{65,9},{73,1},{2,74},{10... | collective-permute-start | bytes 540680 | tf_op jit(solution)/shard_map/ppermute | solution.py:310
  17.7 0.8 constant_dynamic-slice_fusion.1.x_ref
  18.5 3.3 %all-to-all-done.r_ref = bf16[4,96,1024]{2,1,0:T(8,128)(2,1)S(1)} async-done(((bf16[4,96,1024]{2,1,0:T(8,128)(2,1)}), bf16[4,96,1024]{2,1,0:T(8,128)(2,1)S(1)}, u32[]{:S(2)}, u32[]{:S(2)}) %all-to-all-start) | async-done | bytes 786464 | tf_op jit(solution)/shard_map/all_to_all | solution.py:313
  21.8 0.0 copy-done.5
  21.8 0.0 copy-done.6
  21.8 1.5 %hidden.1 = (bf16[4,4,48,256]{3,2,1,0:T(8,128)(2,1)}, f32[8,1024]{1,0:T(8,128)S(1)}) custom-call(bf16[4,96,1024]{2,1,0:T(8,128)(2,1)S(1)} %all-to-all-done.r_ref, f32[1,176]{1,0:T(1,128)S(1)} %bitcast.22, f32[1,176]{1,0:T(1,128)S(1)} %bitcast.23), custom_call_target="tpu_custom_call" | custom-call | tf_op jit(solution)/shard_map/hidden/pallas_call | solution.py:194
  23.3 5.0 %all-to-all-start.1 = ((bf16[16,48,256]{2,1,0:T(8,128)(2,1)}), bf16[16,48,256]{2,1,0:T(8,128)(2,1)S(1)}, u32[]{:S(2)}, u32[]{:S(2)}) async-start(bf16[16,48,256]{2,1,0:T(8,128)(2,1)} %bitcast.7), calls=%async_computation.1 | async-start | bytes 786432 | tf_op jit(solution)/shard_map/all_to_all | solution.py:317
  28.3 0.0 copy-start
  28.3 0.0 copy-start.1
  28.3 0.0 copy-start.2
  28.3 0.0 collective-permute-done
  28.4 0.0 collective-permute-done.1
  28.4 0.0 copy-start.3
  28.4 0.0 copy-start.4
  28.4 1.9 %collective-permute-start.2 = (bf16[176,1536]{1,0:T(8,128)(2,1)S(1)}, bf16[176,1536]{1,0:T(8,128)(2,1)S(1)}, u32[]{:S(2)}, u32[]{:S(2)}) collective-permute-start(bf16[176,1536]{1,0:T(8,128)(2,1)S(1)} %constant_dynamic-update-slice_fusion.fetched_ref), channel_id=1, source_target_pairs={{0,1},{1,0},{2,3},{3,2},{4,5},{5,4},{6,7},{7,6},{8,9},{9,8},{10,11... | collective-permute-start | bytes 1622024 | tf_op jit(solution)/shard_map/ppermute | solution.py:319
  30.3 1.9 %collective-permute-done.2.other_ref = bf16[176,1536]{1,0:T(8,128)(2,1)S(1)} collective-permute-done((bf16[176,1536]{1,0:T(8,128)(2,1)S(1)}, bf16[176,1536]{1,0:T(8,128)(2,1)S(1)}, u32[]{:S(2)}, u32[]{:S(2)}) %collective-permute-start.2) | collective-permute-done | bytes 540704 | tf_op jit(solution)/shard_map/ppermute | solution.py:319
  32.2 3.8 %all-to-all-done.1 = bf16[16,48,256]{2,1,0:T(8,128)(2,1)S(1)} async-done(((bf16[16,48,256]{2,1,0:T(8,128)(2,1)}), bf16[16,48,256]{2,1,0:T(8,128)(2,1)S(1)}, u32[]{:S(2)}, u32[]{:S(2)}) %all-to-all-start.1) | async-done | bytes 393248 | tf_op jit(solution)/shard_map/all_to_all | solution.py:317
  36.0 1.2 %down.1 = bf16[256,1024]{1,0:T(8,128)(2,1)S(1)} custom-call(bf16[4,192,256]{2,1,0:T(8,128)(2,1)S(1)} %bitcast.14, bf16[176,1024]{1,0:T(8,128)(2,1)S(1)} %convert_element_type.3.own_ref, bf16[176,1536]{1,0:T(8,128)(2,1)S(1)} %constant_dynamic-update-slice_fusion.fetched_ref, bf16[176,1536]{1,0:T(8,128)(2,1)S(1)} %collective-permute-done.2.other_ref), custom_call_target="tpu_custom_call" | custom-call | tf_op jit(solution)/shard_map/down/pallas_call | solution.py:226
  37.2 31.6 %all_to_all.20.r_ref = bf16[16,16,1024]{2,1,0:T(8,128)(2,1)S(1)} all-to-all(bf16[16,16,1024]{2,1,0:T(8,128)(2,1)S(1)} %bitcast.13), channel_id=1, replica_groups=mesh['Z'=4,'zl'=2,'Y'=4,'yl'=2,'cb'=4,'dp'=2] {'Z','Y'}, dimensions={0} | all-to-all | bytes 1048576 | tf_op jit(solution)/shard_map/all_to_all | solution.py:321
  68.8 0.0 copy-done
  68.8 0.0 copy-done.1
  68.8 0.0 copy-done.2
  68.8 0.3 mix.1
  69.1 7.9 %all_to_all.21.part_ref = f32[4,16,128]{2,1,0:T(8,128)S(1)} all-to-all(f32[4,16,128]{2,1,0:T(8,128)S(1)} %get-tuple-element.16), channel_id=1, replica_groups=mesh['Z'=4,'zl'=2,'Y'=4,'yl'=2,'cb'=4,'dp'=2] {'cb'}, dimensions={0} | all-to-all | bytes 65536 | tf_op jit(solution)/shard_map/all_to_all | solution.py:323
  77.1 0.0 copy-done.3
  77.1 0.0 copy-done.4
  77.1 0.8 %finish.1 = bf16[16,1024]{1,0:T(8,128)(2,1)} custom-call(f32[16,1024]{1,0:T(8,128)S(1)} %get-tuple-element.15.mixed_ref, f32[4,16,128]{2,1,0:T(8,128)S(1)} %all_to_all.21.part_ref, f32[1,1024]{1,0:T(1,128)S(1)} %bitcast.20, f32[1,1024]{1,0:T(1,128)S(1)} %bitcast.21), custom_call_target="tpu_custom_call" | custom-call | tf_op jit(solution)/shard_map/finish/pallas_call | solution.py:278
  (4 shorter events, 0.1 us)
Async XLA Ops:
  0.0 13.7 %copy-start.7 = (f32[176,1024]{1,0:T(8,128)S(1)}, f32[176,1024]{1,0:T(8,128)}, u32[]{:S(2)}) copy-start(f32[176,1024]{1,0:T(8,128)} %param.18) | copy-start | bytes 2162692
  4.4 17.4 %copy-start.5 = (f32[176]{0:T(256)S(1)}, f32[176]{0:T(256)}, u32[]{:S(2)}) copy-start(f32[176]{0:T(256)} %param.16) | copy-start | bytes 2116
  4.4 17.4 %copy-start.6 = (f32[176]{0:T(256)S(1)}, f32[176]{0:T(256)}, u32[]{:S(2)}) copy-start(f32[176]{0:T(256)} %param.17) | copy-start | bytes 2116
  4.4 17.4 %all-to-all-start = ((bf16[4,96,1024]{2,1,0:T(8,128)(2,1)}), bf16[4,96,1024]{2,1,0:T(8,128)(2,1)S(1)}, u32[]{:S(2)}, u32[]{:S(2)}) async-start(bf16[4,96,1024]{2,1,0:T(8,128)(2,1)} %project.1), calls=%async_computation | async-start | bytes 1572864 | tf_op jit(solution)/shard_map/all_to_all | solution.py:313
  13.8 14.5 %collective-permute-start = (bf16[176,1024]{1,0:T(8,128)(2,1)S(1)}, bf16[176,1024]{1,0:T(8,128)(2,1)S(1)}, u32[]{:S(2)}, u32[]{:S(2)}) collective-permute-start(bf16[176,1024]{1,0:T(8,128)(2,1)S(1)} %convert_element_type.3.own_ref), channel_id=1, source_target_pairs={{0,8},{1,65},{8,0},{9,73},{64,72},{65,1},{72,64},{73,9},{2,10},{3,... | collective-permute-start | bytes 1081352 | tf_op jit(solution)/shard_map/ppermute | solution.py:308
  15.7 12.6 %collective-permute-start.1 = (bf16[176,512]{1,0:T(8,128)(2,1)S(1)}, bf16[176,512]{1,0:T(8,128)(2,1)S(1)}, u32[]{:S(2)}, u32[]{:S(2)}) collective-permute-start(bf16[176,512]{1,0:T(8,128)(2,1)S(1)} %constant_dynamic-slice_fusion), channel_id=1, source_target_pairs={{0,72},{8,64},{64,8},{72,0},{1,73},{9,65},{65,9},{73,1},{2,74},{10... | collective-permute-start | bytes 540680 | tf_op jit(solution)/shard_map/ppermute | solution.py:310
  23.3 12.7 %all-to-all-start.1 = ((bf16[16,48,256]{2,1,0:T(8,128)(2,1)}), bf16[16,48,256]{2,1,0:T(8,128)(2,1)S(1)}, u32[]{:S(2)}, u32[]{:S(2)}) async-start(bf16[16,48,256]{2,1,0:T(8,128)(2,1)} %bitcast.7), calls=%async_computation.1 | async-start | bytes 786432 | tf_op jit(solution)/shard_map/all_to_all | solution.py:317
  28.3 40.6 %copy-start = (f32[1024]{0:T(1024)S(1)}, f32[1024]{0:T(1024)}, u32[]{:S(2)}) copy-start(f32[1024]{0:T(1024)} %param.12) | copy-start | bytes 12292
  28.3 40.5 %copy-start.1 = (f32[1024]{0:T(1024)S(1)}, f32[1024]{0:T(1024)}, u32[]{:S(2)}) copy-start(f32[1024]{0:T(1024)} %param.13) | copy-start | bytes 12292
  28.3 40.5 %copy-start.2 = (f32[1024]{0:T(1024)S(1)}, f32[1024]{0:T(1024)}, u32[]{:S(2)}) copy-start(f32[1024]{0:T(1024)} %param.19) | copy-start | bytes 12292
  28.4 48.7 %copy-start.3 = (f32[1024]{0:T(1024)S(1)}, f32[1024]{0:T(1024)}, u32[]{:S(2)}) copy-start(f32[1024]{0:T(1024)} %param.20) | copy-start | bytes 12292
  28.4 48.7 %copy-start.4 = (f32[1024]{0:T(1024)S(1)}, f32[1024]{0:T(1024)}, u32[]{:S(2)}) copy-start(f32[1024]{0:T(1024)} %param.21) | copy-start | bytes 12292
  28.4 3.8 %collective-permute-start.2 = (bf16[176,1536]{1,0:T(8,128)(2,1)S(1)}, bf16[176,1536]{1,0:T(8,128)(2,1)S(1)}, u32[]{:S(2)}, u32[]{:S(2)}) collective-permute-start(bf16[176,1536]{1,0:T(8,128)(2,1)S(1)} %constant_dynamic-update-slice_fusion.fetched_ref), channel_id=1, source_target_pairs={{0,1},{1,0},{2,3},{3,2},{4,5},{5,4},{6,7},{7,6},{8,9},{9,8},{10,11... | collective-permute-start | bytes 1622024 | tf_op jit(solution)/shard_map/ppermute | solution.py:319

commit v7 on v6

--- a/solution.py
+++ b/solution.py
@@ -200,7 +200,7 @@
     )(*[near(a) for a in (received, gate_scale, up_scale)])
 
 
-def down_kernel(h_ref, own_ref, fetched_ref, other_ref, out_ref):
+def down_kernel(h_ref, own_ref, beside_ref, other_ref, across_ref, out_ref):
     me = lax.axis_index("zl") * 2 + lax.axis_index("yl")
     core = lax.axis_index("dp")
 
@@ -212,12 +212,9 @@
         return dot(h_ref[member], place, 0, 1).astype(BF16)
 
     acc = dot(squeezed(me), own_ref[...], 1, 0)
-    acc = acc + dot(squeezed(me ^ (1 + core)), fetched_ref[:, 0:COLS], 1, 0)
-    acc = acc + dot(squeezed(me ^ (2 - core)), other_ref[:, 0:COLS], 1, 0)
-    h = squeezed(me ^ 3)
-    mine = dot(h, fetched_ref[:, COLS:], 1, 0)
-    theirs = dot(h, other_ref[:, COLS:], 1, 0)
-    acc = acc + jnp.concatenate([jnp.where(core == 0, mine, theirs), jnp.where(core == 0, theirs, mine)], axis=1)
+    acc = acc + dot(squeezed(me ^ (1 + core)), beside_ref[...], 1, 0)
+    acc = acc + dot(squeezed(me ^ (2 - core)), other_ref[...], 1, 0)
+    acc = acc + dot(squeezed(me ^ 3), across_ref[...], 1, 0)
     out_ref[...] = acc.astype(BF16)
 
 
@@ -225,7 +222,7 @@
     vm = pl.BlockSpec(memory_space=pltpu.VMEM)
     return pl.pallas_call(
         down_kernel,
-        in_specs=[vm] * 4,
+        in_specs=[vm] * 5,
         out_specs=vm,
         out_shape=pltpu.VMEM((CHUNK, COLS), BF16),
         name="down",
@@ -306,8 +303,8 @@
 
     w0 = down_weight.astype(BF16)
     beside = lax.ppermute(w0, ("zl", "yl", "dp"), [(i, i ^ (4 if i & 1 else 2)) for i in range(8)])
-    half = lax.dynamic_slice_in_dim(w0, lax.axis_index("dp") * (COLS // 2), COLS // 2, 1)
-    across = lax.ppermute(half, ("zl", "yl"), swapped(4, 3))
+    across = lax.ppermute(w0, ("zl", "yl"), swapped(4, 3))
+    other = lax.ppermute(beside, "dp", swapped(2, 1))
 
     shares = project(tokens, gate_weight.T, up_weight.T, gain, bias)
     received = lax.all_to_all(shares, "cb", 0, 0, tiled=True)
@@ -315,9 +312,7 @@
     own = lax.dynamic_slice_in_dim(tokens, lax.axis_index(RA) * 16, 16, 0)
     sent, own = lax.optimization_barrier((sent, own))
     hidden = lax.all_to_all(sent.reshape(16, SLOT, CHUNK), ("zl", "yl", "cb"), 0, 0, tiled=True)
-    fetched = jnp.concatenate([beside, across], axis=1)
-    other = lax.ppermute(fetched, "dp", swapped(2, 1))
-    partial = down(hidden.reshape(4, 4 * SLOT, CHUNK), (w0, fetched, other))
+    partial = down(hidden.reshape(4, 4 * SLOT, CHUNK), (w0, beside, other, across))
     pieces = lax.all_to_all(partial.reshape(16, 16, COLS), ("Z", "Y"), 0, 0, tiled=True)
     mixed, part = mix(pieces, own, stats, gain, bias, down_scale.reshape(1, COLS))
     parts = lax.all_to_all(part, "cb", 0, 0, tiled=True)

time: 78.4 us -> 90.7 us (1.16)
  the two profiles are of different devices: /device:TPU:2 before, /device:TPU:8 now
where the time goes in v7:
time: 90.7 us; the launch traced here: 90.2 us
  blocking collectives  41.6 us (46%)
  waiting for transfers between devices  20.8 us (23%)
  starting transfers between devices  18.8 us (21%)
  Pallas kernels  8.02 us (9%)
    all_to_all x1, blocking collectives, local(): lax.all_to_all(partial.reshape(16, 16, COLS), ('Z', 'Y'), 0, 0, tiled=True)  32.1 us
    all_to_all x1, waiting for transfers between devices, local(): received = lax.all_to_all(shares, 'cb', 0, 0, tiled=True)  11.5 us
    all_to_all x1, blocking collectives, local(): parts = lax.all_to_all(part, 'cb', 0, 0, tiled=True)  9.52 us
    ppermute x1, waiting for transfers between devices, local(): lax.ppermute(w0, ('zl', 'yl', 'dp'), [(i, i ^ (4 if i & 1 else 2)) for i...  6.15 us
    all_to_all x1, starting transfers between devices, local(): lax.all_to_all(sent.reshape(16, SLOT, CHUNK), ('zl', 'yl', 'cb'), 0, 0, t...  5.71 us
    ppermute x1, starting transfers between devices, local(): across = lax.ppermute(w0, ('zl', 'yl'), swapped(4, 3))  4.73 us
    all_to_all x1, starting transfers between devices, local(): received = lax.all_to_all(shares, 'cb', 0, 0, tiled=True)  4.43 us
    pallas_call x1, Pallas kernels, project(): pl.pallas_call(project_kernel, in_specs=[hbm] * 5, out_specs=hbm, out_sha...  4.31 us
  transfers between devices with their start and end apart: 5, of which 3 were waited for; matrix products, arithmetic and copies ran while one was open for 1% of the time, Pallas kernels for 0%

profile of v7, /device:TPU:8, one launch (start us, length us, event | category | flops | bytes accessed | tf_op | source)
XLA Modules:
  0.0 90.2 jit_solution(2727012675292638143)
XLA Ops:
  0.0 0.0 copy-start.5
  0.0 0.0 copy-start.6
  0.0 4.3 %project.1 = bf16[4,96,1024]{2,1,0:T(8,128)(2,1)} custom-call(bf16[4,2,4,2,16,1024]{5,4,3,2,1,0:T(8,128)(2,1)} %bitcast.24, f32[176,1024]{1,0:T(8,128)} %bitcast.25, f32[176,1024]{1,0:T(8,128)} %bitcast.26, f32[1,1024]{1,0:T(1,128)} %bitcast.15, f32[1,1024]{1,0:T(1,128)} %bitcast.17), custom_call_target="tpu_custom_call" | custom-call | tf_op jit(solution)/shard_map/project/pallas_call | solution.py:118
  4.3 0.0 copy-start.7
  4.3 4.4 %all-to-all-start = ((bf16[4,96,1024]{2,1,0:T(8,128)(2,1)}), bf16[4,96,1024]{2,1,0:T(8,128)(2,1)S(1)}, u32[]{:S(2)}, u32[]{:S(2)}) async-start(bf16[4,96,1024]{2,1,0:T(8,128)(2,1)} %project.1), calls=%async_computation | async-start | bytes 1572864 | tf_op jit(solution)/shard_map/all_to_all | solution.py:310
  8.8 0.8 constant_dynamic-slice_fusion.x_ref
  9.5 11.5 %all-to-all-done.r_ref = bf16[4,96,1024]{2,1,0:T(8,128)(2,1)S(1)} async-done(((bf16[4,96,1024]{2,1,0:T(8,128)(2,1)}), bf16[4,96,1024]{2,1,0:T(8,128)(2,1)S(1)}, u32[]{:S(2)}, u32[]{:S(2)}) %all-to-all-start) | async-done | bytes 786464 | tf_op jit(solution)/shard_map/all_to_all | solution.py:310
  21.1 0.0 copy-done.5
  21.1 0.0 copy-done.6
  21.1 1.5 %hidden.1 = (bf16[4,4,48,256]{3,2,1,0:T(8,128)(2,1)}, f32[8,1024]{1,0:T(8,128)S(1)}) custom-call(bf16[4,96,1024]{2,1,0:T(8,128)(2,1)S(1)} %all-to-all-done.r_ref, f32[1,176]{1,0:T(1,128)S(1)} %bitcast.22, f32[1,176]{1,0:T(1,128)S(1)} %bitcast.23), custom_call_target="tpu_custom_call" | custom-call | tf_op jit(solution)/shard_map/hidden/pallas_call | solution.py:194
  22.6 5.7 %all-to-all-start.1 = ((bf16[16,48,256]{2,1,0:T(8,128)(2,1)}), bf16[16,48,256]{2,1,0:T(8,128)(2,1)S(1)}, u32[]{:S(2)}, u32[]{:S(2)}) async-start(bf16[16,48,256]{2,1,0:T(8,128)(2,1)} %bitcast.7), calls=%async_computation.1 | async-start | bytes 786432 | tf_op jit(solution)/shard_map/all_to_all | solution.py:314
  28.3 0.0 copy-done.7
  28.3 0.0 copy-start
  28.3 0.0 copy-start.1
  28.3 0.0 copy-start.2
  28.4 0.0 copy-start.3
  28.4 0.0 copy-start.4
  28.4 2.0 %collective-permute-start = (bf16[176,1024]{1,0:T(8,128)(2,1)S(1)}, bf16[176,1024]{1,0:T(8,128)(2,1)S(1)}, u32[]{:S(2)}, u32[]{:S(2)}) collective-permute-start(bf16[176,1024]{1,0:T(8,128)(2,1)S(1)} %convert_element_type.3.own_ref), channel_id=1, source_target_pairs={{0,8},{1,65},{8,0},{9,73},{64,72},{65,1},{72,64},{73,9},{2,10},{3,... | collective-permute-start | bytes 1081352 | tf_op jit(solution)/shard_map/ppermute | solution.py:305
  30.4 4.7 %collective-permute-start.2 = (bf16[176,1024]{1,0:T(8,128)(2,1)S(1)}, bf16[176,1024]{1,0:T(8,128)(2,1)S(1)}, u32[]{:S(2)}, u32[]{:S(2)}) collective-permute-start(bf16[176,1024]{1,0:T(8,128)(2,1)S(1)} %convert_element_type.3.own_ref), channel_id=1, source_target_pairs={{0,72},{8,64},{64,8},{72,0},{1,73},{9,65},{65,9},{73,1},{2,74},{10... | collective-permute-start | bytes 1081352 | tf_op jit(solution)/shard_map/ppermute | solution.py:306
  35.1 6.2 %collective-permute-done.beside_ref = bf16[176,1024]{1,0:T(8,128)(2,1)S(1)} collective-permute-done((bf16[176,1024]{1,0:T(8,128)(2,1)S(1)}, bf16[176,1024]{1,0:T(8,128)(2,1)S(1)}, u32[]{:S(2)}, u32[]{:S(2)}) %collective-permute-start) | collective-permute-done | bytes 360480 | tf_op jit(solution)/shard_map/ppermute | solution.py:305
  41.3 1.9 %collective-permute-start.1 = (bf16[176,1024]{1,0:T(8,128)(2,1)S(1)}, bf16[176,1024]{1,0:T(8,128)(2,1)S(1)}, u32[]{:S(2)}, u32[]{:S(2)}) collective-permute-start(bf16[176,1024]{1,0:T(8,128)(2,1)S(1)} %collective-permute-done.beside_ref), channel_id=1, source_target_pairs={{0,1},{1,0},{2,3},{3,2},{4,5},{5,4},{6,7},{7,6},{8,9},{9,8},{10,11... | collective-permute-start | bytes 1081352 | tf_op jit(solution)/shard_map/ppermute | solution.py:307
  43.2 3.1 %collective-permute-done.2.across_ref = bf16[176,1024]{1,0:T(8,128)(2,1)S(1)} collective-permute-done((bf16[176,1024]{1,0:T(8,128)(2,1)S(1)}, bf16[176,1024]{1,0:T(8,128)(2,1)S(1)}, u32[]{:S(2)}, u32[]{:S(2)}) %collective-permute-start.2) | collective-permute-done | bytes 360480 | tf_op jit(solution)/shard_map/ppermute | solution.py:306
  46.3 0.0 collective-permute-done.1.other_ref
  46.3 0.0 all-to-all-done.1
  46.3 1.2 %down.1 = bf16[256,1024]{1,0:T(8,128)(2,1)S(1)} custom-call(bf16[4,192,256]{2,1,0:T(8,128)(2,1)S(1)} %bitcast.14, bf16[176,1024]{1,0:T(8,128)(2,1)S(1)} %convert_element_type.3.own_ref, bf16[176,1024]{1,0:T(8,128)(2,1)S(1)} %collective-permute-done.beside_ref, bf16[176,1024]{1,0:T(8,128)(2,1)S(1)} %collective-permute-done.1.other_ref, ...), custom_call_target="tpu_custom_call" | custom-call | tf_op jit(solution)/shard_map/down/pallas_call | solution.py:223
  47.5 32.1 %all_to_all.20.r_ref = bf16[16,16,1024]{2,1,0:T(8,128)(2,1)S(1)} all-to-all(bf16[16,16,1024]{2,1,0:T(8,128)(2,1)S(1)} %bitcast.13), channel_id=1, replica_groups=mesh['Z'=4,'zl'=2,'Y'=4,'yl'=2,'cb'=4,'dp'=2] {'Z','Y'}, dimensions={0} | all-to-all | bytes 1048576 | tf_op jit(solution)/shard_map/all_to_all | solution.py:316
  79.6 0.0 copy-done
  79.6 0.0 copy-done.1
  79.6 0.0 copy-done.2
  79.6 0.3 mix.1
  79.9 9.5 %all_to_all.21.part_ref = f32[4,16,128]{2,1,0:T(8,128)S(1)} all-to-all(f32[4,16,128]{2,1,0:T(8,128)S(1)} %get-tuple-element.16), channel_id=1, replica_groups=mesh['Z'=4,'zl'=2,'Y'=4,'yl'=2,'cb'=4,'dp'=2] {'cb'}, dimensions={0} | all-to-all | bytes 65536 | tf_op jit(solution)/shard_map/all_to_all | solution.py:318
  89.4 0.0 copy-done.3
  89.4 0.0 copy-done.4
  89.4 0.8 finish.1
  (1 shorter events, 0.0 us)
Async XLA Ops:
  0.0 21.1 %copy-start.5 = (f32[176]{0:T(256)S(1)}, f32[176]{0:T(256)}, u32[]{:S(2)}) copy-start(f32[176]{0:T(256)} %param.16) | copy-start | bytes 2116
  0.0 21.1 %copy-start.6 = (f32[176]{0:T(256)S(1)}, f32[176]{0:T(256)}, u32[]{:S(2)}) copy-start(f32[176]{0:T(256)} %param.17) | copy-start | bytes 2116
  4.3 23.9 %copy-start.7 = (f32[176,1024]{1,0:T(8,128)S(1)}, f32[176,1024]{1,0:T(8,128)}, u32[]{:S(2)}) copy-start(f32[176,1024]{1,0:T(8,128)} %param.18) | copy-start | bytes 2162692
  4.3 16.7 %all-to-all-start = ((bf16[4,96,1024]{2,1,0:T(8,128)(2,1)}), bf16[4,96,1024]{2,1,0:T(8,128)(2,1)S(1)}, u32[]{:S(2)}, u32[]{:S(2)}) async-start(bf16[4,96,1024]{2,1,0:T(8,128)(2,1)} %project.1), calls=%async_computation | async-start | bytes 1572864 | tf_op jit(solution)/shard_map/all_to_all | solution.py:310
  22.6 23.8 %all-to-all-start.1 = ((bf16[16,48,256]{2,1,0:T(8,128)(2,1)}), bf16[16,48,256]{2,1,0:T(8,128)(2,1)S(1)}, u32[]{:S(2)}, u32[]{:S(2)}) async-start(bf16[16,48,256]{2,1,0:T(8,128)(2,1)} %bitcast.7), calls=%async_computation.1 | async-start | bytes 786432 | tf_op jit(solution)/shard_map/all_to_all | solution.py:314
  28.3 51.3 %copy-start = (f32[1024]{0:T(1024)S(1)}, f32[1024]{0:T(1024)}, u32[]{:S(2)}) copy-start(f32[1024]{0:T(1024)} %param.12) | copy-start | bytes 12292
  28.3 51.3 %copy-start.1 = (f32[1024]{0:T(1024)S(1)}, f32[1024]{0:T(1024)}, u32[]{:S(2)}) copy-start(f32[1024]{0:T(1024)} %param.13) | copy-start | bytes 12292
  28.3 51.3 %copy-start.2 = (f32[1024]{0:T(1024)S(1)}, f32[1024]{0:T(1024)}, u32[]{:S(2)}) copy-start(f32[1024]{0:T(1024)} %param.19) | copy-start | bytes 12292
  28.4 61.0 %copy-start.3 = (f32[1024]{0:T(1024)S(1)}, f32[1024]{0:T(1024)}, u32[]{:S(2)}) copy-start(f32[1024]{0:T(1024)} %param.20) | copy-start | bytes 12292
  28.4 61.0 %copy-start.4 = (f32[1024]{0:T(1024)S(1)}, f32[1024]{0:T(1024)}, u32[]{:S(2)}) copy-start(f32[1024]{0:T(1024)} %param.21) | copy-start | bytes 12292
  28.4 12.9 %collective-permute-start = (bf16[176,1024]{1,0:T(8,128)(2,1)S(1)}, bf16[176,1024]{1,0:T(8,128)(2,1)S(1)}, u32[]{:S(2)}, u32[]{:S(2)}) collective-permute-start(bf16[176,1024]{1,0:T(8,128)(2,1)S(1)} %convert_element_type.3.own_ref), channel_id=1, source_target_pairs={{0,8},{1,65},{8,0},{9,73},{64,72},{65,1},{72,64},{73,9},{2,10},{3,... | collective-permute-start | bytes 1081352 | tf_op jit(solution)/shard_map/ppermute | solution.py:305
  30.4 15.9 %collective-permute-start.2 = (bf16[176,1024]{1,0:T(8,128)(2,1)S(1)}, bf16[176,1024]{1,0:T(8,128)(2,1)S(1)}, u32[]{:S(2)}, u32[]{:S(2)}) collective-permute-start(bf16[176,1024]{1,0:T(8,128)(2,1)S(1)} %convert_element_type.3.own_ref), channel_id=1, source_target_pairs={{0,72},{8,64},{64,8},{72,0},{1,73},{9,65},{65,9},{73,1},{2,74},{10... | collective-permute-start | bytes 1081352 | tf_op jit(solution)/shard_map/ppermute | solution.py:306
  41.3 5.0 %collective-permute-start.1 = (bf16[176,1024]{1,0:T(8,128)(2,1)S(1)}, bf16[176,1024]{1,0:T(8,128)(2,1)S(1)}, u32[]{:S(2)}, u32[]{:S(2)}) collective-permute-start(bf16[176,1024]{1,0:T(8,128)(2,1)S(1)} %collective-permute-done.beside_ref), channel_id=1, source_target_pairs={{0,1},{1,0},{2,3},{3,2},{4,5},{5,4},{6,7},{7,6},{8,9},{9,8},{10,11... | collective-permute-start | bytes 1081352 | tf_op jit(solution)/shard_map/ppermute | solution.py:307

commit v8 on v6

--- a/solution.py
+++ b/solution.py
@@ -48,12 +48,16 @@
         pltpu.make_async_copy(gain_ref, gb_buf.at[0], sems.at[2]),
         pltpu.make_async_copy(bias_ref, gb_buf.at[1], sems.at[3]),
     ]
-    tokens = [pltpu.make_async_copy(x_ref.at[:, j // 2, :, j % 2], x_buf.at[j], sems.at[4 + j]) for j in range(4)]
-    for copy in loads + tokens[:PER]:
+    tokens = [
+        pltpu.make_async_copy(x_ref.at[z, (j // 2) ^ flipped(z), :, j % 2], x_buf.at[j, z], sems.at[4 + 4 * j + z])
+        for j in range(4)
+        for z in range(4)
+    ]
+    for copy in loads + tokens[: 4 * PER]:
         copy.start()
     for copy in loads:
         copy.wait()
-    for copy in tokens[PER:]:
+    for copy in tokens[4 * PER :]:
         copy.start()
 
     gain = gb_buf[0]
@@ -82,7 +86,7 @@
     stores = []
     for j in range(4 // PER):
         at = slice(TILE * j, TILE * (j + 1))
-        for copy in tokens[PER * j : PER * (j + 1)]:
+        for copy in tokens[4 * PER * j : 4 * PER * (j + 1)]:
             copy.wait()
         part = dot(w_ref[...], x_buf[PER * j : PER * (j + 1)].reshape(TILE, COLS), 1, 1)
         x = x_buf[PER * j : PER * (j + 1)].reshape(TILE, COLS).astype(F32)
@@ -107,7 +111,7 @@
         for k in range(4):
             rows = slice(PART * k, PART * (k + 1))
             out_buf[k, :, at] = (part[rows] - col[rows] * m_row + extra).astype(BF16)
-        stores.append(pltpu.make_async_copy(out_buf.at[:, :, at], out_ref.at[:, :, at], sems.at[8 + j]))
+        stores.append(pltpu.make_async_copy(out_buf.at[:, :, at], out_ref.at[:, :, at], sems.at[20 + j]))
         stores[-1].start()
     for copy in stores:
         copy.wait()
@@ -128,7 +132,7 @@
             pltpu.VMEM((4, PART, ROWS), BF16),
             pltpu.VMEM((4 * PART, COLS), BF16),
             pltpu.VMEM((8, ROWS), F32),
-            pltpu.SemaphoreType.DMA((12,)),
+            pltpu.SemaphoreType.DMA((24,)),
         ],
         name="project",
     )(*[pltpu.with_memory_space_constraint(a, pltpu.HBM) for a in (tokens.reshape(4, 2, 4, 2, 16, COLS), gate_t, up_t, gain, bias)])
@@ -176,6 +180,7 @@
     scale = jnp.where(iota((PART, 1), 0) < SLOT, sc[:, 0:1] + sc[:, 1:2] + sc[:, 2:3], sc[:, 3:4] + sc[:, 4:5] + sc[:, 5:6])
 
     keep = iota((SLOT, CHUNK), 0) < UNITS
+    turn = 2 * flipped(lax.axis_index("Z"))
     for j in range(4):
         at = slice(CHUNK * j, CHUNK * (j + 1))
         acc = jnp.zeros((PART, CHUNK), F32)
@@ -186,7 +191,7 @@
         up = y[SLOT:PART]
         h = jnp.where(keep, gate / (1.0 + jnp.exp(-gate)) * up, 0.0).astype(BF16)
         for k in range(4):
-            out_ref[j, k] = h
+            out_ref[j ^ turn, k] = h
 
 
 def hidden_of(received, gate_scale, up_scale):
@@ -233,7 +238,7 @@
 
 
 def mix_kernel(r_ref, x_ref, stat_ref, gain_ref, bias_ref, scale_ref, mixed_ref, part_ref):
-    member = lax.axis_index("zl") * 2 + lax.axis_index("yl")
+    member = (lax.axis_index("zl") ^ flipped(lax.axis_index("Z"))) * 2 + lax.axis_index("yl")
     at = member * CHUNK + (lax.axis_index("Z") * 4 + lax.axis_index("Y")) * 16
     branch = jnp.zeros((16, COLS), F32)
     for k in range(16):
@@ -284,6 +289,18 @@
     )(*[near(a) for a in (mixed, parts, gain, bias)])
 
 
+def flipped(z):
+    return (z ^ (z >> 1)) & 1
+
+
+def spread_groups():
+    return [
+        [(2 * z + (jz ^ flipped(z))) * 8 + 2 * y + jy for z in range(4) for y in range(4)]
+        for jz in range(2)
+        for jy in range(2)
+    ]
+
+
 def swapped(n, k):
     return [(i, i ^ k) for i in range(n)]
 
@@ -318,7 +335,9 @@
     fetched = jnp.concatenate([beside, across], axis=1)
     other = lax.ppermute(fetched, "dp", swapped(2, 1))
     partial = down(hidden.reshape(4, 4 * SLOT, CHUNK), (w0, fetched, other))
-    pieces = lax.all_to_all(partial.reshape(16, 16, COLS), ("Z", "Y"), 0, 0, tiled=True)
+    pieces = lax.all_to_all(
+        partial.reshape(16, 16, COLS), RA, 0, 0, axis_index_groups=spread_groups(), tiled=True
+    )
     mixed, part = mix(pieces, own, stats, gain, bias, down_scale.reshape(1, COLS))
     parts = lax.all_to_all(part, "cb", 0, 0, tiled=True)
     return finish(mixed, parts, out_gain.reshape(1, COLS), out_bias.reshape(1, COLS))

time: 78.4 us -> 78.2 us (level)
  the two profiles are of different devices: /device:TPU:2 before, /device:TPU:8 now
where the time goes in v8:
time: 78.2 us; the launch traced here: 77.7 us
  blocking collectives  39.9 us (51%)
  starting transfers between devices  20.8 us (27%)
  Pallas kernels  8.19 us (10%)
  waiting for transfers between devices  7.71 us (10%)
  local copies, waits for them, and re-layouts  0.87 us (1%)
    all_to_all x1, blocking collectives, local(): lax.all_to_all(partial.reshape(16, 16, COLS), RA, 0, 0, axis_index_groups...  29.3 us
    all_to_all x1, blocking collectives, local(): parts = lax.all_to_all(part, 'cb', 0, 0, tiled=True)  10.7 us
    ppermute x1, starting transfers between devices, local(): lax.ppermute(w0, ('zl', 'yl', 'dp'), [(i, i ^ (4 if i & 1 else 2)) for i...  6.92 us
    all_to_all x1, starting transfers between devices, local(): lax.all_to_all(sent.reshape(16, SLOT, CHUNK), ('zl', 'yl', 'cb'), 0, 0, t...  5.73 us
    pallas_call x1, Pallas kernels, project(): pl.pallas_call(project_kernel, in_specs=[hbm] * 5, out_specs=hbm, out_sha...  4.44 us
    all_to_all x1, starting transfers between devices, local(): received = lax.all_to_all(shares, 'cb', 0, 0, tiled=True)  4.31 us
    all_to_all x1, waiting for transfers between devices, local(): lax.all_to_all(sent.reshape(16, SLOT, CHUNK), ('zl', 'yl', 'cb'), 0, 0, t...  3.23 us
    all_to_all x1, waiting for transfers between devices, local(): received = lax.all_to_all(shares, 'cb', 0, 0, tiled=True)  2.57 us
  transfers between devices with their start and end apart: 5, of which 3 were waited for; matrix products, arithmetic and copies ran while one was open for 1% of the time, Pallas kernels for 2%

profile of v8, /device:TPU:8, one launch (start us, length us, event | category | flops | bytes accessed | tf_op | source)
XLA Modules:
  0.0 77.7 jit_solution(6035112352450136860)
XLA Ops:
  0.0 0.0 copy-start.7
  0.0 4.4 %project.1 = bf16[4,96,1024]{2,1,0:T(8,128)(2,1)} custom-call(bf16[4,2,4,2,16,1024]{5,4,3,2,1,0:T(8,128)(2,1)} %bitcast.24, f32[176,1024]{1,0:T(8,128)} %bitcast.25, f32[176,1024]{1,0:T(8,128)} %bitcast.26, f32[1,1024]{1,0:T(1,128)} %bitcast.15, f32[1,1024]{1,0:T(1,128)} %bitcast.17), custom_call_target="tpu_custom_call" | custom-call | tf_op jit(solution)/shard_map/project/pallas_call | solution.py:122
  4.4 0.0 copy-start.5
  4.5 0.0 copy-start.6
  4.5 4.3 %all-to-all-start = ((bf16[4,96,1024]{2,1,0:T(8,128)(2,1)}), bf16[4,96,1024]{2,1,0:T(8,128)(2,1)S(1)}, u32[]{:S(2)}, u32[]{:S(2)}) async-start(bf16[4,96,1024]{2,1,0:T(8,128)(2,1)} %project.1), calls=%async_computation | async-start | bytes 1572864 | tf_op jit(solution)/shard_map/all_to_all | solution.py:330
  8.8 0.0 copy-done.7
  8.8 6.9 %collective-permute-start = (bf16[176,1024]{1,0:T(8,128)(2,1)S(1)}, bf16[176,1024]{1,0:T(8,128)(2,1)S(1)}, u32[]{:S(2)}, u32[]{:S(2)}) collective-permute-start(bf16[176,1024]{1,0:T(8,128)(2,1)S(1)} %convert_element_type.3.own_ref), channel_id=1, source_target_pairs={{0,8},{1,65},{8,0},{9,73},{64,72},{65,1},{72,64},{73,9},{2,10},{3,... | collective-permute-start | bytes 1081352 | tf_op jit(solution)/shard_map/ppermute | solution.py:325
  15.8 1.9 %collective-permute-start.1 = (bf16[176,512]{1,0:T(8,128)(2,1)S(1)}, bf16[176,512]{1,0:T(8,128)(2,1)S(1)}, u32[]{:S(2)}, u32[]{:S(2)}) collective-permute-start(bf16[176,512]{1,0:T(8,128)(2,1)S(1)} %constant_dynamic-slice_fusion), channel_id=1, source_target_pairs={{0,72},{8,64},{64,8},{72,0},{1,73},{9,65},{65,9},{73,1},{2,74},{10... | collective-permute-start | bytes 540680 | tf_op jit(solution)/shard_map/ppermute | solution.py:327
  17.7 0.8 constant_dynamic-slice_fusion.1.x_ref
  18.5 2.6 %all-to-all-done.r_ref = bf16[4,96,1024]{2,1,0:T(8,128)(2,1)S(1)} async-done(((bf16[4,96,1024]{2,1,0:T(8,128)(2,1)}), bf16[4,96,1024]{2,1,0:T(8,128)(2,1)S(1)}, u32[]{:S(2)}, u32[]{:S(2)}) %all-to-all-start) | async-done | bytes 786464 | tf_op jit(solution)/shard_map/all_to_all | solution.py:330
  21.1 0.0 copy-done.5
  21.1 0.0 copy-done.6
  21.1 1.5 %hidden.1 = (bf16[4,4,48,256]{3,2,1,0:T(8,128)(2,1)}, f32[8,1024]{1,0:T(8,128)S(1)}) custom-call(bf16[4,96,1024]{2,1,0:T(8,128)(2,1)S(1)} %all-to-all-done.r_ref, f32[1,176]{1,0:T(1,128)S(1)} %bitcast.22, f32[1,176]{1,0:T(1,128)S(1)} %bitcast.23), custom_call_target="tpu_custom_call" | custom-call | tf_op jit(solution)/shard_map/hidden/pallas_call | solution.py:199
  22.6 5.7 %all-to-all-start.1 = ((bf16[16,48,256]{2,1,0:T(8,128)(2,1)}), bf16[16,48,256]{2,1,0:T(8,128)(2,1)S(1)}, u32[]{:S(2)}, u32[]{:S(2)}) async-start(bf16[16,48,256]{2,1,0:T(8,128)(2,1)} %bitcast.7), calls=%async_computation.1 | async-start | bytes 786432 | tf_op jit(solution)/shard_map/all_to_all | solution.py:334
  28.3 0.0 copy-start
  28.3 0.0 copy-start.1
  28.3 0.0 copy-start.2
  28.3 0.0 collective-permute-done
  28.4 0.0 collective-permute-done.1
  28.4 0.0 copy-start.3
  28.4 0.0 copy-start.4
  28.4 1.9 %collective-permute-start.2 = (bf16[176,1536]{1,0:T(8,128)(2,1)S(1)}, bf16[176,1536]{1,0:T(8,128)(2,1)S(1)}, u32[]{:S(2)}, u32[]{:S(2)}) collective-permute-start(bf16[176,1536]{1,0:T(8,128)(2,1)S(1)} %constant_dynamic-update-slice_fusion.fetched_ref), channel_id=1, source_target_pairs={{0,1},{1,0},{2,3},{3,2},{4,5},{5,4},{6,7},{7,6},{8,9},{9,8},{10,11... | collective-permute-start | bytes 1622024 | tf_op jit(solution)/shard_map/ppermute | solution.py:336
  30.4 1.9 %collective-permute-done.2.other_ref = bf16[176,1536]{1,0:T(8,128)(2,1)S(1)} collective-permute-done((bf16[176,1536]{1,0:T(8,128)(2,1)S(1)}, bf16[176,1536]{1,0:T(8,128)(2,1)S(1)}, u32[]{:S(2)}, u32[]{:S(2)}) %collective-permute-start.2) | collective-permute-done | bytes 540704 | tf_op jit(solution)/shard_map/ppermute | solution.py:336
  32.3 3.2 %all-to-all-done.1 = bf16[16,48,256]{2,1,0:T(8,128)(2,1)S(1)} async-done(((bf16[16,48,256]{2,1,0:T(8,128)(2,1)}), bf16[16,48,256]{2,1,0:T(8,128)(2,1)S(1)}, u32[]{:S(2)}, u32[]{:S(2)}) %all-to-all-start.1) | async-done | bytes 393248 | tf_op jit(solution)/shard_map/all_to_all | solution.py:334
  35.5 1.2 %down.1 = bf16[256,1024]{1,0:T(8,128)(2,1)S(1)} custom-call(bf16[4,192,256]{2,1,0:T(8,128)(2,1)S(1)} %bitcast.14, bf16[176,1024]{1,0:T(8,128)(2,1)S(1)} %convert_element_type.3.own_ref, bf16[176,1536]{1,0:T(8,128)(2,1)S(1)} %constant_dynamic-update-slice_fusion.fetched_ref, bf16[176,1536]{1,0:T(8,128)(2,1)S(1)} %collective-permute-done.2.other_ref), custom_call_target="tpu_custom_call" | custom-call | tf_op jit(solution)/shard_map/down/pallas_call | solution.py:231
  36.7 29.3 %all_to_all.20.r_ref = bf16[16,16,1024]{2,1,0:T(8,128)(2,1)S(1)} all-to-all(bf16[16,16,1024]{2,1,0:T(8,128)(2,1)S(1)} %bitcast.13), channel_id=1, replica_groups={{0,16,32,48,192,208,224,240,320,336,352,368,384,400,416,432},{8,24,40,5..., dimensions={0} | all-to-all | bytes 1048576 | tf_op jit(solution)/shard_map/all_to_all | solution.py:338
  66.0 0.0 copy-done
  66.0 0.0 copy-done.1
  66.0 0.0 copy-done.2
  66.0 0.3 mix.1
  66.3 10.7 %all_to_all.21.part_ref = f32[4,16,128]{2,1,0:T(8,128)S(1)} all-to-all(f32[4,16,128]{2,1,0:T(8,128)S(1)} %get-tuple-element.16), channel_id=1, replica_groups=mesh['Z'=4,'zl'=2,'Y'=4,'yl'=2,'cb'=4,'dp'=2] {'cb'}, dimensions={0} | all-to-all | bytes 65536 | tf_op jit(solution)/shard_map/all_to_all | solution.py:342
  76.9 0.0 copy-done.3
  76.9 0.0 copy-done.4
  76.9 0.8 %finish.1 = bf16[16,1024]{1,0:T(8,128)(2,1)} custom-call(f32[16,1024]{1,0:T(8,128)S(1)} %get-tuple-element.15.mixed_ref, f32[4,16,128]{2,1,0:T(8,128)S(1)} %all_to_all.21.part_ref, f32[1,1024]{1,0:T(1,128)S(1)} %bitcast.20, f32[1,1024]{1,0:T(1,128)S(1)} %bitcast.21), custom_call_target="tpu_custom_call" | custom-call | tf_op jit(solution)/shard_map/finish/pallas_call | solution.py:283
  (4 shorter events, 0.1 us)
Async XLA Ops:
  0.0 8.8 %copy-start.7 = (f32[176,1024]{1,0:T(8,128)S(1)}, f32[176,1024]{1,0:T(8,128)}, u32[]{:S(2)}) copy-start(f32[176,1024]{1,0:T(8,128)} %param.18) | copy-start | bytes 2162692
  4.4 16.6 %copy-start.5 = (f32[176]{0:T(256)S(1)}, f32[176]{0:T(256)}, u32[]{:S(2)}) copy-start(f32[176]{0:T(256)} %param.16) | copy-start | bytes 2116
  4.5 16.6 %copy-start.6 = (f32[176]{0:T(256)S(1)}, f32[176]{0:T(256)}, u32[]{:S(2)}) copy-start(f32[176]{0:T(256)} %param.17) | copy-start | bytes 2116
  4.5 16.6 %all-to-all-start = ((bf16[4,96,1024]{2,1,0:T(8,128)(2,1)}), bf16[4,96,1024]{2,1,0:T(8,128)(2,1)S(1)}, u32[]{:S(2)}, u32[]{:S(2)}) async-start(bf16[4,96,1024]{2,1,0:T(8,128)(2,1)} %project.1), calls=%async_computation | async-start | bytes 1572864 | tf_op jit(solution)/shard_map/all_to_all | solution.py:330
  8.8 19.5 %collective-permute-start = (bf16[176,1024]{1,0:T(8,128)(2,1)S(1)}, bf16[176,1024]{1,0:T(8,128)(2,1)S(1)}, u32[]{:S(2)}, u32[]{:S(2)}) collective-permute-start(bf16[176,1024]{1,0:T(8,128)(2,1)S(1)} %convert_element_type.3.own_ref), channel_id=1, source_target_pairs={{0,8},{1,65},{8,0},{9,73},{64,72},{65,1},{72,64},{73,9},{2,10},{3,... | collective-permute-start | bytes 1081352 | tf_op jit(solution)/shard_map/ppermute | solution.py:325
  15.8 12.6 %collective-permute-start.1 = (bf16[176,512]{1,0:T(8,128)(2,1)S(1)}, bf16[176,512]{1,0:T(8,128)(2,1)S(1)}, u32[]{:S(2)}, u32[]{:S(2)}) collective-permute-start(bf16[176,512]{1,0:T(8,128)(2,1)S(1)} %constant_dynamic-slice_fusion), channel_id=1, source_target_pairs={{0,72},{8,64},{64,8},{72,0},{1,73},{9,65},{65,9},{73,1},{2,74},{10... | collective-permute-start | bytes 540680 | tf_op jit(solution)/shard_map/ppermute | solution.py:327
  22.6 12.9 %all-to-all-start.1 = ((bf16[16,48,256]{2,1,0:T(8,128)(2,1)}), bf16[16,48,256]{2,1,0:T(8,128)(2,1)S(1)}, u32[]{:S(2)}, u32[]{:S(2)}) async-start(bf16[16,48,256]{2,1,0:T(8,128)(2,1)} %bitcast.7), calls=%async_computation.1 | async-start | bytes 786432 | tf_op jit(solution)/shard_map/all_to_all | solution.py:334
  28.3 37.7 %copy-start = (f32[1024]{0:T(1024)S(1)}, f32[1024]{0:T(1024)}, u32[]{:S(2)}) copy-start(f32[1024]{0:T(1024)} %param.12) | copy-start | bytes 12292
  28.3 37.7 %copy-start.1 = (f32[1024]{0:T(1024)S(1)}, f32[1024]{0:T(1024)}, u32[]{:S(2)}) copy-start(f32[1024]{0:T(1024)} %param.13) | copy-start | bytes 12292
  28.3 37.7 %copy-start.2 = (f32[1024]{0:T(1024)S(1)}, f32[1024]{0:T(1024)}, u32[]{:S(2)}) copy-start(f32[1024]{0:T(1024)} %param.19) | copy-start | bytes 12292
  28.4 48.5 %copy-start.3 = (f32[1024]{0:T(1024)S(1)}, f32[1024]{0:T(1024)}, u32[]{:S(2)}) copy-start(f32[1024]{0:T(1024)} %param.20) | copy-start | bytes 12292
  28.4 48.5 %copy-start.4 = (f32[1024]{0:T(1024)S(1)}, f32[1024]{0:T(1024)}, u32[]{:S(2)}) copy-start(f32[1024]{0:T(1024)} %param.21) | copy-start | bytes 12292
  28.4 3.8 %collective-permute-start.2 = (bf16[176,1536]{1,0:T(8,128)(2,1)S(1)}, bf16[176,1536]{1,0:T(8,128)(2,1)S(1)}, u32[]{:S(2)}, u32[]{:S(2)}) collective-permute-start(bf16[176,1536]{1,0:T(8,128)(2,1)S(1)} %constant_dynamic-update-slice_fusion.fetched_ref), channel_id=1, source_target_pairs={{0,1},{1,0},{2,3},{3,2},{4,5},{5,4},{6,7},{7,6},{8,9},{9,8},{10,11... | collective-permute-start | bytes 1622024 | tf_op jit(solution)/shard_map/ppermute | solution.py:336

commit v9 on v8

--- a/solution.py
+++ b/solution.py
@@ -48,16 +48,17 @@
         pltpu.make_async_copy(gain_ref, gb_buf.at[0], sems.at[2]),
         pltpu.make_async_copy(bias_ref, gb_buf.at[1], sems.at[3]),
     ]
+    runs = ((0, 1), (1, 3), (3, 4))
     tokens = [
-        pltpu.make_async_copy(x_ref.at[z, (j // 2) ^ flipped(z), :, j % 2], x_buf.at[j, z], sems.at[4 + 4 * j + z])
+        pltpu.make_async_copy(x_ref.at[a:b, (j // 2) ^ flipped(a), :, j % 2], x_buf.at[j, a:b], sems.at[4 + 3 * j + i])
         for j in range(4)
-        for z in range(4)
+        for i, (a, b) in enumerate(runs)
     ]
-    for copy in loads + tokens[: 4 * PER]:
+    for copy in loads + tokens[: 3 * PER]:
         copy.start()
     for copy in loads:
         copy.wait()
-    for copy in tokens[4 * PER :]:
+    for copy in tokens[3 * PER :]:
         copy.start()
 
     gain = gb_buf[0]
@@ -86,7 +87,7 @@
     stores = []
     for j in range(4 // PER):
         at = slice(TILE * j, TILE * (j + 1))
-        for copy in tokens[4 * PER * j : 4 * PER * (j + 1)]:
+        for copy in tokens[3 * PER * j : 3 * PER * (j + 1)]:
             copy.wait()
         part = dot(w_ref[...], x_buf[PER * j : PER * (j + 1)].reshape(TILE, COLS), 1, 1)
         x = x_buf[PER * j : PER * (j + 1)].reshape(TILE, COLS).astype(F32)
@@ -191,7 +192,7 @@
         up = y[SLOT:PART]
         h = jnp.where(keep, gate / (1.0 + jnp.exp(-gate)) * up, 0.0).astype(BF16)
         for k in range(4):
-            out_ref[j ^ turn, k] = h
+            out_ref[k, j ^ turn] = h
 
 
 def hidden_of(received, gate_scale, up_scale):
@@ -214,7 +215,8 @@
     place = one_hot(iota((FFL, 4 * SLOT), 1) == unit + (SLOT - UNITS) * slot)
 
     def squeezed(member):
-        return dot(h_ref[member], place, 0, 1).astype(BF16)
+        h = jnp.concatenate([h_ref[k, member] for k in range(4)], axis=0)
+        return dot(h, place, 0, 1).astype(BF16)
 
     acc = dot(squeezed(me), own_ref[...], 1, 0)
     acc = acc + dot(squeezed(me ^ (1 + core)), fetched_ref[:, 0:COLS], 1, 0)
@@ -331,10 +333,10 @@
     sent, stats = hidden_of(received, gate_scale.reshape(1, FFL), up_scale.reshape(1, FFL))
     own = lax.dynamic_slice_in_dim(tokens, lax.axis_index(RA) * 16, 16, 0)
     sent, own = lax.optimization_barrier((sent, own))
-    hidden = lax.all_to_all(sent.reshape(16, SLOT, CHUNK), ("zl", "yl", "cb"), 0, 0, tiled=True)
+    hidden = lax.all_to_all(sent.reshape(16, SLOT, CHUNK), ("cb", "zl", "yl"), 0, 0, tiled=True)
     fetched = jnp.concatenate([beside, across], axis=1)
     other = lax.ppermute(fetched, "dp", swapped(2, 1))
-    partial = down(hidden.reshape(4, 4 * SLOT, CHUNK), (w0, fetched, other))
+    partial = down(hidden.reshape(4, 4, SLOT, CHUNK), (w0, fetched, other))
     pieces = lax.all_to_all(
         partial.reshape(16, 16, COLS), RA, 0, 0, axis_index_groups=spread_groups(), tiled=True
     )

time: 78.2 us -> 78.3 us (level)
    all_to_all x1, blocking collectives: 29.3 us -> 31.1 us  [local(): lax.all_to_all(partial.reshape(16, 16, COLS), RA, 0, 0, axis_index_groups...]
    all_to_all x1, blocking collectives: 10.7 us -> 8.86 us  [local(): parts = lax.all_to_all(part, 'cb', 0, 0, tiled=True)]
where the time goes in v9:
time: 78.3 us; the launch traced here: 77.7 us
  blocking collectives  40 us (51%)
  starting transfers between devices  20.8 us (27%)
  Pallas kernels  8.2 us (10%)
  waiting for transfers between devices  7.67 us (10%)
  local copies, waits for them, and re-layouts  0.87 us (1%)
    all_to_all x1, blocking collectives, local(): lax.all_to_all(partial.reshape(16, 16, COLS), RA, 0, 0, axis_index_groups...  31.1 us
    all_to_all x1, blocking collectives, local(): parts = lax.all_to_all(part, 'cb', 0, 0, tiled=True)  8.86 us
    ppermute x1, starting transfers between devices, local(): lax.ppermute(w0, ('zl', 'yl', 'dp'), [(i, i ^ (4 if i & 1 else 2)) for i...  6.92 us
    all_to_all x1, starting transfers between devices, local(): lax.all_to_all(sent.reshape(16, SLOT, CHUNK), ('cb', 'zl', 'yl'), 0, 0, t...  5.72 us
    pallas_call x1, Pallas kernels, project(): pl.pallas_call(project_kernel, in_specs=[hbm] * 5, out_specs=hbm, out_sha...  4.45 us
    all_to_all x1, starting transfers between devices, local(): received = lax.all_to_all(shares, 'cb', 0, 0, tiled=True)  4.3 us
    all_to_all x1, waiting for transfers between devices, local(): lax.all_to_all(sent.reshape(16, SLOT, CHUNK), ('cb', 'zl', 'yl'), 0, 0, t...  3.2 us
    all_to_all x1, waiting for transfers between devices, local(): received = lax.all_to_all(shares, 'cb', 0, 0, tiled=True)  2.56 us
  transfers between devices with their start and end apart: 5, of which 3 were waited for; matrix products, arithmetic and copies ran while one was open for 1% of the time, Pallas kernels for 2%

profile of v9, /device:TPU:8, one launch (start us, length us, event | category | flops | bytes accessed | tf_op | source)
XLA Modules:
  0.0 77.7 jit_solution(10403718002659557555)
XLA Ops:
  0.0 0.0 copy-start.7
  0.0 4.5 %project.1 = bf16[4,96,1024]{2,1,0:T(8,128)(2,1)} custom-call(bf16[4,2,4,2,16,1024]{5,4,3,2,1,0:T(8,128)(2,1)} %bitcast.24, f32[176,1024]{1,0:T(8,128)} %bitcast.25, f32[176,1024]{1,0:T(8,128)} %bitcast.26, f32[1,1024]{1,0:T(1,128)} %bitcast.15, f32[1,1024]{1,0:T(1,128)} %bitcast.17), custom_call_target="tpu_custom_call" | custom-call | tf_op jit(solution)/shard_map/project/pallas_call | solution.py:123
  4.5 0.0 copy-start.5
  4.5 0.0 copy-start.6
  4.5 4.3 %all-to-all-start = ((bf16[4,96,1024]{2,1,0:T(8,128)(2,1)}), bf16[4,96,1024]{2,1,0:T(8,128)(2,1)S(1)}, u32[]{:S(2)}, u32[]{:S(2)}) async-start(bf16[4,96,1024]{2,1,0:T(8,128)(2,1)} %project.1), calls=%async_computation | async-start | bytes 1572864 | tf_op jit(solution)/shard_map/all_to_all | solution.py:332
  8.8 0.0 copy-done.7
  8.8 6.9 %collective-permute-start = (bf16[176,1024]{1,0:T(8,128)(2,1)S(1)}, bf16[176,1024]{1,0:T(8,128)(2,1)S(1)}, u32[]{:S(2)}, u32[]{:S(2)}) collective-permute-start(bf16[176,1024]{1,0:T(8,128)(2,1)S(1)} %convert_element_type.3.own_ref), channel_id=1, source_target_pairs={{0,8},{1,65},{8,0},{9,73},{64,72},{65,1},{72,64},{73,9},{2,10},{3,... | collective-permute-start | bytes 1081352 | tf_op jit(solution)/shard_map/ppermute | solution.py:327
  15.8 1.9 %collective-permute-start.1 = (bf16[176,512]{1,0:T(8,128)(2,1)S(1)}, bf16[176,512]{1,0:T(8,128)(2,1)S(1)}, u32[]{:S(2)}, u32[]{:S(2)}) collective-permute-start(bf16[176,512]{1,0:T(8,128)(2,1)S(1)} %constant_dynamic-slice_fusion), channel_id=1, source_target_pairs={{0,72},{8,64},{64,8},{72,0},{1,73},{9,65},{65,9},{73,1},{2,74},{10... | collective-permute-start | bytes 540680 | tf_op jit(solution)/shard_map/ppermute | solution.py:329
  17.7 0.8 constant_dynamic-slice_fusion.1.x_ref
  18.5 2.6 %all-to-all-done.r_ref = bf16[4,96,1024]{2,1,0:T(8,128)(2,1)S(1)} async-done(((bf16[4,96,1024]{2,1,0:T(8,128)(2,1)}), bf16[4,96,1024]{2,1,0:T(8,128)(2,1)S(1)}, u32[]{:S(2)}, u32[]{:S(2)}) %all-to-all-start) | async-done | bytes 786464 | tf_op jit(solution)/shard_map/all_to_all | solution.py:332
  21.1 0.0 copy-done.5
  21.1 0.0 copy-done.6
  21.1 1.5 %hidden.1 = (bf16[4,4,48,256]{3,2,1,0:T(8,128)(2,1)}, f32[8,1024]{1,0:T(8,128)S(1)}) custom-call(bf16[4,96,1024]{2,1,0:T(8,128)(2,1)S(1)} %all-to-all-done.r_ref, f32[1,176]{1,0:T(1,128)S(1)} %bitcast.22, f32[1,176]{1,0:T(1,128)S(1)} %bitcast.23), custom_call_target="tpu_custom_call" | custom-call | tf_op jit(solution)/shard_map/hidden/pallas_call | solution.py:200
  22.6 5.7 %all-to-all-start.1 = ((bf16[16,48,256]{2,1,0:T(8,128)(2,1)}), bf16[16,48,256]{2,1,0:T(8,128)(2,1)S(1)}, u32[]{:S(2)}, u32[]{:S(2)}) async-start(bf16[16,48,256]{2,1,0:T(8,128)(2,1)} %bitcast.7), calls=%async_computation.1 | async-start | bytes 786432 | tf_op jit(solution)/shard_map/all_to_all | solution.py:336
  28.3 0.0 copy-start
  28.3 0.0 copy-start.1
  28.3 0.0 copy-start.2
  28.3 0.0 collective-permute-done
  28.4 0.0 collective-permute-done.1
  28.4 0.0 copy-start.3
  28.4 0.0 copy-start.4
  28.4 1.9 %collective-permute-start.2 = (bf16[176,1536]{1,0:T(8,128)(2,1)S(1)}, bf16[176,1536]{1,0:T(8,128)(2,1)S(1)}, u32[]{:S(2)}, u32[]{:S(2)}) collective-permute-start(bf16[176,1536]{1,0:T(8,128)(2,1)S(1)} %constant_dynamic-update-slice_fusion.fetched_ref), channel_id=1, source_target_pairs={{0,1},{1,0},{2,3},{3,2},{4,5},{5,4},{6,7},{7,6},{8,9},{9,8},{10,11... | collective-permute-start | bytes 1622024 | tf_op jit(solution)/shard_map/ppermute | solution.py:338
  30.3 1.9 %collective-permute-done.2.other_ref = bf16[176,1536]{1,0:T(8,128)(2,1)S(1)} collective-permute-done((bf16[176,1536]{1,0:T(8,128)(2,1)S(1)}, bf16[176,1536]{1,0:T(8,128)(2,1)S(1)}, u32[]{:S(2)}, u32[]{:S(2)}) %collective-permute-start.2) | collective-permute-done | bytes 540704 | tf_op jit(solution)/shard_map/ppermute | solution.py:338
  32.2 3.2 %all-to-all-done.1 = bf16[16,48,256]{2,1,0:T(8,128)(2,1)S(1)} async-done(((bf16[16,48,256]{2,1,0:T(8,128)(2,1)}), bf16[16,48,256]{2,1,0:T(8,128)(2,1)S(1)}, u32[]{:S(2)}, u32[]{:S(2)}) %all-to-all-start.1) | async-done | bytes 393248 | tf_op jit(solution)/shard_map/all_to_all | solution.py:336
  35.5 1.2 %down.1 = bf16[256,1024]{1,0:T(8,128)(2,1)S(1)} custom-call(bf16[4,4,48,256]{3,2,1,0:T(8,128)(2,1)S(1)} %bitcast.14, bf16[176,1024]{1,0:T(8,128)(2,1)S(1)} %convert_element_type.3.own_ref, bf16[176,1536]{1,0:T(8,128)(2,1)S(1)} %constant_dynamic-update-slice_fusion.fetched_ref, bf16[176,1536]{1,0:T(8,128)(2,1)S(1)} %collective-permute-done.2.other_ref), custom_call_target="tpu_custom_call" | custom-call | tf_op jit(solution)/shard_map/down/pallas_call | solution.py:233
  36.6 31.1 %all_to_all.20.r_ref = bf16[16,16,1024]{2,1,0:T(8,128)(2,1)S(1)} all-to-all(bf16[16,16,1024]{2,1,0:T(8,128)(2,1)S(1)} %bitcast.13), channel_id=1, replica_groups={{0,16,32,48,192,208,224,240,320,336,352,368,384,400,416,432},{8,24,40,5..., dimensions={0} | all-to-all | bytes 1048576 | tf_op jit(solution)/shard_map/all_to_all | solution.py:340
  67.8 0.0 copy-done
  67.8 0.0 copy-done.1
  67.8 0.0 copy-done.2
  67.8 0.3 mix.1
  68.1 8.9 %all_to_all.21.part_ref = f32[4,16,128]{2,1,0:T(8,128)S(1)} all-to-all(f32[4,16,128]{2,1,0:T(8,128)S(1)} %get-tuple-element.16), channel_id=1, replica_groups=mesh['Z'=4,'zl'=2,'Y'=4,'yl'=2,'cb'=4,'dp'=2] {'cb'}, dimensions={0} | all-to-all | bytes 65536 | tf_op jit(solution)/shard_map/all_to_all | solution.py:344
  77.0 0.0 copy-done.3
  77.0 0.0 copy-done.4
  77.0 0.8 %finish.1 = bf16[16,1024]{1,0:T(8,128)(2,1)} custom-call(f32[16,1024]{1,0:T(8,128)S(1)} %get-tuple-element.15.mixed_ref, f32[4,16,128]{2,1,0:T(8,128)S(1)} %all_to_all.21.part_ref, f32[1,1024]{1,0:T(1,128)S(1)} %bitcast.20, f32[1,1024]{1,0:T(1,128)S(1)} %bitcast.21), custom_call_target="tpu_custom_call" | custom-call | tf_op jit(solution)/shard_map/finish/pallas_call | solution.py:285
  (4 shorter events, 0.1 us)
Async XLA Ops:
  0.0 8.8 %copy-start.7 = (f32[176,1024]{1,0:T(8,128)S(1)}, f32[176,1024]{1,0:T(8,128)}, u32[]{:S(2)}) copy-start(f32[176,1024]{1,0:T(8,128)} %param.18) | copy-start | bytes 2162692
  4.5 16.6 %copy-start.5 = (f32[176]{0:T(256)S(1)}, f32[176]{0:T(256)}, u32[]{:S(2)}) copy-start(f32[176]{0:T(256)} %param.16) | copy-start | bytes 2116
  4.5 16.6 %copy-start.6 = (f32[176]{0:T(256)S(1)}, f32[176]{0:T(256)}, u32[]{:S(2)}) copy-start(f32[176]{0:T(256)} %param.17) | copy-start | bytes 2116
  4.5 16.6 %all-to-all-start = ((bf16[4,96,1024]{2,1,0:T(8,128)(2,1)}), bf16[4,96,1024]{2,1,0:T(8,128)(2,1)S(1)}, u32[]{:S(2)}, u32[]{:S(2)}) async-start(bf16[4,96,1024]{2,1,0:T(8,128)(2,1)} %project.1), calls=%async_computation | async-start | bytes 1572864 | tf_op jit(solution)/shard_map/all_to_all | solution.py:332
  8.8 19.5 %collective-permute-start = (bf16[176,1024]{1,0:T(8,128)(2,1)S(1)}, bf16[176,1024]{1,0:T(8,128)(2,1)S(1)}, u32[]{:S(2)}, u32[]{:S(2)}) collective-permute-start(bf16[176,1024]{1,0:T(8,128)(2,1)S(1)} %convert_element_type.3.own_ref), channel_id=1, source_target_pairs={{0,8},{1,65},{8,0},{9,73},{64,72},{65,1},{72,64},{73,9},{2,10},{3,... | collective-permute-start | bytes 1081352 | tf_op jit(solution)/shard_map/ppermute | solution.py:327
  15.8 12.6 %collective-permute-start.1 = (bf16[176,512]{1,0:T(8,128)(2,1)S(1)}, bf16[176,512]{1,0:T(8,128)(2,1)S(1)}, u32[]{:S(2)}, u32[]{:S(2)}) collective-permute-start(bf16[176,512]{1,0:T(8,128)(2,1)S(1)} %constant_dynamic-slice_fusion), channel_id=1, source_target_pairs={{0,72},{8,64},{64,8},{72,0},{1,73},{9,65},{65,9},{73,1},{2,74},{10... | collective-permute-start | bytes 540680 | tf_op jit(solution)/shard_map/ppermute | solution.py:329
  22.6 12.9 %all-to-all-start.1 = ((bf16[16,48,256]{2,1,0:T(8,128)(2,1)}), bf16[16,48,256]{2,1,0:T(8,128)(2,1)S(1)}, u32[]{:S(2)}, u32[]{:S(2)}) async-start(bf16[16,48,256]{2,1,0:T(8,128)(2,1)} %bitcast.7), calls=%async_computation.1 | async-start | bytes 786432 | tf_op jit(solution)/shard_map/all_to_all | solution.py:336
  28.3 39.5 %copy-start = (f32[1024]{0:T(1024)S(1)}, f32[1024]{0:T(1024)}, u32[]{:S(2)}) copy-start(f32[1024]{0:T(1024)} %param.12) | copy-start | bytes 12292
  28.3 39.5 %copy-start.1 = (f32[1024]{0:T(1024)S(1)}, f32[1024]{0:T(1024)}, u32[]{:S(2)}) copy-start(f32[1024]{0:T(1024)} %param.13) | copy-start | bytes 12292
  28.3 39.5 %copy-start.2 = (f32[1024]{0:T(1024)S(1)}, f32[1024]{0:T(1024)}, u32[]{:S(2)}) copy-start(f32[1024]{0:T(1024)} %param.19) | copy-start | bytes 12292
  28.4 48.6 %copy-start.3 = (f32[1024]{0:T(1024)S(1)}, f32[1024]{0:T(1024)}, u32[]{:S(2)}) copy-start(f32[1024]{0:T(1024)} %param.20) | copy-start | bytes 12292
  28.4 48.5 %copy-start.4 = (f32[1024]{0:T(1024)S(1)}, f32[1024]{0:T(1024)}, u32[]{:S(2)}) copy-start(f32[1024]{0:T(1024)} %param.21) | copy-start | bytes 12292
  28.4 3.8 %collective-permute-start.2 = (bf16[176,1536]{1,0:T(8,128)(2,1)S(1)}, bf16[176,1536]{1,0:T(8,128)(2,1)S(1)}, u32[]{:S(2)}, u32[]{:S(2)}) collective-permute-start(bf16[176,1536]{1,0:T(8,128)(2,1)S(1)} %constant_dynamic-update-slice_fusion.fetched_ref), channel_id=1, source_target_pairs={{0,1},{1,0},{2,3},{3,2},{4,5},{5,4},{6,7},{7,6},{8,9},{9,8},{10,11... | collective-permute-start | bytes 1622024 | tf_op jit(solution)/shard_map/ppermute | solution.py:338

commit v10 on v9

--- a/solution.py
+++ b/solution.py
@@ -50,15 +50,20 @@
     ]
     runs = ((0, 1), (1, 3), (3, 4))
     tokens = [
-        pltpu.make_async_copy(x_ref.at[a:b, (j // 2) ^ flipped(a), :, j % 2], x_buf.at[j, a:b], sems.at[4 + 3 * j + i])
+        pltpu.make_async_copy(
+            x_ref.at[a:b, (j // 2) ^ flipped(a), c:d, (j % 2) ^ flipped(c)],
+            x_buf.at[j, a:b, c:d],
+            sems.at[4 + 9 * j + 3 * i + k],
+        )
         for j in range(4)
         for i, (a, b) in enumerate(runs)
+        for k, (c, d) in enumerate(runs)
     ]
-    for copy in loads + tokens[: 3 * PER]:
+    for copy in loads + tokens[: 9 * PER]:
         copy.start()
     for copy in loads:
         copy.wait()
-    for copy in tokens[3 * PER :]:
+    for copy in tokens[9 * PER :]:
         copy.start()
 
     gain = gb_buf[0]
@@ -87,7 +92,7 @@
     stores = []
     for j in range(4 // PER):
         at = slice(TILE * j, TILE * (j + 1))
-        for copy in tokens[3 * PER * j : 3 * PER * (j + 1)]:
+        for copy in tokens[9 * PER * j : 9 * PER * (j + 1)]:
             copy.wait()
         part = dot(w_ref[...], x_buf[PER * j : PER * (j + 1)].reshape(TILE, COLS), 1, 1)
         x = x_buf[PER * j : PER * (j + 1)].reshape(TILE, COLS).astype(F32)
@@ -112,7 +117,7 @@
         for k in range(4):
             rows = slice(PART * k, PART * (k + 1))
             out_buf[k, :, at] = (part[rows] - col[rows] * m_row + extra).astype(BF16)
-        stores.append(pltpu.make_async_copy(out_buf.at[:, :, at], out_ref.at[:, :, at], sems.at[20 + j]))
+        stores.append(pltpu.make_async_copy(out_buf.at[:, :, at], out_ref.at[:, :, at], sems.at[40 + j]))
         stores[-1].start()
     for copy in stores:
         copy.wait()
@@ -133,7 +138,7 @@
             pltpu.VMEM((4, PART, ROWS), BF16),
             pltpu.VMEM((4 * PART, COLS), BF16),
             pltpu.VMEM((8, ROWS), F32),
-            pltpu.SemaphoreType.DMA((24,)),
+            pltpu.SemaphoreType.DMA((44,)),
         ],
         name="project",
     )(*[pltpu.with_memory_space_constraint(a, pltpu.HBM) for a in (tokens.reshape(4, 2, 4, 2, 16, COLS), gate_t, up_t, gain, bias)])
@@ -181,7 +186,7 @@
     scale = jnp.where(iota((PART, 1), 0) < SLOT, sc[:, 0:1] + sc[:, 1:2] + sc[:, 2:3], sc[:, 3:4] + sc[:, 4:5] + sc[:, 5:6])
 
     keep = iota((SLOT, CHUNK), 0) < UNITS
-    turn = 2 * flipped(lax.axis_index("Z"))
+    turn = 2 * flipped(lax.axis_index("Z")) + flipped(lax.axis_index("Y"))
     for j in range(4):
         at = slice(CHUNK * j, CHUNK * (j + 1))
         acc = jnp.zeros((PART, CHUNK), F32)
@@ -240,7 +245,7 @@
 
 
 def mix_kernel(r_ref, x_ref, stat_ref, gain_ref, bias_ref, scale_ref, mixed_ref, part_ref):
-    member = (lax.axis_index("zl") ^ flipped(lax.axis_index("Z"))) * 2 + lax.axis_index("yl")
+    member = (lax.axis_index("zl") ^ flipped(lax.axis_index("Z"))) * 2 + (lax.axis_index("yl") ^ flipped(lax.axis_index("Y")))
     at = member * CHUNK + (lax.axis_index("Z") * 4 + lax.axis_index("Y")) * 16
     branch = jnp.zeros((16, COLS), F32)
     for k in range(16):
@@ -297,7 +302,7 @@
 
 def spread_groups():
     return [
-        [(2 * z + (jz ^ flipped(z))) * 8 + 2 * y + jy for z in range(4) for y in range(4)]
+        [(2 * z + (jz ^ flipped(z))) * 8 + 2 * y + (jy ^ flipped(y)) for z in range(4) for y in range(4)]
         for jz in range(2)
         for jy in range(2)
     ]

time: 78.3 us -> 78.4 us (level)
  the two profiles are of different devices: /device:TPU:8 before, /device:TPU:1 now
where the time goes in v10:
time: 78.4 us; the launch traced here: 77.9 us
  blocking collectives  41.3 us (53%)
  starting transfers between devices  24 us (31%)
  Pallas kernels  8.4 us (11%)
  waiting for transfers between devices  3.2 us (4%)
  local copies, waits for them, and re-layouts  0.87 us (1%)
    all_to_all x1, blocking collectives, local(): lax.all_to_all(partial.reshape(16, 16, COLS), RA, 0, 0, axis_index_groups...  31.7 us
    all_to_all x1, blocking collectives, local(): parts = lax.all_to_all(part, 'cb', 0, 0, tiled=True)  9.53 us
    all_to_all x1, starting transfers between devices, local(): lax.all_to_all(sent.reshape(16, SLOT, CHUNK), ('cb', 'zl', 'yl'), 0, 0, t...  8.17 us
    all_to_all x1, starting transfers between devices, local(): received = lax.all_to_all(shares, 'cb', 0, 0, tiled=True)  4.85 us
    pallas_call x1, Pallas kernels, project(): pl.pallas_call(project_kernel, in_specs=[hbm] * 5, out_specs=hbm, out_sha...  4.66 us
    ppermute x1, starting transfers between devices, local(): other = lax.ppermute(fetched, 'dp', swapped(2, 1))  4.01 us
    ppermute x1, starting transfers between devices, local(): lax.ppermute(w0, ('zl', 'yl', 'dp'), [(i, i ^ (4 if i & 1 else 2)) for i...  4 us
    ppermute x1, starting transfers between devices, local(): across = lax.ppermute(half, ('zl', 'yl'), swapped(4, 3))  2.93 us
  transfers between devices with their start and end apart: 5, of which 3 were waited for; matrix products, arithmetic and copies ran while one was open for 1% of the time, Pallas kernels for 2%

profile of v10, /device:TPU:1, one launch (start us, length us, event | category | flops | bytes accessed | tf_op | source)
XLA Modules:
  0.0 77.9 jit_solution(14110305016525268606)
XLA Ops:
  0.0 0.0 copy-start.7
  0.0 4.7 %project.1 = bf16[4,96,1024]{2,1,0:T(8,128)(2,1)} custom-call(bf16[4,2,4,2,16,1024]{5,4,3,2,1,0:T(8,128)(2,1)} %bitcast.24, f32[176,1024]{1,0:T(8,128)} %bitcast.25, f32[176,1024]{1,0:T(8,128)} %bitcast.26, f32[1,1024]{1,0:T(1,128)} %bitcast.15, f32[1,1024]{1,0:T(1,128)} %bitcast.17), custom_call_target="tpu_custom_call" | custom-call | tf_op jit(solution)/shard_map/project/pallas_call | solution.py:128
  4.7 0.0 copy-start.5
  4.7 0.0 copy-start.6
  4.7 4.8 %all-to-all-start = ((bf16[4,96,1024]{2,1,0:T(8,128)(2,1)}), bf16[4,96,1024]{2,1,0:T(8,128)(2,1)S(1)}, u32[]{:S(2)}, u32[]{:S(2)}) async-start(bf16[4,96,1024]{2,1,0:T(8,128)(2,1)} %project.1), calls=%async_computation | async-start | bytes 1572864 | tf_op jit(solution)/shard_map/all_to_all | solution.py:337
  9.5 0.0 copy-done.7
  9.6 4.0 %collective-permute-start = (bf16[176,1024]{1,0:T(8,128)(2,1)S(1)}, bf16[176,1024]{1,0:T(8,128)(2,1)S(1)}, u32[]{:S(2)}, u32[]{:S(2)}) collective-permute-start(bf16[176,1024]{1,0:T(8,128)(2,1)S(1)} %convert_element_type.3.own_ref), channel_id=1, source_target_pairs={{0,8},{1,65},{8,0},{9,73},{64,72},{65,1},{72,64},{73,9},{2,10},{3,... | collective-permute-start | bytes 1081352 | tf_op jit(solution)/shard_map/ppermute | solution.py:332
  13.6 2.9 %collective-permute-start.1 = (bf16[176,512]{1,0:T(8,128)(2,1)S(1)}, bf16[176,512]{1,0:T(8,128)(2,1)S(1)}, u32[]{:S(2)}, u32[]{:S(2)}) collective-permute-start(bf16[176,512]{1,0:T(8,128)(2,1)S(1)} %constant_dynamic-slice_fusion), channel_id=1, source_target_pairs={{0,72},{8,64},{64,8},{72,0},{1,73},{9,65},{65,9},{73,1},{2,74},{10... | collective-permute-start | bytes 540680 | tf_op jit(solution)/shard_map/ppermute | solution.py:334
  16.6 0.8 constant_dynamic-slice_fusion.1.x_ref
  17.4 0.5 all-to-all-done.r_ref
  17.9 0.0 copy-done.5
  17.9 0.0 copy-done.6
  17.9 1.5 %hidden.1 = (bf16[4,4,48,256]{3,2,1,0:T(8,128)(2,1)}, f32[8,1024]{1,0:T(8,128)S(1)}) custom-call(bf16[4,96,1024]{2,1,0:T(8,128)(2,1)S(1)} %all-to-all-done.r_ref, f32[1,176]{1,0:T(1,128)S(1)} %bitcast.22, f32[1,176]{1,0:T(1,128)S(1)} %bitcast.23), custom_call_target="tpu_custom_call" | custom-call | tf_op jit(solution)/shard_map/hidden/pallas_call | solution.py:205
  19.4 8.2 %all-to-all-start.1 = ((bf16[16,48,256]{2,1,0:T(8,128)(2,1)}), bf16[16,48,256]{2,1,0:T(8,128)(2,1)S(1)}, u32[]{:S(2)}, u32[]{:S(2)}) async-start(bf16[16,48,256]{2,1,0:T(8,128)(2,1)} %bitcast.7), calls=%async_computation.1 | async-start | bytes 786432 | tf_op jit(solution)/shard_map/all_to_all | solution.py:341
  27.5 0.0 copy-start
  27.6 0.0 copy-start.1
  27.6 0.0 copy-start.2
  27.6 0.0 collective-permute-done
  27.6 0.0 collective-permute-done.1
  27.7 0.0 copy-start.3
  27.7 0.0 copy-start.4
  27.7 4.0 %collective-permute-start.2 = (bf16[176,1536]{1,0:T(8,128)(2,1)S(1)}, bf16[176,1536]{1,0:T(8,128)(2,1)S(1)}, u32[]{:S(2)}, u32[]{:S(2)}) collective-permute-start(bf16[176,1536]{1,0:T(8,128)(2,1)S(1)} %constant_dynamic-update-slice_fusion.fetched_ref), channel_id=1, source_target_pairs={{0,1},{1,0},{2,3},{3,2},{4,5},{5,4},{6,7},{7,6},{8,9},{9,8},{10,11... | collective-permute-start | bytes 1622024 | tf_op jit(solution)/shard_map/ppermute | solution.py:343
  31.7 1.5 %collective-permute-done.2.other_ref = bf16[176,1536]{1,0:T(8,128)(2,1)S(1)} collective-permute-done((bf16[176,1536]{1,0:T(8,128)(2,1)S(1)}, bf16[176,1536]{1,0:T(8,128)(2,1)S(1)}, u32[]{:S(2)}, u32[]{:S(2)}) %collective-permute-start.2) | collective-permute-done | bytes 540704 | tf_op jit(solution)/shard_map/ppermute | solution.py:343
  33.2 1.1 %all-to-all-done.1 = bf16[16,48,256]{2,1,0:T(8,128)(2,1)S(1)} async-done(((bf16[16,48,256]{2,1,0:T(8,128)(2,1)}), bf16[16,48,256]{2,1,0:T(8,128)(2,1)S(1)}, u32[]{:S(2)}, u32[]{:S(2)}) %all-to-all-start.1) | async-done | bytes 393248 | tf_op jit(solution)/shard_map/all_to_all | solution.py:341
  34.4 1.2 %down.1 = bf16[256,1024]{1,0:T(8,128)(2,1)S(1)} custom-call(bf16[4,4,48,256]{3,2,1,0:T(8,128)(2,1)S(1)} %bitcast.14, bf16[176,1024]{1,0:T(8,128)(2,1)S(1)} %convert_element_type.3.own_ref, bf16[176,1536]{1,0:T(8,128)(2,1)S(1)} %constant_dynamic-update-slice_fusion.fetched_ref, bf16[176,1536]{1,0:T(8,128)(2,1)S(1)} %collective-permute-done.2.other_ref), custom_call_target="tpu_custom_call" | custom-call | tf_op jit(solution)/shard_map/down/pallas_call | solution.py:238
  35.6 31.7 %all_to_all.20.r_ref = bf16[16,16,1024]{2,1,0:T(8,128)(2,1)S(1)} all-to-all(bf16[16,16,1024]{2,1,0:T(8,128)(2,1)S(1)} %bitcast.13), channel_id=1, replica_groups={{0,24,40,48,192,216,232,240,320,344,360,368,384,408,424,432},{8,16,32,5..., dimensions={0} | all-to-all | bytes 1048576 | tf_op jit(solution)/shard_map/all_to_all | solution.py:345
  67.3 0.0 copy-done
  67.3 0.0 copy-done.1
  67.3 0.0 copy-done.2
  67.3 0.3 mix.1
  67.6 9.5 %all_to_all.21.part_ref = f32[4,16,128]{2,1,0:T(8,128)S(1)} all-to-all(f32[4,16,128]{2,1,0:T(8,128)S(1)} %get-tuple-element.16), channel_id=1, replica_groups=mesh['Z'=4,'zl'=2,'Y'=4,'yl'=2,'cb'=4,'dp'=2] {'cb'}, dimensions={0} | all-to-all | bytes 65536 | tf_op jit(solution)/shard_map/all_to_all | solution.py:349
  77.1 0.0 copy-done.3
  77.1 0.0 copy-done.4
  77.2 0.8 %finish.1 = bf16[16,1024]{1,0:T(8,128)(2,1)} custom-call(f32[16,1024]{1,0:T(8,128)S(1)} %get-tuple-element.15.mixed_ref, f32[4,16,128]{2,1,0:T(8,128)S(1)} %all_to_all.21.part_ref, f32[1,1024]{1,0:T(1,128)S(1)} %bitcast.20, f32[1,1024]{1,0:T(1,128)S(1)} %bitcast.21), custom_call_target="tpu_custom_call" | custom-call | tf_op jit(solution)/shard_map/finish/pallas_call | solution.py:290
  (4 shorter events, 0.1 us)
Async XLA Ops:
  0.0 9.5 %copy-start.7 = (f32[176,1024]{1,0:T(8,128)S(1)}, f32[176,1024]{1,0:T(8,128)}, u32[]{:S(2)}) copy-start(f32[176,1024]{1,0:T(8,128)} %param.18) | copy-start | bytes 2162692
  4.7 13.2 %copy-start.5 = (f32[176]{0:T(256)S(1)}, f32[176]{0:T(256)}, u32[]{:S(2)}) copy-start(f32[176]{0:T(256)} %param.16) | copy-start | bytes 2116
  4.7 13.2 %copy-start.6 = (f32[176]{0:T(256)S(1)}, f32[176]{0:T(256)}, u32[]{:S(2)}) copy-start(f32[176]{0:T(256)} %param.17) | copy-start | bytes 2116
  4.7 13.2 %all-to-all-start = ((bf16[4,96,1024]{2,1,0:T(8,128)(2,1)}), bf16[4,96,1024]{2,1,0:T(8,128)(2,1)S(1)}, u32[]{:S(2)}, u32[]{:S(2)}) async-start(bf16[4,96,1024]{2,1,0:T(8,128)(2,1)} %project.1), calls=%async_computation | async-start | bytes 1572864 | tf_op jit(solution)/shard_map/all_to_all | solution.py:337
  9.6 18.0 %collective-permute-start = (bf16[176,1024]{1,0:T(8,128)(2,1)S(1)}, bf16[176,1024]{1,0:T(8,128)(2,1)S(1)}, u32[]{:S(2)}, u32[]{:S(2)}) collective-permute-start(bf16[176,1024]{1,0:T(8,128)(2,1)S(1)} %convert_element_type.3.own_ref), channel_id=1, source_target_pairs={{0,8},{1,65},{8,0},{9,73},{64,72},{65,1},{72,64},{73,9},{2,10},{3,... | collective-permute-start | bytes 1081352 | tf_op jit(solution)/shard_map/ppermute | solution.py:332
  13.6 14.0 %collective-permute-start.1 = (bf16[176,512]{1,0:T(8,128)(2,1)S(1)}, bf16[176,512]{1,0:T(8,128)(2,1)S(1)}, u32[]{:S(2)}, u32[]{:S(2)}) collective-permute-start(bf16[176,512]{1,0:T(8,128)(2,1)S(1)} %constant_dynamic-slice_fusion), channel_id=1, source_target_pairs={{0,72},{8,64},{64,8},{72,0},{1,73},{9,65},{65,9},{73,1},{2,74},{10... | collective-permute-start | bytes 540680 | tf_op jit(solution)/shard_map/ppermute | solution.py:334
  19.4 15.0 %all-to-all-start.1 = ((bf16[16,48,256]{2,1,0:T(8,128)(2,1)}), bf16[16,48,256]{2,1,0:T(8,128)(2,1)S(1)}, u32[]{:S(2)}, u32[]{:S(2)}) async-start(bf16[16,48,256]{2,1,0:T(8,128)(2,1)} %bitcast.7), calls=%async_computation.1 | async-start | bytes 786432 | tf_op jit(solution)/shard_map/all_to_all | solution.py:341
  27.5 39.8 %copy-start = (f32[1024]{0:T(1024)S(1)}, f32[1024]{0:T(1024)}, u32[]{:S(2)}) copy-start(f32[1024]{0:T(1024)} %param.12) | copy-start | bytes 12292
  27.6 39.8 %copy-start.1 = (f32[1024]{0:T(1024)S(1)}, f32[1024]{0:T(1024)}, u32[]{:S(2)}) copy-start(f32[1024]{0:T(1024)} %param.13) | copy-start | bytes 12292
  27.6 39.7 %copy-start.2 = (f32[1024]{0:T(1024)S(1)}, f32[1024]{0:T(1024)}, u32[]{:S(2)}) copy-start(f32[1024]{0:T(1024)} %param.19) | copy-start | bytes 12292
  27.7 49.5 %copy-start.3 = (f32[1024]{0:T(1024)S(1)}, f32[1024]{0:T(1024)}, u32[]{:S(2)}) copy-start(f32[1024]{0:T(1024)} %param.20) | copy-start | bytes 12292
  27.7 49.5 %copy-start.4 = (f32[1024]{0:T(1024)S(1)}, f32[1024]{0:T(1024)}, u32[]{:S(2)}) copy-start(f32[1024]{0:T(1024)} %param.21) | copy-start | bytes 12292
  27.7 5.6 %collective-permute-start.2 = (bf16[176,1536]{1,0:T(8,128)(2,1)S(1)}, bf16[176,1536]{1,0:T(8,128)(2,1)S(1)}, u32[]{:S(2)}, u32[]{:S(2)}) collective-permute-start(bf16[176,1536]{1,0:T(8,128)(2,1)S(1)} %constant_dynamic-update-slice_fusion.fetched_ref), channel_id=1, source_target_pairs={{0,1},{1,0},{2,3},{3,2},{4,5},{5,4},{6,7},{7,6},{8,9},{9,8},{10,11... | collective-permute-start | bytes 1622024 | tf_op jit(solution)/shard_map/ppermute | solution.py:343
